TPU v7x, 256 devices: a whole 4x4x8 slice. The times are simulated.
256 devices in a mesh: ep: 32 (over z, x), tp: 8 (over y, core).
Axes of the slice: x: 4, y: 4, z: 8, core: 2. Of those that a mesh axis runs over, the one named last changes fastest.
Arguments:
- tokens: bfloat16 [768, 4096], P('ep'), may hold values from -6 to 6
- delta_state: float32 [768, 16, 128, 128], P('ep', 'tp'), may hold values from -0.625 to 0.625
- attn_gain: float32 [4096], replicated, may hold values from 0.1 to 1.9
- query_weight: bfloat16 [4096, 2048], P('ep', 'tp'), may hold values from -0.09375 to 0.09375
- key_weight: bfloat16 [4096, 2048], P('ep', 'tp'), may hold values from -0.09375 to 0.09375
- value_weight: bfloat16 [4096, 2048], P('ep', 'tp'), may hold values from -0.09375 to 0.09375
- decay_weight: bfloat16 [4096, 16], replicated, may hold values from -0.09375 to 0.09375
- beta_weight: bfloat16 [4096, 16], replicated, may hold values from -0.09375 to 0.09375
- decay_rate: float32 [16], P('tp'), may hold values from 0.05 to 3
- head_gain: float32 [128], replicated, may hold values from 0.1 to 1.9
- output_weight: bfloat16 [2048, 4096], P('tp'), may hold values from -0.125 to 0.125
- ffn_gain: float32 [4096], replicated, may hold values from 0.1 to 1.9
- expert_ids: int32 [768, 2], P('ep'), may hold values from 0 to 31, all different within a row; in each aligned block of 24 rows (0 to 23, 24 to 47, ...) at most 3 rows name the same one
- group_prob: float32 [768], P('ep'), may hold values from 0.3 to 1
- expert_logit: float32 [768, 2], P('ep'), may hold values from -8 to 8
- expert_gate: bfloat16 [32, 4096, 1024], P('ep', None, 'tp'), may hold values from -0.09375 to 0.09375
- expert_up: bfloat16 [32, 4096, 1024], P('ep', None, 'tp'), may hold values from -0.09375 to 0.09375
- expert_down: bfloat16 [32, 1024, 4096], P('ep', 'tp'), may hold values from -0.1875 to 0.1875
- dense_gate: bfloat16 [4096, 4096], P('tp', 'ep'), may hold values from -0.09375 to 0.09375
- dense_up: bfloat16 [4096, 4096], P('tp', 'ep'), may hold values from -0.09375 to 0.09375
- dense_down: bfloat16 [4096, 4096], P('ep', 'tp'), may hold values from -0.09375 to 0.09375
- dense_mix: float32 [4096], P('tp'), may hold values from -3 to 3
Outputs:
- mixed_out: bfloat16 [768, 4096], P('ep', 'tp')
- new_state: float32 [768, 16, 128, 128], P('ep', 'tp')
Inputs may be any that keep to these rules, and one draw needn't show every extreme that they name: `expert_ids`: each row names 2 different experts. Among the rows of one device (aligned blocks of 24 rows) no expert is named by more than 3 rows, and in every draw some expert reaches 3 in some block.
All inputs are finite; a program needn't handle non-finite values.
Results may differ from a plain program's by a relative error of at most 0.02.
Values may be sent and summed in bfloat16 or wider, within the bound.
No kernel may reach another device: no remote copies, remote signals or barrier semaphores. Data moves between devices by JAX's collectives and lax.ppermute only.
A program may use at most 64 MiB of HBM per device.

v0:
```python
import jax
import jax.numpy as jnp
from jax import lax
from jax.experimental import pallas as pl
from jax.experimental.pallas import tpu as pltpu
from jax.sharding import Mesh, PartitionSpec as P

EPS = 1e-06
BF = jnp.bfloat16
F32 = jnp.float32
NZ, NX, NT = 8, 4, 8
CAP = 3
MIB = 1 << 20


def exchange(tiles, axes):
    return lax.all_to_all(tiles, axes, split_axis=0, concat_axis=0, tiled=True)


def from_neighbours(shard, axis):
    count = lax.axis_size(axis)
    parts = [shard]
    for step in range(1, count):
        pairs = [(source, (source - step) % count) for source in range(count)]
        parts.append(lax.ppermute(shard, axis, pairs))
    return parts


def unit_rows(values):
    return values * lax.rsqrt(jnp.sum(values * values, axis=-1, keepdims=True) + EPS)


def silu(values):
    return values / (1.0 + jnp.exp(-values))


class Late:
    def __init__(self, source, near, done):
        self.near = near
        self.copy = pltpu.make_async_copy(source, near, done)
        self.copy.start()
        self.waits = True

    def arrive(self):
        if self.waits:
            self.copy.wait()
            self.waits = False
        return self.near

    def __getitem__(self, where):
        return self.arrive()[where]

    @property
    def shape(self):
        return self.near.shape


def kernel(
    body, outs, *args, far=(), plain=(), parts=None, far_outs=(), scratch=(), flops=0, limit=16
):
    parts = parts or {}
    far = tuple(far)
    nears = [parts[n][0] if n in parts else args[n].shape for n in far]

    def run(*refs):
        sides = [lax.axis_index(name) for name in ("z", "x", "y", "c")]
        index = (sides[0], sides[1], sides[2] * 2 + sides[3])
        refs = list(refs)
        ins, refs = refs[: len(args)], refs[len(args) :]
        dones = refs.pop() if far else None
        buffers = refs[len(refs) - len(far) :]
        refs = refs[: len(refs) - len(far)]
        for place, number in enumerate(far):
            source = ins[number]
            if number in parts:
                source = parts[number][1](source, index)
            ins[number] = Late(source, buffers[place], dones.at[place])
        body(index, *ins, *refs)
        for number in far:
            ins[number].arrive()

    specs = [
        pl.BlockSpec(memory_space=pltpu.HBM if number in far or number in plain else pltpu.VMEM)
        for number in range(len(args))
    ]
    out_specs = [
        pl.BlockSpec(memory_space=pltpu.HBM if number in far_outs else pltpu.VMEM)
        for number in range(len(outs))
    ]
    scratches = list(scratch) + [pltpu.VMEM(near, args[n].dtype) for n, near in zip(far, nears)]
    if far:
        scratches.append(pltpu.SemaphoreType.DMA((len(far),)))
    return pl.pallas_call(
        run,
        out_shape=outs,
        in_specs=specs,
        out_specs=out_specs,
        scratch_shapes=scratches,
        cost_estimate=pl.CostEstimate(flops=flops, bytes_accessed=0, transcendentals=0),
        compiler_params=pltpu.CompilerParams(vmem_limit_bytes=limit * MIB),
    )(*args)


def wrapped(value, count):
    return jnp.where(value >= count, value - count, value)


def spread_body(index, tokens, gain, query, key, value, out, weights, packed):
    cols = query.shape[1]
    copies = []
    for place, weight in enumerate((query, key, value)):
        target = weights.at[:, place * cols : (place + 1) * cols]
        copies.append(pltpu.make_async_copy(weight, target, packed.at[place]))
        copies[-1].start()
    block = out.shape[2]
    for z in range(NZ):
        cols = slice(z * block, (z + 1) * block)
        out[z] = (tokens[:, cols].astype(F32) * gain[:, cols]).astype(BF)
    for copy in copies:
        copy.wait()


def pack_body(index, after, gate, up, down, out, packed):
    block, size = gate.shape
    half = down.shape[1] // 2
    moves = (
        (gate, out.at[:block, :size]),
        (up, out.at[:block, size:]),
        (down.at[:, :half], out.at[block : block + size, :]),
        (down.at[:, half:], out.at[block + size :, :]),
    )
    copies = [
        pltpu.make_async_copy(source, target, packed.at[place])
        for place, (source, target) in enumerate(moves)
    ]
    for copy in copies:
        copy.start()
    for copy in copies:
        copy.wait()


def turned(row, rows):
    shape = (rows, row.shape[1])
    same = lax.broadcasted_iota(jnp.int32, shape, 0) == lax.broadcasted_iota(jnp.int32, shape, 1)
    return jnp.sum(jnp.where(same, row, 0.0), axis=1, keepdims=True)


def prepare_body(
    index, tokens, gain, decay_weight, beta_weight, rate, ids, prob, logit, meta, factors
):
    rows, width = tokens.shape
    block = meta.shape[1]
    wide = tokens[...].astype(F32)
    row_scale = lax.rsqrt(jnp.sum(wide * wide, axis=1, keepdims=True) / width + EPS)
    gained = (wide * gain[...]).astype(BF)
    over_width = (((1,), (1,)), ((), ()))
    heads = rate.shape[1]
    factor_lane = lax.broadcasted_iota(jnp.int32, factors.shape, 1)
    table = jnp.where(factor_lane == 0, row_scale, 0.0)

    def own_heads(weight):
        product = lax.dot_general(gained, weight[...], over_width, preferred_element_type=F32)
        lane = lax.broadcasted_iota(jnp.int32, product.shape, 1)
        columns = []
        for h in range(heads):
            own = lane == index[2] * heads + h
            columns.append(jnp.sum(jnp.where(own, product, 0.0), axis=1, keepdims=True) * row_scale)
        return columns

    for h, column in enumerate(own_heads(decay_weight)):
        soft = jnp.maximum(column, 0.0) + jnp.log1p(jnp.exp(-jnp.abs(column)))
        table = jnp.where(factor_lane == 1 + h, jnp.exp(-rate[:, h : h + 1] * soft), table)
    for h, column in enumerate(own_heads(beta_weight)):
        table = jnp.where(factor_lane == 1 + heads + h, 1.0 / (1.0 + jnp.exp(-column)), table)
    factors[...] = table

    picks = [ids[k : k + 1, :].astype(F32) for k in range(2)]
    pick_cols = [turned(pick, rows) for pick in picks]
    shape = (rows, rows)
    earlier = lax.broadcasted_iota(jnp.int32, shape, 0) < lax.broadcasted_iota(jnp.int32, shape, 1)
    powers = [jnp.exp(logit[k : k + 1, :]) for k in range(2)]
    total = powers[0] + powers[1]
    lines = []
    for k in range(2):
        named = jnp.zeros(shape, F32)
        for column in pick_cols:
            named = named + jnp.where(earlier & (column == picks[k]), 1.0, 0.0)
        lines.append(picks[k] * CAP + jnp.sum(named, axis=0, keepdims=True))
    for k in range(2):
        route = prob[...] * powers[k] / total
        high = route.astype(BF).astype(F32)
        lines += [high, route - high]
    line = lax.broadcasted_iota(jnp.int32, (8, rows), 0)
    table = jnp.zeros((8, rows), F32)
    for number, values in enumerate(lines):
        table = jnp.where(line == number, values, table)
    shape = (rows, block)
    lane = lax.broadcasted_iota(jnp.int32, shape, 1)
    spot = lane == lax.broadcasted_iota(jnp.int32, shape, 0) + index[0] * rows
    spot = jnp.where(spot, 1.0, 0.0).astype(BF)
    meta[...] = jnp.dot(table.astype(BF), spot, preferred_element_type=F32).astype(BF)


def project_body(index, arrived, w0, w1, w2, w3, out):
    groups, rows, _ = arrived.shape
    total = None
    for step, weight in enumerate((w0, w1, w2, w3)):
        size = weight.shape[0]
        place = pl.multiple_of(wrapped(index[1] + step, NX) * size, size)
        left = arrived[:, :, pl.ds(place, size)].astype(F32).reshape(groups * rows, size).astype(BF)
        part = jnp.dot(left, weight[...], preferred_element_type=F32)
        total = part if total is None else total + part
    out[...] = total.reshape(groups, rows, -1).astype(BF)


def state_body(
    index, arrived, factors, state, head_gain, weight, new_state, out, read, fresh, stored
):
    rows, heads, size = state.shape[:3]
    cols = heads * size
    summed = arrived[0].astype(F32)
    for z in range(1, NZ):
        summed = summed + arrived[z].astype(F32)
    summed = summed * factors[:, 0:1]
    parts = []
    for h in range(heads):
        query = unit_rows(summed[:, h * size : (h + 1) * size]) * size ** (-0.5)
        key = unit_rows(summed[:, cols + h * size : cols + (h + 1) * size])
        value = summed[:, 2 * cols + h * size : 2 * cols + (h + 1) * size]
        both = jnp.sum(query * key, axis=1, keepdims=True)
        parts.append((query.T, key.T, value, both))
    batch = rows // stored.shape[0]
    stores = []
    for b in range(rows):
        for h, (query_cols, key_cols, value, both) in enumerate(parts):
            old = state[b, h]
            key_col = key_cols[:, b : b + 1]
            query_col = query_cols[:, b : b + 1]
            fade = factors[b : b + 1, 1 + h : 2 + h]
            recalled = jnp.sum(key_col * old, axis=0, keepdims=True)
            asked = jnp.sum(query_col * old, axis=0, keepdims=True)
            gate = factors[b : b + 1, 1 + heads + h : 2 + heads + h]
            correction = gate * (value[b : b + 1] - fade * recalled)
            fresh[b, h] = fade * old + key_col * correction
            read[b : b + 1, h * size : (h + 1) * size] = (
                fade * asked + both[b : b + 1] * correction
            )
        if (b + 1) % batch == 0:
            group = pl.ds(b + 1 - batch, batch)
            stores.append(
                pltpu.make_async_copy(fresh.at[group], new_state.at[group], stored.at[b // batch])
            )
            stores[-1].start()
    head_rows = []
    for h in range(heads):
        result = read[:, h * size : (h + 1) * size]
        mean_sq = jnp.mean(result * result, axis=1, keepdims=True)
        head_rows.append(result * lax.rsqrt(mean_sq + EPS) * head_gain[...])
    left = jnp.concatenate(head_rows, axis=1).astype(BF)
    block = out.shape[2]
    for t in range(NT):
        right = weight[:, t * block : (t + 1) * block]
        out[t] = jnp.dot(left, right, preferred_element_type=F32).astype(BF)
    for store in stores:
        store.wait()


def middle_body(index, arrived, tokens, meta, middle, out):
    block = middle.shape[1]
    rows = middle.shape[0]
    summed = arrived[0].astype(F32)
    for t in range(1, NT):
        summed = summed + arrived[t].astype(F32)
    total = tokens[...].astype(F32) + summed
    middle[...] = total
    narrow = total.astype(BF)
    for z in range(NZ):
        out[z, :rows, :] = narrow
        out[z, rows:, :] = meta[...]


def slots_of(route, zi):
    tokens = route.shape[1]
    lane = lax.broadcasted_iota(jnp.int32, (1, tokens), 1)
    source = jnp.zeros((1, tokens), jnp.int32)
    for z in range(1, NZ):
        source = source + jnp.where(lane >= z * (tokens // NZ), 1, 0)
    slots = []
    for k in range(2):
        code = route[k : k + 1, :].astype(jnp.int32) - zi * (NX * CAP)
        expert = jnp.zeros((1, tokens), jnp.int32)
        for x in range(1, NX):
            expert = expert + jnp.where(code >= x * CAP, 1, 0)
        slot = expert * (NZ * CAP) + source * CAP + (code - expert * CAP)
        slots.append(jnp.where((code >= 0) & (code < NX * CAP), slot, -1))
    return slots


def dispatch_body(index, arrived, gain, g0, g1, g2, g3, out, route):
    rows = out.shape[2] - 8
    rows = rows // 3
    tokens = NZ * rows
    block = arrived.shape[2]
    half = block // 2
    wide = arrived[:, :rows, :].astype(F32).reshape(tokens, block)
    narrow = wide.astype(BF)
    routing = arrived[0, rows:, :tokens].astype(F32)
    for z in range(1, NZ):
        routing = routing + arrived[z, rows:, :tokens].astype(F32)
    route[...] = routing
    slot0, slot1 = slots_of(routing, index[0])
    place = lax.broadcasted_iota(jnp.int32, (NX * rows, tokens), 0)
    picks = jnp.where((place == slot0) | (place == slot1), 1.0, 0.0).astype(BF)
    chosen = jnp.dot(picks, narrow, preferred_element_type=F32).astype(BF)
    square = lax.dot_general(
        jnp.ones((8, block), F32),
        wide * wide,
        (((1,), (1,)), ((), ())),
        precision=lax.Precision.HIGHEST,
        preferred_element_type=F32,
    )
    high = square.astype(BF).astype(F32)
    first = lax.broadcasted_iota(jnp.int32, square.shape, 0) == 0
    square = jnp.where(first, high, square - high).astype(BF)
    for x in range(NX):
        own = chosen[x * rows : (x + 1) * rows]
        for t in range(NT):
            out[x, t, :rows, :] = own[:, :half]
            out[x, t, rows : 2 * rows, :] = own[:, half:]
            out[x, t, 3 * rows :, :tokens] = square
            out[x, t, 3 * rows :, tokens:] = jnp.zeros((8, half - tokens), BF)
    scaled = (wide * gain[...]).astype(BF)
    for step, weight in enumerate((g0, g1, g2, g3)):
        part = jnp.dot(scaled, weight[...], preferred_element_type=F32)
        x = wrapped(index[1] + step, NX)
        out[x, :, 2 * rows : 3 * rows, :] = part.reshape(NT, rows, half).astype(BF)


def expert_body(index, arrived, gain, gate, up, down, out):
    rows = out.shape[2]
    block = out.shape[3] - 128
    half = block // 2
    width = gate.shape[0]
    slots = NX * rows
    squares = jnp.zeros((slots, half), F32)
    gate_sum = jnp.zeros((slots, gate.shape[1]), F32)
    up_sum = jnp.zeros((slots, gate.shape[1]), F32)
    for t in range(NT):
        for part in range(2):
            wide = arrived[:, t, part * rows : (part + 1) * rows, :].astype(F32).reshape(slots, half)
            squares = squares + wide * wide
            place = t * block + part * half
            left = (wide * gain[:, place : place + half]).astype(BF)
            gate_sum += jnp.dot(left, gate[place : place + half, :], preferred_element_type=F32)
            up_sum += jnp.dot(left, up[place : place + half, :], preferred_element_type=F32)
    scale = lax.rsqrt(jnp.sum(squares, axis=1, keepdims=True) / width + EPS)
    hidden = (silu(gate_sum * scale) * (up_sum * scale)).astype(BF)
    for t in range(NT):
        result = jnp.dot(hidden, down[:, t * block : (t + 1) * block], preferred_element_type=F32)
        out[:, t, :, :block] = result.reshape(NX, rows, block).astype(BF)
    tokens = NZ * rows
    lane = lax.broadcasted_iota(jnp.int32, (rows, tokens), 1)
    own = lane == lax.broadcasted_iota(jnp.int32, (rows, tokens), 0) + index[2] * rows
    for x in range(NX):
        summed = arrived[x, 0, 2 * rows : 3 * rows, :].astype(F32)
        square = arrived[x, 0, 3 * rows :, :tokens].astype(F32)
        for t in range(1, NT):
            summed = summed + arrived[x, t, 2 * rows : 3 * rows, :].astype(F32)
            square = square + arrived[x, t, 3 * rows :, :tokens].astype(F32)
        square = square[0:1, :] + square[1:2, :]
        square = jnp.sum(jnp.where(own, square, 0.0), axis=1, keepdims=True)
        summed = summed * lax.rsqrt(square / width + EPS)
        result = (silu(summed[:, : half // 2]) * summed[:, half // 2 :]).astype(BF)
        for t in range(NT):
            out[x, t, :, block:] = result


def combine_body(index, arrived, route, d0, d1, d2, d3, mix, out):
    rows = arrived.shape[2]
    block = out.shape[2]
    tokens = NZ * rows
    results = []
    for x in range(NX):
        summed = arrived[x, 0, :, :block].astype(F32)
        for t in range(1, NT):
            summed = summed + arrived[x, t, :, :block].astype(F32)
        results.append(summed)
    results = jnp.concatenate(results, axis=0).astype(BF)
    routing = route[...]
    slot0, slot1 = slots_of(routing, index[0])
    place = lax.broadcasted_iota(jnp.int32, (NX * rows, tokens), 0)
    mixed = jnp.zeros((tokens, block), F32)
    for k in range(2):
        share = jnp.where(place == slot0, routing[2 + k : 3 + k, :], 0.0)
        share = jnp.where(place == slot1, routing[4 + k : 5 + k, :], share).astype(BF)
        mixed += lax.dot_general(
            share, results, (((0,), (0,)), ((), ())), preferred_element_type=F32
        )
    lower = jnp.zeros((tokens, block // 2), F32)
    upper = jnp.zeros((tokens, block // 2), F32)
    for step, weight in enumerate((d0, d1, d2, d3)):
        x = wrapped(index[1] + step, NX)
        left = arrived[x, :, :, block:].astype(F32).reshape(tokens, -1).astype(BF)
        size = left.shape[1]
        lower += jnp.dot(left, weight[:size, :], preferred_element_type=F32)
        upper += jnp.dot(left, weight[size:, :], preferred_element_type=F32)
    gate = 1.0 / (1.0 + jnp.exp(-mix[...]))
    dense = jnp.concatenate((lower, upper), axis=1)
    out[...] = (gate * dense + mixed).reshape(NZ, rows, block).astype(BF)


def final_body(index, arrived, middle, out):
    summed = arrived[0].astype(F32)
    for z in range(1, NZ):
        summed = summed + arrived[z].astype(F32)
    out[...] = (middle[...] + summed).astype(BF)


def per_device(
    tokens,
    delta_state,
    attn_gain,
    query_weight,
    key_weight,
    value_weight,
    decay_weight,
    beta_weight,
    decay_rate,
    head_gain,
    output_weight,
    ffn_gain,
    expert_ids,
    group_prob,
    expert_logit,
    expert_gate,
    expert_up,
    expert_down,
    dense_gate,
    dense_up,
    dense_down,
    dense_mix,
):
    rows, width = tokens.shape
    heads, size = delta_state.shape[1:3]
    cols = heads * size
    block = width // NT
    half = block // 2

    def shape(*dims, dtype=BF):
        return jax.ShapeDtypeStruct(dims, dtype)

    def own_block(ref, index):
        place = pl.multiple_of(index[2] * block, block)
        return ref.at[:, pl.ds(place, block)]

    message, own_weights = kernel(
        spread_body,
        (shape(NZ, rows, block), shape(query_weight.shape[0], 3 * cols)),
        tokens,
        attn_gain[None],
        query_weight,
        key_weight,
        value_weight,
        far=(0, 1),
        plain=(2, 3, 4),
        far_outs=(1,),
        scratch=(pltpu.SemaphoreType.DMA((3,)),),
        limit=63,
    )
    qkv_weights = from_neighbours(own_weights, "x")
    spread = exchange(message, "z")
    meta, factors = kernel(
        prepare_body,
        (shape(8, block), shape(rows, 128, dtype=F32)),
        tokens,
        attn_gain[None],
        decay_weight.T,
        beta_weight.T,
        decay_rate[None],
        expert_ids.T,
        group_prob[None],
        expert_logit.T,
        far=range(8),
        flops=10**8,
        limit=63,
    )
    (part,) = kernel(
        project_body,
        (shape(NZ, rows, 3 * cols),),
        spread,
        *qkv_weights,
        far=range(5),
        flops=2 * NZ * rows * block * 3 * cols,
        limit=63,
    )
    (packed,) = kernel(
        pack_body,
        (shape(block + dense_gate.shape[1] * 2, half),),
        part,
        dense_gate,
        dense_up,
        dense_down,
        plain=(0, 1, 2, 3),
        far_outs=(0,),
        scratch=(pltpu.SemaphoreType.DMA((4,)),),
        limit=63,
    )
    dense_weights = from_neighbours(packed, "x")
    arrived = exchange(part, "z")
    new_state, attn_part = kernel(
        state_body,
        (shape(*delta_state.shape, dtype=F32), shape(NT, rows, block)),
        arrived,
        factors,
        delta_state,
        head_gain[None],
        output_weight,
        far=range(5),
        far_outs=(0,),
        scratch=(
            pltpu.VMEM((rows, cols), F32),
            pltpu.VMEM(delta_state.shape, F32),
            pltpu.SemaphoreType.DMA((3,)),
        ),
        flops=2 * rows * cols * width,
        limit=63,
    )
    arrived = exchange(attn_part, ("y", "c"))
    middle, message = kernel(
        middle_body,
        (shape(rows, block, dtype=F32), shape(NZ, rows + 8, block)),
        arrived,
        tokens,
        meta,
        far=(1, 2),
        parts={1: ((rows, block), own_block)},
    )

    arrived = exchange(message, "z")
    message, route_rows = kernel(
        dispatch_body,
        (shape(NX, NT, 3 * rows + 8, half), shape(8, NZ * rows, dtype=F32)),
        arrived,
        ffn_gain[None],
        *dense_weights,
        far=(1, 2, 3, 4, 5),
        parts={
            1: ((1, block), own_block),
            **{n: ((block, half), lambda ref, index: ref.at[:block]) for n in range(2, 6)},
        },
        flops=2 * NZ * rows * block * 2 * block,
    )
    sides = ("x", "y", "c")
    arrived = exchange(message.reshape(NX * NT, -1, half), sides).reshape(message.shape)
    (message,) = kernel(
        expert_body,
        (shape(NX, NT, rows, block + 128),),
        arrived,
        ffn_gain[None],
        expert_gate[0],
        expert_up[0],
        expert_down[0],
        far=(1,),
        flops=6 * NX * rows * width * 128,
    )
    arrived = exchange(message.reshape(NX * NT, rows, -1), sides).reshape(message.shape)
    (message,) = kernel(
        combine_body,
        (shape(NZ, rows, block),),
        arrived,
        route_rows,
        *dense_weights,
        dense_mix[None],
        far=(1, 2, 3, 4, 5, 6),
        parts={n: ((half, half), lambda ref, index: ref.at[block:]) for n in range(2, 6)},
        flops=2 * NZ * rows * block * block,
    )
    arrived = exchange(message, "z")
    (mixed_out,) = kernel(
        final_body, (shape(rows, block),), arrived, middle, far=(1,)
    )
    return (mixed_out, new_state)


def solution(mesh):
    fine = Mesh(mesh.devices.reshape(NZ, NX, 4, 2), ("z", "x", "y", "c"))
    ep, tp = ("z", "x"), ("y", "c")

    return jax.shard_map(
        per_device,
        mesh=fine,
        in_specs=(
            P(ep, None),
            P(ep, tp, None, None),
            P(),
            P(ep, tp),
            P(ep, tp),
            P(ep, tp),
            P(),
            P(),
            P(tp),
            P(),
            P(tp, None),
            P(),
            P(ep, None),
            P(ep),
            P(ep, None),
            P(ep, None, tp),
            P(ep, None, tp),
            P(ep, tp, None),
            P(tp, ep),
            P(tp, ep),
            P(ep, tp),
            P(tp),
        ),
        out_specs=(P(ep, tp), P(ep, tp, None, None)),
        check_vma=False,
    )
```

profile of v0, /device:TPU:2, one launch (start us, length us, event | category | flops | bytes accessed | tf_op | source)
XLA Modules:
  0.0 176.5 jit_solution(12166434905632078474)
XLA Ops:
  0.6 7.8 %shard_map.221 = (bf16[8,24,512]{2,1,0:T(8,128)(2,1)}, bf16[128,768]{1,0:T(8,128)(2,1)}) custom-call(bf16[24,4096]{1,0:T(8,128)(2,1)} %refs_1_.2, f32[1,4096]{1,0:T(1,128)} %bitcast.29, bf16[128,256]{1,0:T(8,128)(2,1)} %refs_2_.3, bf16[128,256]{1,0:T(8,128)(2,1)} %refs_3_.2, bf16[128,256]{1,0:T(8,128)(2,1)} %refs_4_.2), custom_call_target="tpu_custom_call" | custom-call | tf_op jit(solution)/shard_map/pallas_call | solution.py:93
  8.4 8.5 %all-to-all-start = ((bf16[8,24,512]{2,1,0:T(8,128)(2,1)}), bf16[8,24,512]{2,1,0:T(8,128)(2,1)S(1)}, u32[]{:S(2)}, u32[]{:S(2)}) async-start(bf16[8,24,512]{2,1,0:T(8,128)(2,1)} %get-tuple-element.12), calls=%async_computation | async-start | bytes 393216 | tf_op jit(solution)/shard_map/all_to_all | solution.py:17
  16.9 1.5 collective-permute-start.2
  18.4 1.1 collective-permute-start.1
  19.5 2.2 %collective-permute-start = (bf16[128,768]{1,0:T(8,128)(2,1)}, bf16[128,768]{1,0:T(8,128)(2,1)S(1)}, u32[]{:S(2)}, u32[]{:S(2)}) collective-permute-start(bf16[128,768]{1,0:T(8,128)(2,1)} %get-tuple-element.13.refs_1_), channel_id=1, source_target_pairs={{0,24},{8,0},{16,8},{24,16},{1,25},{9,1},{17,9},{25,17},{2,26},{10... | collective-permute-start | bytes 589832 | tf_op jit(solution)/shard_map/ppermute | solution.py:25
  21.7 3.2 %collective-permute-done.2.refs_4_ = bf16[128,768]{1,0:T(8,128)(2,1)S(1)} collective-permute-done((bf16[128,768]{1,0:T(8,128)(2,1)}, bf16[128,768]{1,0:T(8,128)(2,1)S(1)}, u32[]{:S(2)}, u32[]{:S(2)}) %collective-permute-start.2) | collective-permute-done | bytes 196640 | tf_op jit(solution)/shard_map/ppermute | solution.py:25
  24.9 0.0 copy-start.11
  24.9 3.0 %collective-permute-done.1.refs_3_ = bf16[128,768]{1,0:T(8,128)(2,1)S(1)} collective-permute-done((bf16[128,768]{1,0:T(8,128)(2,1)}, bf16[128,768]{1,0:T(8,128)(2,1)S(1)}, u32[]{:S(2)}, u32[]{:S(2)}) %collective-permute-start.1) | collective-permute-done | bytes 196640 | tf_op jit(solution)/shard_map/ppermute | solution.py:25
  27.9 0.0 copy-start.12
  27.9 1.8 %collective-permute-done.refs_2_ = bf16[128,768]{1,0:T(8,128)(2,1)S(1)} collective-permute-done((bf16[128,768]{1,0:T(8,128)(2,1)}, bf16[128,768]{1,0:T(8,128)(2,1)S(1)}, u32[]{:S(2)}, u32[]{:S(2)}) %collective-permute-start) | collective-permute-done | bytes 196640 | tf_op jit(solution)/shard_map/ppermute | solution.py:25
  29.7 0.0 copy-start.13
  29.7 0.0 all-to-all-done.refs_0_
  29.7 0.0 copy-done.11
  29.7 0.0 copy-done.12
  29.7 0.7 copy-done.13
  30.4 0.0 copy-start.10
  30.4 0.7 copy-done.10
  31.1 2.5 %shard_map.222.refs_0_ = bf16[8,24,768]{2,1,0:T(8,128)(2,1)} custom-call(bf16[8,24,512]{2,1,0:T(8,128)(2,1)} %copy-done.10, bf16[128,768]{1,0:T(8,128)(2,1)} %get-tuple-element.13.refs_1_, bf16[128,768]{1,0:T(8,128)(2,1)} %copy-done.13, bf16[128,768]{1,0:T(8,128)(2,1)} %copy-done.12, bf16[128,768]{1,0:T(8,128)(2,1)} %copy-done.11), custom_call_target="tpu_custom_call" | custom-call | flops 150994944 | tf_op jit(solution)/shard_map/pallas_call | solution.py:93
  33.6 6.9 %all-to-all-start.1 = ((bf16[8,24,768]{2,1,0:T(8,128)(2,1)}), bf16[8,24,768]{2,1,0:T(8,128)(2,1)S(1)}, u32[]{:S(2)}, u32[]{:S(2)}) async-start(bf16[8,24,768]{2,1,0:T(8,128)(2,1)} %shard_map.222.refs_0_), calls=%async_computation.1 | async-start | bytes 589824 | tf_op jit(solution)/shard_map/all_to_all | solution.py:17
  40.6 2.9 %shard_map.223 = (bf16[8,512]{1,0:T(8,128)(2,1)}, f32[24,128]{1,0:T(8,128)}) custom-call(bf16[24,4096]{1,0:T(8,128)(2,1)} %refs_1_.2, f32[1,4096]{1,0:T(1,128)} %bitcast.30, bf16[16,4096]{1,0:T(8,128)(2,1)} %bitcast.27, bf16[16,4096]{1,0:T(8,128)(2,1)} %bitcast.28, f32[1,2]{1,0:T(1,128)} %bitcast.34, s32[2,24]{1,0:T(2,128)} %bitcast.31, f32[1,24]{1,0:T(1,128)} %bitcast.35, ...), custom_call_target="tpu_custom_call" | custom-call | flops 100000000 | tf_op jit(solution)/shard_map/pallas_call | solution.py:93
  43.4 9.2 %all-to-all-done.1.refs_0_ = bf16[8,24,768]{2,1,0:T(8,128)(2,1)S(1)} async-done(((bf16[8,24,768]{2,1,0:T(8,128)(2,1)}), bf16[8,24,768]{2,1,0:T(8,128)(2,1)S(1)}, u32[]{:S(2)}, u32[]{:S(2)}) %all-to-all-start.1) | async-done | bytes 294944 | tf_op jit(solution)/shard_map/all_to_all | solution.py:17
  52.6 0.0 copy-start.9
  52.6 0.7 copy-done.9
  53.4 0.0 copy-start.2
  53.4 0.0 copy-start.7
  53.4 7.1 %shard_map.224 = (f32[24,2,128,128]{3,2,1,0:T(8,128)}, bf16[8,24,512]{2,1,0:T(8,128)(2,1)}) custom-call(bf16[8,24,768]{2,1,0:T(8,128)(2,1)} %copy-done.9, f32[24,128]{1,0:T(8,128)} %get-tuple-element.14.refs_1_, f32[24,2,128,128]{3,2,1,0:T(8,128)} %refs_2_.4, f32[1,128]{1,0:T(1,128)} %bitcast.33, bf16[256,4096]{1,0:T(8,128)(2,1)} %refs_4_.3), custom_call_target="tpu_custom_call" | custom-call | flops 50331648 | tf_op jit(solution)/shard_map/pallas_call | solution.py:93
  60.5 0.0 copy-start.6
  60.5 11.3 %all_to_all.35.refs_0_ = bf16[8,24,512]{2,1,0:T(8,128)(2,1)S(1)} all-to-all(bf16[8,24,512]{2,1,0:T(8,128)(2,1)} %get-tuple-element.15), channel_id=1, replica_groups=mesh['z'=8,'x'=4,'y'=4,'c'=2] {'y','c'}, dimensions={0} | all-to-all | bytes 393216 | tf_op jit(solution)/shard_map/all_to_all | solution.py:17
  71.8 0.0 copy-done.2
  71.8 0.0 copy-done.7
  71.8 0.8 shard_map.225
  72.6 3.4 %all-to-all-start.3 = ((bf16[8,32,512]{2,1,0:T(8,128)(2,1)}), bf16[8,32,512]{2,1,0:T(8,128)(2,1)S(1)}, u32[]{:S(2)}, u32[]{:S(2)}) async-start(bf16[8,32,512]{2,1,0:T(8,128)(2,1)} %get-tuple-element.17), calls=%async_computation.3 | async-start | bytes 524288 | tf_op jit(solution)/shard_map/all_to_all | solution.py:17
  76.0 13.1 %shard_map.226.refs_2_ = bf16[768,256]{1,0:T(8,128)(2,1)} custom-call(bf16[8,24,768]{2,1,0:T(8,128)(2,1)} %shard_map.222.refs_0_, bf16[512,128]{1,0:T(8,128)(2,1)} %refs_1_.3, bf16[512,128]{1,0:T(8,128)(2,1)} %refs_2_.5, bf16[128,512]{1,0:T(8,128)(2,1)} %refs_3_.3), custom_call_target="tpu_custom_call" | custom-call | tf_op jit(solution)/shard_map/pallas_call | solution.py:93
  89.1 0.2 collective-permute-start.5
  89.3 1.8 %collective-permute-start.4 = (bf16[768,256]{1,0:T(8,128)(2,1)}, bf16[768,256]{1,0:T(8,128)(2,1)S(1)}, u32[]{:S(2)}, u32[]{:S(2)}) collective-permute-start(bf16[768,256]{1,0:T(8,128)(2,1)} %shard_map.226.refs_2_), channel_id=1, source_target_pairs={{0,16},{8,24},{16,0},{24,8},{1,17},{9,25},{17,1},{25,9},{2,18},{10... | collective-permute-start | bytes 1179656 | tf_op jit(solution)/shard_map/ppermute | solution.py:25
  91.0 2.3 %collective-permute-start.3 = (bf16[768,256]{1,0:T(8,128)(2,1)}, bf16[768,256]{1,0:T(8,128)(2,1)S(1)}, u32[]{:S(2)}, u32[]{:S(2)}) collective-permute-start(bf16[768,256]{1,0:T(8,128)(2,1)} %shard_map.226.refs_2_), channel_id=1, source_target_pairs={{0,24},{8,0},{16,8},{24,16},{1,25},{9,1},{17,9},{25,17},{2,26},{10... | collective-permute-start | bytes 1179656 | tf_op jit(solution)/shard_map/ppermute | solution.py:25
  93.4 7.9 %collective-permute-done.5.refs_5_ = bf16[768,256]{1,0:T(8,128)(2,1)S(1)} collective-permute-done((bf16[768,256]{1,0:T(8,128)(2,1)}, bf16[768,256]{1,0:T(8,128)(2,1)S(1)}, u32[]{:S(2)}, u32[]{:S(2)}) %collective-permute-start.5) | collective-permute-done | bytes 393248 | tf_op jit(solution)/shard_map/ppermute | solution.py:25
  101.3 1.6 collective-permute-done.4.refs_4_
  103.0 6.8 %collective-permute-done.3.refs_3_ = bf16[768,256]{1,0:T(8,128)(2,1)S(1)} collective-permute-done((bf16[768,256]{1,0:T(8,128)(2,1)}, bf16[768,256]{1,0:T(8,128)(2,1)S(1)}, u32[]{:S(2)}, u32[]{:S(2)}) %collective-permute-start.3) | collective-permute-done | bytes 393248 | tf_op jit(solution)/shard_map/ppermute | solution.py:25
  109.8 0.0 all-to-all-done.3.refs_0_
  109.8 0.0 copy-done.6
  109.8 0.0 copy-start
  109.8 1.0 copy-done
  110.8 0.0 copy-start.3
  110.8 0.0 copy-start.4
  110.8 0.0 copy-start.5
  110.8 1.9 %shard_map.227 = (bf16[4,8,80,256]{3,2,1,0:T(8,128)(2,1)S(1)}, f32[8,192]{1,0:T(8,128)S(1)}) custom-call(bf16[8,32,512]{2,1,0:T(8,128)(2,1)S(1)} %all-to-all-done.3.refs_0_, f32[1,4096]{1,0:T(1,128)S(1)} %bitcast.24, bf16[768,256]{1,0:T(8,128)(2,1)S(1)} %copy-done, bf16[768,256]{1,0:T(8,128)(2,1)S(1)} %collective-permute-done.3.refs_3_, ...), custom_call_target="tpu_custom_call" | custom-call | flops 201326592 | tf_op jit(solution)/shard_map/pallas_call | solution.py:93
  112.7 23.7 %all_to_all.36 = bf16[32,80,256]{2,1,0:T(8,128)(2,1)S(1)} all-to-all(bf16[32,80,256]{2,1,0:T(8,128)(2,1)S(1)} %bitcast.20), channel_id=1, replica_groups=mesh['z'=8,'x'=4,'y'=4,'c'=2] {'x','y','c'}, dimensions={0} | all-to-all | bytes 2621440 | tf_op jit(solution)/shard_map/all_to_all | solution.py:17
  136.4 0.0 copy-done.3
  136.4 0.0 copy-done.4
  136.4 0.0 copy-done.5
  136.4 0.0 copy-start.8
  136.4 1.0 shard_map.228
  137.4 0.0 copy-start.1
  137.4 18.7 %all_to_all.37 = bf16[32,24,640]{2,1,0:T(8,128)(2,1)S(1)} all-to-all(bf16[32,24,640]{2,1,0:T(8,128)(2,1)S(1)} %bitcast.19), channel_id=1, replica_groups=mesh['z'=8,'x'=4,'y'=4,'c'=2] {'x','y','c'}, dimensions={0} | all-to-all | bytes 1966080 | tf_op jit(solution)/shard_map/all_to_all | solution.py:17
  156.1 0.0 copy-done.8
  156.1 0.0 copy-done.1
  156.1 1.6 shard_map.229
  157.7 18.1 %all_to_all.38.refs_0_ = bf16[8,24,512]{2,1,0:T(8,128)(2,1)S(1)} all-to-all(bf16[8,24,512]{2,1,0:T(8,128)(2,1)S(1)} %shard_map.229), channel_id=1, replica_groups=mesh['z'=8,'x'=4,'y'=4,'c'=2] {'z'}, dimensions={0} | all-to-all | bytes 393216 | tf_op jit(solution)/shard_map/all_to_all | solution.py:17
  175.8 0.7 shard_map.230
Async XLA Ops:
  8.4 21.3 %all-to-all-start = ((bf16[8,24,512]{2,1,0:T(8,128)(2,1)}), bf16[8,24,512]{2,1,0:T(8,128)(2,1)S(1)}, u32[]{:S(2)}, u32[]{:S(2)}) async-start(bf16[8,24,512]{2,1,0:T(8,128)(2,1)} %get-tuple-element.12), calls=%async_computation | async-start | bytes 393216 | tf_op jit(solution)/shard_map/all_to_all | solution.py:17
  16.9 8.0 %collective-permute-start.2 = (bf16[128,768]{1,0:T(8,128)(2,1)}, bf16[128,768]{1,0:T(8,128)(2,1)S(1)}, u32[]{:S(2)}, u32[]{:S(2)}) collective-permute-start(bf16[128,768]{1,0:T(8,128)(2,1)} %get-tuple-element.13.refs_1_), channel_id=1, source_target_pairs={{0,8},{8,16},{16,24},{24,0},{1,9},{9,17},{17,25},{25,1},{2,10},{10... | collective-permute-start | bytes 589832 | tf_op jit(solution)/shard_map/ppermute | solution.py:25
  18.4 9.5 %collective-permute-start.1 = (bf16[128,768]{1,0:T(8,128)(2,1)}, bf16[128,768]{1,0:T(8,128)(2,1)S(1)}, u32[]{:S(2)}, u32[]{:S(2)}) collective-permute-start(bf16[128,768]{1,0:T(8,128)(2,1)} %get-tuple-element.13.refs_1_), channel_id=1, source_target_pairs={{0,16},{8,24},{16,0},{24,8},{1,17},{9,25},{17,1},{25,9},{2,18},{10... | collective-permute-start | bytes 589832 | tf_op jit(solution)/shard_map/ppermute | solution.py:25
  19.5 10.2 %collective-permute-start = (bf16[128,768]{1,0:T(8,128)(2,1)}, bf16[128,768]{1,0:T(8,128)(2,1)S(1)}, u32[]{:S(2)}, u32[]{:S(2)}) collective-permute-start(bf16[128,768]{1,0:T(8,128)(2,1)} %get-tuple-element.13.refs_1_), channel_id=1, source_target_pairs={{0,24},{8,0},{16,8},{24,16},{1,25},{9,1},{17,9},{25,17},{2,26},{10... | collective-permute-start | bytes 589832 | tf_op jit(solution)/shard_map/ppermute | solution.py:25
  24.9 4.9 %copy-start.11 = (bf16[128,768]{1,0:T(8,128)(2,1)}, bf16[128,768]{1,0:T(8,128)(2,1)S(1)}, u32[]{:S(2)}) copy-start(bf16[128,768]{1,0:T(8,128)(2,1)S(1)} %collective-permute-done.2.refs_4_) | copy-start | bytes 589828
  27.9 1.9 %copy-start.12 = (bf16[128,768]{1,0:T(8,128)(2,1)}, bf16[128,768]{1,0:T(8,128)(2,1)S(1)}, u32[]{:S(2)}) copy-start(bf16[128,768]{1,0:T(8,128)(2,1)S(1)} %collective-permute-done.1.refs_3_) | copy-start | bytes 589828
  29.7 0.7 copy-start.13
  30.4 0.7 copy-start.10
  33.6 19.0 %all-to-all-start.1 = ((bf16[8,24,768]{2,1,0:T(8,128)(2,1)}), bf16[8,24,768]{2,1,0:T(8,128)(2,1)S(1)}, u32[]{:S(2)}, u32[]{:S(2)}) async-start(bf16[8,24,768]{2,1,0:T(8,128)(2,1)} %shard_map.222.refs_0_), calls=%async_computation.1 | async-start | bytes 589824 | tf_op jit(solution)/shard_map/all_to_all | solution.py:17
  52.6 0.7 copy-start.9
  53.4 18.4 %copy-start.2 = (bf16[24,4096]{1,0:T(8,128)(2,1)S(1)}, bf16[24,4096]{1,0:T(8,128)(2,1)}, u32[]{:S(2)}) copy-start(bf16[24,4096]{1,0:T(8,128)(2,1)} %refs_1_.2) | copy-start | bytes 589828
  53.4 18.4 %copy-start.7 = (bf16[8,512]{1,0:T(8,128)(2,1)S(1)}, bf16[8,512]{1,0:T(8,128)(2,1)}, u32[]{:S(2)}) copy-start(bf16[8,512]{1,0:T(8,128)(2,1)} %get-tuple-element.16.refs_2_) | copy-start | bytes 24580
  60.5 49.3 %copy-start.6 = (f32[4096]{0:T(1024)S(1)}, f32[4096]{0:T(1024)}, u32[]{:S(2)}) copy-start(f32[4096]{0:T(1024)} %param.33) | copy-start | bytes 49156
  72.6 37.2 %all-to-all-start.3 = ((bf16[8,32,512]{2,1,0:T(8,128)(2,1)}), bf16[8,32,512]{2,1,0:T(8,128)(2,1)S(1)}, u32[]{:S(2)}, u32[]{:S(2)}) async-start(bf16[8,32,512]{2,1,0:T(8,128)(2,1)} %get-tuple-element.17), calls=%async_computation.3 | async-start | bytes 524288 | tf_op jit(solution)/shard_map/all_to_all | solution.py:17
  89.1 12.3 %collective-permute-start.5 = (bf16[768,256]{1,0:T(8,128)(2,1)}, bf16[768,256]{1,0:T(8,128)(2,1)S(1)}, u32[]{:S(2)}, u32[]{:S(2)}) collective-permute-start(bf16[768,256]{1,0:T(8,128)(2,1)} %shard_map.226.refs_2_), channel_id=1, source_target_pairs={{0,8},{8,16},{16,24},{24,0},{1,9},{9,17},{17,25},{25,1},{2,10},{10... | collective-permute-start | bytes 1179656 | tf_op jit(solution)/shard_map/ppermute | solution.py:25
  89.3 13.7 %collective-permute-start.4 = (bf16[768,256]{1,0:T(8,128)(2,1)}, bf16[768,256]{1,0:T(8,128)(2,1)S(1)}, u32[]{:S(2)}, u32[]{:S(2)}) collective-permute-start(bf16[768,256]{1,0:T(8,128)(2,1)} %shard_map.226.refs_2_), channel_id=1, source_target_pairs={{0,16},{8,24},{16,0},{24,8},{1,17},{9,25},{17,1},{25,9},{2,18},{10... | collective-permute-start | bytes 1179656 | tf_op jit(solution)/shard_map/ppermute | solution.py:25
  91.0 18.7 %collective-permute-start.3 = (bf16[768,256]{1,0:T(8,128)(2,1)}, bf16[768,256]{1,0:T(8,128)(2,1)S(1)}, u32[]{:S(2)}, u32[]{:S(2)}) collective-permute-start(bf16[768,256]{1,0:T(8,128)(2,1)} %shard_map.226.refs_2_), channel_id=1, source_target_pairs={{0,24},{8,0},{16,8},{24,16},{1,25},{9,1},{17,9},{25,17},{2,26},{10... | collective-permute-start | bytes 1179656 | tf_op jit(solution)/shard_map/ppermute | solution.py:25
  109.8 1.0 copy-start
  110.8 25.6 %copy-start.3 = (bf16[1,4096,128]{2,1,0:T(8,128)(2,1)S(1)}, bf16[1,4096,128]{2,1,0:T(8,128)(2,1)}, u32[]{:S(2)}) copy-start(bf16[1,4096,128]{2,1,0:T(8,128)(2,1)} %param.37) | copy-start | bytes 3145732
  110.8 25.6 %copy-start.4 = (bf16[1,4096,128]{2,1,0:T(8,128)(2,1)S(1)}, bf16[1,4096,128]{2,1,0:T(8,128)(2,1)}, u32[]{:S(2)}) copy-start(bf16[1,4096,128]{2,1,0:T(8,128)(2,1)} %param.38) | copy-start | bytes 3145732
  110.8 25.6 %copy-start.5 = (bf16[1,128,4096]{2,1,0:T(8,128)(2,1)S(1)}, bf16[1,128,4096]{2,1,0:T(8,128)(2,1)}, u32[]{:S(2)}) copy-start(bf16[1,128,4096]{2,1,0:T(8,128)(2,1)} %param.39) | copy-start | bytes 3145732
  136.4 19.7 %copy-start.8 = (f32[512]{0:T(512)S(1)}, f32[512]{0:T(512)}, u32[]{:S(2)}) copy-start(f32[512]{0:T(512)} %param.43) | copy-start | bytes 6148
  137.4 18.7 %copy-start.1 = (bf16[768,256]{1,0:T(8,128)(2,1)S(1)}, bf16[768,256]{1,0:T(8,128)(2,1)}, u32[]{:S(2)}) copy-start(bf16[768,256]{1,0:T(8,128)(2,1)} %shard_map.226.refs_2_) | copy-start | bytes 1179652
where the time goes:
time: 179 us; the launch traced here: 176 us
  blocking collectives  71.8 us (40%)
  Pallas kernels  39.2 us (22%)
  waiting for transfers between devices  33.7 us (19%)
  starting transfers between devices  27.9 us (16%)
  local copies, waits for them, and re-layouts  3.08 us (2%)
    all_to_all x4, blocking collectives, exchange(): return lax.all_to_all(tiles, axes, split_axis=0, concat_axis=0, tiled=True)  71.8 us
    pallas_call x10, Pallas kernels, kernel(): pl.pallas_call(run, out_shape=outs, in_specs=specs, out_specs=out_specs,...  39.2 us
    ppermute x6, waiting for transfers between devices, from_neighbours(): parts.append(lax.ppermute(shard, axis, pairs))  24.5 us
    all_to_all x3, starting transfers between devices, exchange(): return lax.all_to_all(tiles, axes, split_axis=0, concat_axis=0, tiled=True)  18.8 us
    all_to_all x3, waiting for transfers between devices, exchange(): return lax.all_to_all(tiles, axes, split_axis=0, concat_axis=0, tiled=True)  9.22 us
    ppermute x6, starting transfers between devices, from_neighbours(): parts.append(lax.ppermute(shard, axis, pairs))  9.08 us
  transfers between devices with their start and end apart: 9, of which 7 were waited for; matrix products, arithmetic and copies ran while one was open for 0% of the time, Pallas kernels for 9%

commit v1 on v0

--- a/solution.py
+++ b/solution.py
@@ -8,7 +8,7 @@
 EPS = 1e-06
 BF = jnp.bfloat16
 F32 = jnp.float32
-NZ, NX, NT = 8, 4, 8
+NZ, NX, NY, NT = 8, 4, 4, 8
 CAP = 3
 MIB = 1 << 20
 
@@ -59,12 +59,12 @@
     body, outs, *args, far=(), plain=(), parts=None, far_outs=(), scratch=(), flops=0, limit=16
 ):
     parts = parts or {}
-    far = tuple(far)
+    far, plain = tuple(far), tuple(plain)
     nears = [parts[n][0] if n in parts else args[n].shape for n in far]
 
     def run(*refs):
         sides = [lax.axis_index(name) for name in ("z", "x", "y", "c")]
-        index = (sides[0], sides[1], sides[2] * 2 + sides[3])
+        index = (sides[0], sides[1], sides[2] * 2 + sides[3], sides[3])
         refs = list(refs)
         ins, refs = refs[: len(args)], refs[len(args) :]
         dones = refs.pop() if far else None
@@ -90,6 +90,10 @@
     scratches = list(scratch) + [pltpu.VMEM(near, args[n].dtype) for n, near in zip(far, nears)]
     if far:
         scratches.append(pltpu.SemaphoreType.DMA((len(far),)))
+    args = [
+        pltpu.with_memory_space_constraint(arg, pltpu.HBM) if n in far or n in plain else arg
+        for n, arg in enumerate(args)
+    ]
     return pl.pallas_call(
         run,
         out_shape=outs,
@@ -105,38 +109,26 @@
     return jnp.where(value >= count, value - count, value)
 
 
-def spread_body(index, tokens, gain, query, key, value, out, weights, packed):
+def join_body(index, query, key, value, out):
     cols = query.shape[1]
-    copies = []
     for place, weight in enumerate((query, key, value)):
-        target = weights.at[:, place * cols : (place + 1) * cols]
-        copies.append(pltpu.make_async_copy(weight, target, packed.at[place]))
-        copies[-1].start()
+        out[:, place * cols : (place + 1) * cols] = weight[...]
+
+
+def spread_body(index, tokens, gain, out):
     block = out.shape[2]
     for z in range(NZ):
         cols = slice(z * block, (z + 1) * block)
         out[z] = (tokens[:, cols].astype(F32) * gain[:, cols]).astype(BF)
-    for copy in copies:
-        copy.wait()
-
-
-def pack_body(index, after, gate, up, down, out, packed):
+
+
+def pack_body(index, after, gate, up, down, out):
     block, size = gate.shape
     half = down.shape[1] // 2
-    moves = (
-        (gate, out.at[:block, :size]),
-        (up, out.at[:block, size:]),
-        (down.at[:, :half], out.at[block : block + size, :]),
-        (down.at[:, half:], out.at[block + size :, :]),
-    )
-    copies = [
-        pltpu.make_async_copy(source, target, packed.at[place])
-        for place, (source, target) in enumerate(moves)
-    ]
-    for copy in copies:
-        copy.start()
-    for copy in copies:
-        copy.wait()
+    out[:block, :size] = gate[...]
+    out[:block, size:] = up[...]
+    out[block : block + size, :] = down[:, :half]
+    out[block + size :, :] = down[:, half:]
 
 
 def turned(row, rows):
@@ -201,7 +193,7 @@
     meta[...] = jnp.dot(table.astype(BF), spot, preferred_element_type=F32).astype(BF)
 
 
-def project_body(index, arrived, w0, w1, w2, w3, out):
+def project_body(index, arrived, w0, w1, w2, w3, after, out):
     groups, rows, _ = arrived.shape
     total = None
     for step, weight in enumerate((w0, w1, w2, w3)):
@@ -296,9 +288,21 @@
     return slots
 
 
-def dispatch_body(index, arrived, gain, g0, g1, g2, g3, out, route):
-    rows = out.shape[2] - 8
-    rows = rows // 3
+def half_tokens(arrived, gain, core, rows):
+    blocks = [arrived[2 * y + core, :rows, :].astype(F32) for y in range(NY)]
+    return (jnp.concatenate(blocks, axis=0) * gain[...]).astype(BF)
+
+
+def away_body(index, arrived, gain, g0, g1, g2, g3, out):
+    rows, half = out.shape[2:]
+    scaled = half_tokens(arrived, gain, 1 - index[3], rows)
+    for step, weight in enumerate((g0, g1, g2, g3)):
+        part = jnp.dot(scaled, weight[...], preferred_element_type=F32)
+        out[wrapped(index[1] + step, NX)] = part.reshape(NY, rows, half).astype(BF)
+
+
+def dispatch_body(index, arrived, gain, g0, g1, g2, g3, away, out, route):
+    rows = away.shape[2]
     tokens = NZ * rows
     block = arrived.shape[2]
     half = block // 2
@@ -324,89 +328,106 @@
     square = jnp.where(first, high, square - high).astype(BF)
     for x in range(NX):
         own = chosen[x * rows : (x + 1) * rows]
-        for t in range(NT):
-            out[x, t, :rows, :] = own[:, :half]
-            out[x, t, rows : 2 * rows, :] = own[:, half:]
-            out[x, t, 3 * rows :, :tokens] = square
-            out[x, t, 3 * rows :, tokens:] = jnp.zeros((8, half - tokens), BF)
-    scaled = (wide * gain[...]).astype(BF)
+        for y in range(NY):
+            out[x, y, :rows, :] = own[:, :half]
+            out[x, y, rows : 2 * rows, :] = own[:, half:]
+            out[x, y, 3 * rows :, :tokens] = square
+            out[x, y, 3 * rows :, tokens:] = jnp.zeros((8, half - tokens), BF)
+    scaled = half_tokens(arrived, gain, index[3], rows)
     for step, weight in enumerate((g0, g1, g2, g3)):
-        part = jnp.dot(scaled, weight[...], preferred_element_type=F32)
+        part = jnp.dot(scaled, weight[...], preferred_element_type=F32).reshape(NY, rows, half)
         x = wrapped(index[1] + step, NX)
-        out[x, :, 2 * rows : 3 * rows, :] = part.reshape(NT, rows, half).astype(BF)
-
-
-def expert_body(index, arrived, gain, gate, up, down, out):
-    rows = out.shape[2]
-    block = out.shape[3] - 128
+        out[x, :, 2 * rows : 3 * rows, :] = (part + away[x].astype(F32)).astype(BF)
+
+
+def expert_body(index, arrived, partner, gain, gate, up, down, away, hidden, dense):
+    rows, block = away.shape[2:]
     half = block // 2
     width = gate.shape[0]
     slots = NX * rows
     squares = jnp.zeros((slots, half), F32)
     gate_sum = jnp.zeros((slots, gate.shape[1]), F32)
     up_sum = jnp.zeros((slots, gate.shape[1]), F32)
-    for t in range(NT):
-        for part in range(2):
-            wide = arrived[:, t, part * rows : (part + 1) * rows, :].astype(F32).reshape(slots, half)
-            squares = squares + wide * wide
-            place = t * block + part * half
-            left = (wide * gain[:, place : place + half]).astype(BF)
-            gate_sum += jnp.dot(left, gate[place : place + half, :], preferred_element_type=F32)
-            up_sum += jnp.dot(left, up[place : place + half, :], preferred_element_type=F32)
+    for y in range(NY):
+        for source, core in ((arrived, index[3]), (partner, 1 - index[3])):
+            for part in range(2):
+                wide = source[:, y, part * rows : (part + 1) * rows, :].astype(F32)
+                wide = wide.reshape(slots, half)
+                squares = squares + wide * wide
+                place = pl.multiple_of((2 * y + core) * block + part * half, half)
+                left = (wide * gain[:, pl.ds(place, half)]).astype(BF)
+                own = pl.ds(place, half)
+                gate_sum += jnp.dot(left, gate[own, :], preferred_element_type=F32)
+                up_sum += jnp.dot(left, up[own, :], preferred_element_type=F32)
     scale = lax.rsqrt(jnp.sum(squares, axis=1, keepdims=True) / width + EPS)
-    hidden = (silu(gate_sum * scale) * (up_sum * scale)).astype(BF)
-    for t in range(NT):
-        result = jnp.dot(hidden, down[:, t * block : (t + 1) * block], preferred_element_type=F32)
-        out[:, t, :, :block] = result.reshape(NX, rows, block).astype(BF)
+    result = (silu(gate_sum * scale) * (up_sum * scale)).astype(BF)
+    hidden[...] = result
+    for y in range(NY):
+        place = pl.multiple_of((2 * y + 1 - index[3]) * block, block)
+        part = jnp.dot(result, down[:, pl.ds(place, block)], preferred_element_type=F32)
+        away[:, y] = part.reshape(NX, rows, block).astype(BF)
     tokens = NZ * rows
     lane = lax.broadcasted_iota(jnp.int32, (rows, tokens), 1)
     own = lane == lax.broadcasted_iota(jnp.int32, (rows, tokens), 0) + index[2] * rows
     for x in range(NX):
-        summed = arrived[x, 0, 2 * rows : 3 * rows, :].astype(F32)
-        square = arrived[x, 0, 3 * rows :, :tokens].astype(F32)
-        for t in range(1, NT):
-            summed = summed + arrived[x, t, 2 * rows : 3 * rows, :].astype(F32)
-            square = square + arrived[x, t, 3 * rows :, :tokens].astype(F32)
+        summed = jnp.zeros((rows, half), F32)
+        square = jnp.zeros((8, tokens), F32)
+        for y in range(NY):
+            summed = summed + arrived[x, y, 2 * rows : 3 * rows, :].astype(F32)
+            for source in (arrived, partner):
+                square = square + source[x, y, 3 * rows :, :tokens].astype(F32)
         square = square[0:1, :] + square[1:2, :]
         square = jnp.sum(jnp.where(own, square, 0.0), axis=1, keepdims=True)
         summed = summed * lax.rsqrt(square / width + EPS)
-        result = (silu(summed[:, : half // 2]) * summed[:, half // 2 :]).astype(BF)
-        for t in range(NT):
-            out[x, t, :, block:] = result
-
-
-def combine_body(index, arrived, route, d0, d1, d2, d3, mix, out):
+        dense[x] = (silu(summed[:, : half // 2]) * summed[:, half // 2 :]).astype(BF)
+
+
+def result_body(index, hidden, dense, away, down, out):
+    rows, block = away.shape[2:]
+    for y in range(NY):
+        place = pl.multiple_of((2 * y + index[3]) * block, block)
+        part = jnp.dot(hidden[...], down[:, pl.ds(place, block)], preferred_element_type=F32)
+        part = part.reshape(NX, rows, block) + away[:, y].astype(F32)
+        out[:, y, :, :block] = part.astype(BF)
+        out[:, y, :, block:] = dense[...]
+
+
+def combine_body(index, arrived, partner, route, d0, d1, d2, d3, mix, out, mixed):
     rows = arrived.shape[2]
     block = out.shape[2]
     tokens = NZ * rows
     results = []
     for x in range(NX):
         summed = arrived[x, 0, :, :block].astype(F32)
-        for t in range(1, NT):
-            summed = summed + arrived[x, t, :, :block].astype(F32)
+        for y in range(1, NY):
+            summed = summed + arrived[x, y, :, :block].astype(F32)
         results.append(summed)
     results = jnp.concatenate(results, axis=0).astype(BF)
     routing = route[...]
     slot0, slot1 = slots_of(routing, index[0])
     place = lax.broadcasted_iota(jnp.int32, (NX * rows, tokens), 0)
-    mixed = jnp.zeros((tokens, block), F32)
+    total = jnp.zeros((tokens, block), F32)
     for k in range(2):
         share = jnp.where(place == slot0, routing[2 + k : 3 + k, :], 0.0)
         share = jnp.where(place == slot1, routing[4 + k : 5 + k, :], share).astype(BF)
-        mixed += lax.dot_general(
+        total += lax.dot_general(
             share, results, (((0,), (0,)), ((), ())), preferred_element_type=F32
         )
-    lower = jnp.zeros((tokens, block // 2), F32)
-    upper = jnp.zeros((tokens, block // 2), F32)
-    for step, weight in enumerate((d0, d1, d2, d3)):
-        x = wrapped(index[1] + step, NX)
-        left = arrived[x, :, :, block:].astype(F32).reshape(tokens, -1).astype(BF)
-        size = left.shape[1]
-        lower += jnp.dot(left, weight[:size, :], preferred_element_type=F32)
-        upper += jnp.dot(left, weight[size:, :], preferred_element_type=F32)
+    mixed[...] = total.reshape(NZ, rows, block)
     gate = 1.0 / (1.0 + jnp.exp(-mix[...]))
-    dense = jnp.concatenate((lower, upper), axis=1)
-    out[...] = (gate * dense + mixed).reshape(NZ, rows, block).astype(BF)
+    for source, core in ((arrived, index[3]), (partner, 1 - index[3])):
+        lower = jnp.zeros((NY * rows, block // 2), F32)
+        upper = jnp.zeros((NY * rows, block // 2), F32)
+        for step, weight in enumerate((d0, d1, d2, d3)):
+            x = wrapped(index[1] + step, NX)
+            left = source[x, :, :, block:].astype(F32).reshape(NY * rows, -1).astype(BF)
+            size = left.shape[1]
+            lower += jnp.dot(left, weight[:size, :], preferred_element_type=F32)
+            upper += jnp.dot(left, weight[size:, :], preferred_element_type=F32)
+        dense = gate * jnp.concatenate((lower, upper), axis=1)
+        for y in range(NY):
+            z = 2 * y + core
+            out[z] = (dense[y * rows : (y + 1) * rows] + mixed[z]).astype(BF)
 
 
 def final_body(index, arrived, middle, out):
@@ -453,21 +474,19 @@
         place = pl.multiple_of(index[2] * block, block)
         return ref.at[:, pl.ds(place, block)]
 
-    message, own_weights = kernel(
-        spread_body,
-        (shape(NZ, rows, block), shape(query_weight.shape[0], 3 * cols)),
-        tokens,
-        attn_gain[None],
+    (own_weights,) = kernel(
+        join_body,
+        (shape(query_weight.shape[0], 3 * cols),),
         query_weight,
         key_weight,
         value_weight,
-        far=(0, 1),
-        plain=(2, 3, 4),
-        far_outs=(1,),
-        scratch=(pltpu.SemaphoreType.DMA((3,)),),
-        limit=63,
+        far=range(3),
     )
     qkv_weights = from_neighbours(own_weights, "x")
+
+    (message,) = kernel(
+        spread_body, (pltpu.HBM((NZ, rows, block), BF),), tokens, attn_gain[None], far=range(2)
+    )
     spread = exchange(message, "z")
     meta, factors = kernel(
         prepare_body,
@@ -482,16 +501,16 @@
         expert_logit.T,
         far=range(8),
         flops=10**8,
-        limit=63,
     )
     (part,) = kernel(
         project_body,
         (shape(NZ, rows, 3 * cols),),
         spread,
         *qkv_weights,
-        far=range(5),
+        factors,
+        far=(1, 2, 3, 4),
+        plain=(5,),
         flops=2 * NZ * rows * block * 3 * cols,
-        limit=63,
     )
     (packed,) = kernel(
         pack_body,
@@ -500,10 +519,8 @@
         dense_gate,
         dense_up,
         dense_down,
-        plain=(0, 1, 2, 3),
-        far_outs=(0,),
-        scratch=(pltpu.SemaphoreType.DMA((4,)),),
-        limit=63,
+        plain=(0,),
+        far=(1, 2, 3),
     )
     dense_weights = from_neighbours(packed, "x")
     arrived = exchange(part, "z")
@@ -515,7 +532,7 @@
         delta_state,
         head_gain[None],
         output_weight,
-        far=range(5),
+        far=(1, 3, 4),
         far_outs=(0,),
         scratch=(
             pltpu.VMEM((rows, cols), F32),
@@ -523,7 +540,7 @@
             pltpu.SemaphoreType.DMA((3,)),
         ),
         flops=2 * rows * cols * width,
-        limit=63,
+        limit=24,
     )
     arrived = exchange(attn_part, ("y", "c"))
     middle, message = kernel(
@@ -536,43 +553,70 @@
         parts={1: ((rows, block), own_block)},
     )
 
+    swap = [(0, 1), (1, 0)]
     arrived = exchange(message, "z")
-    message, route_rows = kernel(
-        dispatch_body,
-        (shape(NX, NT, 3 * rows + 8, half), shape(8, NZ * rows, dtype=F32)),
+    gate_up = {
+        1: ((1, block), own_block),
+        **{n: ((block, half), lambda ref, index: ref.at[:block]) for n in range(2, 6)},
+    }
+    (away,) = kernel(
+        away_body,
+        (shape(NX, NY, rows, half),),
         arrived,
         ffn_gain[None],
         *dense_weights,
-        far=(1, 2, 3, 4, 5),
-        parts={
-            1: ((1, block), own_block),
-            **{n: ((block, half), lambda ref, index: ref.at[:block]) for n in range(2, 6)},
-        },
-        flops=2 * NZ * rows * block * 2 * block,
-    )
-    sides = ("x", "y", "c")
-    arrived = exchange(message.reshape(NX * NT, -1, half), sides).reshape(message.shape)
-    (message,) = kernel(
+        far=range(1, 6),
+        parts=gate_up,
+        flops=NZ * rows * block * 2 * block,
+    )
+    message, route_rows = kernel(
+        dispatch_body,
+        (shape(NX, NY, 3 * rows + 8, half), shape(8, NZ * rows, dtype=F32)),
+        arrived,
+        ffn_gain[None],
+        *dense_weights,
+        lax.ppermute(away, "c", swap),
+        far=range(1, 6),
+        parts=gate_up,
+        flops=NZ * rows * block * 2 * block,
+    )
+    sides = ("x", "y")
+    arrived = exchange(message.reshape(NX * NY, -1, half), sides)
+    partner = lax.ppermute(arrived, "c", swap).reshape(message.shape)
+    away, hidden, dense = kernel(
         expert_body,
-        (shape(NX, NT, rows, block + 128),),
-        arrived,
+        (shape(NX, NY, rows, block), shape(NX * rows, 128), shape(NX, rows, 128)),
+        arrived.reshape(message.shape),
+        partner,
         ffn_gain[None],
         expert_gate[0],
         expert_up[0],
         expert_down[0],
-        far=(1,),
-        flops=6 * NX * rows * width * 128,
-    )
-    arrived = exchange(message.reshape(NX * NT, rows, -1), sides).reshape(message.shape)
+        far=(2,),
+        flops=5 * NX * rows * width * 128,
+    )
+    (message,) = kernel(
+        result_body,
+        (shape(NX, NY, rows, block + 128),),
+        hidden,
+        dense,
+        lax.ppermute(away, "c", swap),
+        expert_down[0],
+        flops=NX * rows * width * 128,
+    )
+    arrived = exchange(message.reshape(NX * NY, rows, -1), sides)
+    partner = lax.ppermute(arrived, "c", swap).reshape(message.shape)
     (message,) = kernel(
         combine_body,
         (shape(NZ, rows, block),),
-        arrived,
+        arrived.reshape(message.shape),
+        partner,
         route_rows,
         *dense_weights,
         dense_mix[None],
-        far=(1, 2, 3, 4, 5, 6),
-        parts={n: ((half, half), lambda ref, index: ref.at[block:]) for n in range(2, 6)},
+        far=range(2, 8),
+        parts={n: ((half, half), lambda ref, index: ref.at[block:]) for n in range(3, 7)},
+        scratch=(pltpu.VMEM((NZ, rows, block), F32),),
         flops=2 * NZ * rows * block * block,
     )
     arrived = exchange(message, "z")

time: 179 us -> 157 us (0.88)
  Pallas kernels: 39.2 us -> 23.2 us
  starting transfers between devices: 27.9 us -> 21.4 us
  waiting for transfers between devices: 33.7 us -> 27.3 us
  blocking collectives: 71.8 us -> 77.8 us
    pallas_call x10 -> x13, Pallas kernels: 39.2 us -> 23.2 us  [kernel(): pl.pallas_call(run, out_shape=outs, in_specs=specs, out_specs=out_specs,...]
    all_to_all x3 -> x2, waiting for transfers between devices: 9.22 us -> 0.01 us  [exchange(): return lax.all_to_all(tiles, axes, split_axis=0, concat_axis=0, tiled=True)]
    ppermute x0 -> x4, waiting for transfers between devices: none -> 6.97 us  [the longest x2 3.96 us: per_device(): partner = lax.ppermute(arrived, 'c', swap).reshape(message.shape)]
    all_to_all x3 -> x2, starting transfers between devices: 18.8 us -> 11.9 us  [exchange(): return lax.all_to_all(tiles, axes, split_axis=0, concat_axis=0, tiled=True)]
    all_to_all x4 -> x5, blocking collectives: 71.8 us -> 77.8 us  [exchange(): return lax.all_to_all(tiles, axes, split_axis=0, concat_axis=0, tiled=True)]
    ppermute x6, waiting for transfers between devices: 24.5 us -> 20.3 us  [from_neighbours(): parts.append(lax.ppermute(shard, axis, pairs))]
    unnamed x28 -> x34, local copies, waits for them, and re-layouts: 3.08 us -> 4.12 us
  transfers between devices with their start and end apart: 9 -> 12, of which waited for: 7 -> 9; matrix products, arithmetic and copies ran while one was open for 0% -> 0% of each run, Pallas kernels for 9% -> 3%
where the time goes in v1:
time: 157 us; the launch traced here: 155 us
  blocking collectives  77.8 us (50%)
  waiting for transfers between devices  27.3 us (17%)
  Pallas kernels  23.2 us (15%)
  starting transfers between devices  21.4 us (14%)
  local copies, waits for them, and re-layouts  4.12 us (3%)
    all_to_all x5, blocking collectives, exchange(): return lax.all_to_all(tiles, axes, split_axis=0, concat_axis=0, tiled=True)  77.8 us
    pallas_call x13, Pallas kernels, kernel(): pl.pallas_call(run, out_shape=outs, in_specs=specs, out_specs=out_specs,...  23.2 us
    ppermute x6, waiting for transfers between devices, from_neighbours(): parts.append(lax.ppermute(shard, axis, pairs))  20.3 us
    all_to_all x2, starting transfers between devices, exchange(): return lax.all_to_all(tiles, axes, split_axis=0, concat_axis=0, tiled=True)  11.9 us
    ppermute x6, starting transfers between devices, from_neighbours(): parts.append(lax.ppermute(shard, axis, pairs))  9.16 us
    unnamed x34, local copies, waits for them, and re-layouts  4.12 us
    ppermute x2, waiting for transfers between devices, per_device(): partner = lax.ppermute(arrived, 'c', swap).reshape(message.shape)  3.96 us
  transfers between devices with their start and end apart: 12, of which 9 were waited for; matrix products, arithmetic and copies ran while one was open for 0% of the time, Pallas kernels for 3%

profile of v1, /device:TPU:2, one launch (start us, length us, event | category | flops | bytes accessed | tf_op | source)
XLA Modules:
  0.0 154.8 jit_solution(14302752009296367267)
XLA Ops:
  0.6 0.0 copy-start.2
  0.6 1.8 %shard_map.221 = bf16[8,24,512]{2,1,0:T(8,128)(2,1)} custom-call(bf16[24,4096]{1,0:T(8,128)(2,1)} %refs_1_.4, f32[1,4096]{1,0:T(1,128)} %bitcast.34), custom_call_target="tpu_custom_call" | custom-call | tf_op jit(solution)/shard_map/pallas_call | solution.py:97
  2.5 8.5 %all-to-all-start = ((bf16[8,24,512]{2,1,0:T(8,128)(2,1)}), bf16[8,24,512]{2,1,0:T(8,128)(2,1)S(1)}, u32[]{:S(2)}, u32[]{:S(2)}) async-start(bf16[8,24,512]{2,1,0:T(8,128)(2,1)} %shard_map.221), calls=%async_computation | async-start | bytes 393216 | tf_op jit(solution)/shard_map/all_to_all | solution.py:17
  10.9 0.9 shard_map.222.refs_1_
  11.9 0.0 copy-start.8
  11.9 1.6 %collective-permute-start.2 = (bf16[128,768]{1,0:T(8,128)(2,1)S(1)}, bf16[128,768]{1,0:T(8,128)(2,1)S(1)}, u32[]{:S(2)}, u32[]{:S(2)}) collective-permute-start(bf16[128,768]{1,0:T(8,128)(2,1)S(1)} %shard_map.222.refs_1_), channel_id=1, source_target_pairs={{0,8},{8,16},{16,24},{24,0},{1,9},{9,17},{17,25},{25,1},{2,10},{10... | collective-permute-start | bytes 589832 | tf_op jit(solution)/shard_map/ppermute | solution.py:25
  13.5 1.1 collective-permute-start.1
  14.6 2.2 %collective-permute-start = (bf16[128,768]{1,0:T(8,128)(2,1)S(1)}, bf16[128,768]{1,0:T(8,128)(2,1)}, u32[]{:S(2)}, u32[]{:S(2)}) collective-permute-start(bf16[128,768]{1,0:T(8,128)(2,1)S(1)} %shard_map.222.refs_1_), channel_id=1, source_target_pairs={{0,24},{8,0},{16,8},{24,16},{1,25},{9,1},{17,9},{25,17},{2,26},{10... | collective-permute-start | bytes 589832 | tf_op jit(solution)/shard_map/ppermute | solution.py:25
  16.7 2.3 %shard_map.223 = (bf16[8,512]{1,0:T(8,128)(2,1)S(1)}, f32[24,128]{1,0:T(8,128)S(1)}) custom-call(bf16[24,4096]{1,0:T(8,128)(2,1)} %refs_1_.4, f32[1,4096]{1,0:T(1,128)} %bitcast.35, bf16[16,4096]{1,0:T(8,128)(2,1)} %bitcast.32, bf16[16,4096]{1,0:T(8,128)(2,1)} %bitcast.33, f32[1,2]{1,0:T(1,128)} %bitcast.40, s32[2,24]{1,0:T(2,128)} %bitcast.37, ...), custom_call_target="tpu_custom_call" | custom-call | flops 100000000 | tf_op jit(solution)/shard_map/pallas_call | solution.py:97
  19.0 0.0 copy-start.9
  19.0 0.6 copy-done.9
  19.6 0.6 copy-done.12
  20.2 0.0 collective-permute-done.2.refs_4_
  20.2 2.5 %collective-permute-done.1.refs_3_ = bf16[128,768]{1,0:T(8,128)(2,1)S(1)} collective-permute-done((bf16[128,768]{1,0:T(8,128)(2,1)S(1)}, bf16[128,768]{1,0:T(8,128)(2,1)S(1)}, u32[]{:S(2)}, u32[]{:S(2)}) %collective-permute-start.1) | collective-permute-done | bytes 196640 | tf_op jit(solution)/shard_map/ppermute | solution.py:25
  22.7 0.0 copy-done.8
  22.7 0.7 copy-done.16
  23.4 1.3 collective-permute-done.refs_2_
  24.7 0.0 all-to-all-done.refs_0_
  24.7 0.7 copy-done.6
  25.4 0.0 copy-done.15
  25.4 0.9 copy-done.7
  26.3 1.7 %shard_map.224.refs_0_ = bf16[8,24,768]{2,1,0:T(8,128)(2,1)S(1)} custom-call(bf16[8,24,512]{2,1,0:T(8,128)(2,1)S(1)} %copy-done.7, bf16[128,768]{1,0:T(8,128)(2,1)} %copy-done.8, bf16[128,768]{1,0:T(8,128)(2,1)} %collective-permute-done.refs_2_, bf16[128,768]{1,0:T(8,128)(2,1)} %copy-done.16, bf16[128,768]{1,0:T(8,128)(2,1)} %copy-done.15, f32[24,128]{1,0:T(8,128)} %copy-done.9), custom_call_target="tpu_custom_call" | custom-call | flops 150994944 | tf_op jit(solution)/shard_map/pallas_call | solution.py:97
  28.0 0.0 copy-start.3
  28.0 18.8 %all_to_all.35.refs_0_ = bf16[8,24,768]{2,1,0:T(8,128)(2,1)S(1)} all-to-all(bf16[8,24,768]{2,1,0:T(8,128)(2,1)S(1)} %shard_map.224.refs_0_), channel_id=1, replica_groups=mesh['z'=8,'x'=4,'y'=4,'c'=2] {'z'}, dimensions={0} | all-to-all | bytes 589824 | tf_op jit(solution)/shard_map/all_to_all | solution.py:17
  46.9 0.0 copy-done.2
  46.9 5.2 %shard_map.225 = (f32[24,2,128,128]{3,2,1,0:T(8,128)}, bf16[8,24,512]{2,1,0:T(8,128)(2,1)S(1)}) custom-call(bf16[8,24,768]{2,1,0:T(8,128)(2,1)S(1)} %all_to_all.35.refs_0_, f32[24,128]{1,0:T(8,128)} %copy-done.9, f32[24,2,128,128]{3,2,1,0:T(8,128)S(1)} %copy-done.2, f32[1,128]{1,0:T(1,128)} %bitcast.39, bf16[256,4096]{1,0:T(8,128)(2,1)} %refs_4_.1), custom_call_target="tpu_custom_call" | custom-call | flops 50331648 | tf_op jit(solution)/shard_map/pallas_call | solution.py:97
  52.1 11.1 %all_to_all.36.refs_0_ = bf16[8,24,512]{2,1,0:T(8,128)(2,1)S(1)} all-to-all(bf16[8,24,512]{2,1,0:T(8,128)(2,1)S(1)} %get-tuple-element.14), channel_id=1, replica_groups=mesh['z'=8,'x'=4,'y'=4,'c'=2] {'y','c'}, dimensions={0} | all-to-all | bytes 393216 | tf_op jit(solution)/shard_map/all_to_all | solution.py:17
  63.1 0.0 copy-done.3
  63.1 1.5 shard_map.226
  64.7 0.0 copy-start.10
  64.7 0.6 copy-done.10
  65.3 3.4 %all-to-all-start.3 = ((bf16[8,32,512]{2,1,0:T(8,128)(2,1)}), bf16[8,32,512]{2,1,0:T(8,128)(2,1)S(1)}, u32[]{:S(2)}, u32[]{:S(2)}) async-start(bf16[8,32,512]{2,1,0:T(8,128)(2,1)} %get-tuple-element.16), calls=%async_computation.3 | async-start | bytes 524288 | tf_op jit(solution)/shard_map/all_to_all | solution.py:17
  68.7 0.0 copy-start.1
  68.7 0.0 copy-start.4
  68.7 1.2 shard_map.227.refs_2_.refs_3_
  69.9 0.0 copy-start
  70.0 0.2 collective-permute-start.5
  70.2 2.3 %collective-permute-start.4 = (bf16[768,256]{1,0:T(8,128)(2,1)S(1)}, bf16[768,256]{1,0:T(8,128)(2,1)S(1)}, u32[]{:S(2)}, u32[]{:S(2)}) collective-permute-start(bf16[768,256]{1,0:T(8,128)(2,1)S(1)} %shard_map.227.refs_2_.refs_3_), channel_id=1, source_target_pairs={{0,16},{8,24},{16,0},{24,8},{1,17},{9,25},{17,1},{25,9},{2,18},{10... | collective-permute-start | bytes 1179656 | tf_op jit(solution)/shard_map/ppermute | solution.py:25
  72.4 1.9 %collective-permute-start.3 = (bf16[768,256]{1,0:T(8,128)(2,1)S(1)}, bf16[768,256]{1,0:T(8,128)(2,1)}, u32[]{:S(2)}, u32[]{:S(2)}) collective-permute-start(bf16[768,256]{1,0:T(8,128)(2,1)S(1)} %shard_map.227.refs_2_.refs_3_), channel_id=1, source_target_pairs={{0,24},{8,0},{16,8},{24,16},{1,25},{9,1},{17,9},{25,17},{2,26},{10... | collective-permute-start | bytes 1179656 | tf_op jit(solution)/shard_map/ppermute | solution.py:25
  74.3 7.7 %collective-permute-done.5.refs_5_.refs_6_ = bf16[768,256]{1,0:T(8,128)(2,1)S(1)} collective-permute-done((bf16[768,256]{1,0:T(8,128)(2,1)S(1)}, bf16[768,256]{1,0:T(8,128)(2,1)S(1)}, u32[]{:S(2)}, u32[]{:S(2)}) %collective-permute-start.5) | collective-permute-done | bytes 393248 | tf_op jit(solution)/shard_map/ppermute | solution.py:25
  82.0 1.7 %collective-permute-done.4.refs_4_.refs_5_ = bf16[768,256]{1,0:T(8,128)(2,1)S(1)} collective-permute-done((bf16[768,256]{1,0:T(8,128)(2,1)S(1)}, bf16[768,256]{1,0:T(8,128)(2,1)S(1)}, u32[]{:S(2)}, u32[]{:S(2)}) %collective-permute-start.4) | collective-permute-done | bytes 393248 | tf_op jit(solution)/shard_map/ppermute | solution.py:25
  83.7 7.0 %collective-permute-done.3.refs_3_.refs_4_ = bf16[768,256]{1,0:T(8,128)(2,1)} collective-permute-done((bf16[768,256]{1,0:T(8,128)(2,1)S(1)}, bf16[768,256]{1,0:T(8,128)(2,1)}, u32[]{:S(2)}, u32[]{:S(2)}) %collective-permute-start.3) | collective-permute-done | bytes 393248 | tf_op jit(solution)/shard_map/ppermute | solution.py:25
  90.7 0.0 all-to-all-done.3.refs_0_
  90.7 0.0 copy-done
  90.8 0.0 copy-done.13
  90.8 1.9 %shard_map.228 = bf16[4,4,24,256]{3,2,1,0:T(8,128)(2,1)S(1)} custom-call(bf16[8,32,512]{2,1,0:T(8,128)(2,1)S(1)} %all-to-all-done.3.refs_0_, f32[1,4096]{1,0:T(1,128)} %bitcast.29, bf16[768,256]{1,0:T(8,128)(2,1)} %copy-done, bf16[768,256]{1,0:T(8,128)(2,1)} %collective-permute-done.3.refs_3_.refs_4_, bf16[768,256]{1,0:T(8,128)(2,1)} %copy-done.14, ...), custom_call_target="tpu_custom_call" | custom-call | flops 100663296 | tf_op jit(solution)/shard_map/pallas_call | solution.py:97
  92.7 0.1 collective-permute-start.6
  92.8 1.4 collective-permute-done.6.refs_6_
  94.3 1.9 %shard_map.229 = (bf16[4,4,80,256]{3,2,1,0:T(8,128)(2,1)S(1)}, f32[8,192]{1,0:T(8,128)S(1)}) custom-call(bf16[8,32,512]{2,1,0:T(8,128)(2,1)S(1)} %all-to-all-done.3.refs_0_, f32[1,4096]{1,0:T(1,128)} %bitcast.30, bf16[768,256]{1,0:T(8,128)(2,1)} %copy-done, bf16[768,256]{1,0:T(8,128)(2,1)} %collective-permute-done.3.refs_3_.refs_4_, ...), custom_call_target="tpu_custom_call" | custom-call | flops 100663296 | tf_op jit(solution)/shard_map/pallas_call | solution.py:97
  96.1 0.0 copy-start.11
  96.1 16.5 %all_to_all.37 = bf16[16,80,256]{2,1,0:T(8,128)(2,1)S(1)} all-to-all(bf16[16,80,256]{2,1,0:T(8,128)(2,1)S(1)} %bitcast.27), channel_id=1, replica_groups=mesh['z'=8,'x'=4,'y'=4,'c'=2] {'x','y'}, dimensions={0} | all-to-all | bytes 1310720 | tf_op jit(solution)/shard_map/all_to_all | solution.py:17
  112.6 0.0 collective-permute-start.7
  112.6 2.1 %collective-permute-done.7 = bf16[16,80,256]{2,1,0:T(8,128)(2,1)S(1)} collective-permute-done((bf16[16,80,256]{2,1,0:T(8,128)(2,1)S(1)}, bf16[16,80,256]{2,1,0:T(8,128)(2,1)S(1)}, u32[]{:S(2)}, u32[]{:S(2)}) %collective-permute-start.7) | collective-permute-done | bytes 655392 | tf_op jit(solution)/shard_map/ppermute | solution.py:585
  114.7 0.0 copy-done.1
  114.7 1.6 %shard_map.230 = (bf16[4,4,24,512]{3,2,1,0:T(8,128)(2,1)S(1)}, bf16[96,128]{1,0:T(8,128)(2,1)S(1)}, bf16[4,24,128]{2,1,0:T(8,128)(2,1)S(1)}) custom-call(bf16[4,4,80,256]{3,2,1,0:T(8,128)(2,1)S(1)} %bitcast.21, bf16[4,4,80,256]{3,2,1,0:T(8,128)(2,1)S(1)} %bitcast.26, f32[1,4096]{1,0:T(1,128)} %bitcast.31, bf16[4096,128]{1,0:T(8,128)(2,1)S(1)} %bitcast.24, ...), custom_call_target="tpu_custom_call" | custom-call | flops 251658240 | tf_op jit(solution)/shard_map/pallas_call | solution.py:97
  116.3 0.2 collective-permute-start.8
  116.5 1.6 %collective-permute-done.8.refs_2_ = bf16[4,4,24,512]{3,2,1,0:T(8,128)(2,1)S(1)} collective-permute-done((bf16[4,4,24,512]{3,2,1,0:T(8,128)(2,1)S(1)}, bf16[4,4,24,512]{3,2,1,0:T(8,128)(2,1)S(1)}, u32[]{:S(2)}, u32[]{:S(2)}) %collective-permute-start.8) | collective-permute-done | bytes 393248 | tf_op jit(solution)/shard_map/ppermute | solution.py:603
  118.1 0.3 shard_map.231
  118.4 14.1 %all_to_all.38 = bf16[16,24,640]{2,1,0:T(8,128)(2,1)S(1)} all-to-all(bf16[16,24,640]{2,1,0:T(8,128)(2,1)S(1)} %bitcast.23), channel_id=1, replica_groups=mesh['z'=8,'x'=4,'y'=4,'c'=2] {'x','y'}, dimensions={0} | all-to-all | bytes 983040 | tf_op jit(solution)/shard_map/all_to_all | solution.py:17
  132.5 0.0 collective-permute-start.9
  132.5 1.9 %collective-permute-done.9 = bf16[16,24,640]{2,1,0:T(8,128)(2,1)S(1)} collective-permute-done((bf16[16,24,640]{2,1,0:T(8,128)(2,1)S(1)}, bf16[16,24,640]{2,1,0:T(8,128)(2,1)S(1)}, u32[]{:S(2)}, u32[]{:S(2)}) %collective-permute-start.9) | collective-permute-done | bytes 491552 | tf_op jit(solution)/shard_map/ppermute | solution.py:608
  134.3 1.5 shard_map.232
  135.8 17.4 %all_to_all.39.refs_0_ = bf16[8,24,512]{2,1,0:T(8,128)(2,1)S(1)} all-to-all(bf16[8,24,512]{2,1,0:T(8,128)(2,1)S(1)} %shard_map.232), channel_id=1, replica_groups=mesh['z'=8,'x'=4,'y'=4,'c'=2] {'z'}, dimensions={0} | all-to-all | bytes 393216 | tf_op jit(solution)/shard_map/all_to_all | solution.py:17
  153.2 1.4 shard_map.233
  (12 shorter events, 0.0 us)
Async XLA Ops:
  0.6 46.2 %copy-start.2 = (f32[24,2,128,128]{3,2,1,0:T(8,128)S(1)}, f32[24,2,128,128]{3,2,1,0:T(8,128)}, u32[]{:S(2)}) copy-start(f32[24,2,128,128]{3,2,1,0:T(8,128)} %refs_2_.4) | copy-start | bytes 9437188
  2.5 22.2 %all-to-all-start = ((bf16[8,24,512]{2,1,0:T(8,128)(2,1)}), bf16[8,24,512]{2,1,0:T(8,128)(2,1)S(1)}, u32[]{:S(2)}, u32[]{:S(2)}) async-start(bf16[8,24,512]{2,1,0:T(8,128)(2,1)} %shard_map.221), calls=%async_computation | async-start | bytes 393216 | tf_op jit(solution)/shard_map/all_to_all | solution.py:17
  11.9 10.9 %copy-start.8 = (bf16[128,768]{1,0:T(8,128)(2,1)}, bf16[128,768]{1,0:T(8,128)(2,1)S(1)}, u32[]{:S(2)}) copy-start(bf16[128,768]{1,0:T(8,128)(2,1)S(1)} %shard_map.222.refs_1_) | copy-start | bytes 589828
  11.9 8.3 %collective-permute-start.2 = (bf16[128,768]{1,0:T(8,128)(2,1)S(1)}, bf16[128,768]{1,0:T(8,128)(2,1)S(1)}, u32[]{:S(2)}, u32[]{:S(2)}) collective-permute-start(bf16[128,768]{1,0:T(8,128)(2,1)S(1)} %shard_map.222.refs_1_), channel_id=1, source_target_pairs={{0,8},{8,16},{16,24},{24,0},{1,9},{9,17},{17,25},{25,1},{2,10},{10... | collective-permute-start | bytes 589832 | tf_op jit(solution)/shard_map/ppermute | solution.py:25
  13.5 9.3 %collective-permute-start.1 = (bf16[128,768]{1,0:T(8,128)(2,1)S(1)}, bf16[128,768]{1,0:T(8,128)(2,1)S(1)}, u32[]{:S(2)}, u32[]{:S(2)}) collective-permute-start(bf16[128,768]{1,0:T(8,128)(2,1)S(1)} %shard_map.222.refs_1_), channel_id=1, source_target_pairs={{0,16},{8,24},{16,0},{24,8},{1,17},{9,25},{17,1},{25,9},{2,18},{10... | collective-permute-start | bytes 589832 | tf_op jit(solution)/shard_map/ppermute | solution.py:25
  14.6 10.1 %collective-permute-start = (bf16[128,768]{1,0:T(8,128)(2,1)S(1)}, bf16[128,768]{1,0:T(8,128)(2,1)}, u32[]{:S(2)}, u32[]{:S(2)}) collective-permute-start(bf16[128,768]{1,0:T(8,128)(2,1)S(1)} %shard_map.222.refs_1_), channel_id=1, source_target_pairs={{0,24},{8,0},{16,8},{24,16},{1,25},{9,1},{17,9},{25,17},{2,26},{10... | collective-permute-start | bytes 589832 | tf_op jit(solution)/shard_map/ppermute | solution.py:25
  19.0 0.6 copy-start.9
  19.6 0.6 copy-start.12
  20.2 5.2 %copy-start.15 = (bf16[128,768]{1,0:T(8,128)(2,1)}, bf16[128,768]{1,0:T(8,128)(2,1)S(1)}, u32[]{:S(2)}) copy-start(bf16[128,768]{1,0:T(8,128)(2,1)S(1)} %collective-permute-done.2.refs_4_) | copy-start | bytes 589828
  22.7 0.7 copy-start.16
  24.7 0.7 copy-start.6
  25.4 0.9 copy-start.7
  28.0 35.1 %copy-start.3 = (bf16[8,24,768]{2,1,0:T(8,128)(2,1)}, bf16[8,24,768]{2,1,0:T(8,128)(2,1)S(1)}, u32[]{:S(2)}) copy-start(bf16[8,24,768]{2,1,0:T(8,128)(2,1)S(1)} %shard_map.224.refs_0_) | copy-start | bytes 884740
  64.7 0.6 copy-start.10
  65.3 25.5 %all-to-all-start.3 = ((bf16[8,32,512]{2,1,0:T(8,128)(2,1)}), bf16[8,32,512]{2,1,0:T(8,128)(2,1)S(1)}, u32[]{:S(2)}, u32[]{:S(2)}) async-start(bf16[8,32,512]{2,1,0:T(8,128)(2,1)} %get-tuple-element.16), calls=%async_computation.3 | async-start | bytes 524288 | tf_op jit(solution)/shard_map/all_to_all | solution.py:17
  68.7 46.0 %copy-start.1 = (bf16[1,128,4096]{2,1,0:T(8,128)(2,1)S(1)}, bf16[1,128,4096]{2,1,0:T(8,128)(2,1)}, u32[]{:S(2)}) copy-start(bf16[1,128,4096]{2,1,0:T(8,128)(2,1)} %param.39) | copy-start | bytes 3145732
  68.7 46.0 %copy-start.4 = (bf16[1,4096,128]{2,1,0:T(8,128)(2,1)S(1)}, bf16[1,4096,128]{2,1,0:T(8,128)(2,1)}, u32[]{:S(2)}) copy-start(bf16[1,4096,128]{2,1,0:T(8,128)(2,1)} %param.37) | copy-start | bytes 3145732
  69.9 20.8 %copy-start = (bf16[768,256]{1,0:T(8,128)(2,1)}, bf16[768,256]{1,0:T(8,128)(2,1)S(1)}, u32[]{:S(2)}) copy-start(bf16[768,256]{1,0:T(8,128)(2,1)S(1)} %shard_map.227.refs_2_.refs_3_) | copy-start | bytes 1179652
  70.0 12.1 %collective-permute-start.5 = (bf16[768,256]{1,0:T(8,128)(2,1)S(1)}, bf16[768,256]{1,0:T(8,128)(2,1)S(1)}, u32[]{:S(2)}, u32[]{:S(2)}) collective-permute-start(bf16[768,256]{1,0:T(8,128)(2,1)S(1)} %shard_map.227.refs_2_.refs_3_), channel_id=1, source_target_pairs={{0,8},{8,16},{16,24},{24,0},{1,9},{9,17},{17,25},{25,1},{2,10},{10... | collective-permute-start | bytes 1179656 | tf_op jit(solution)/shard_map/ppermute | solution.py:25
  70.2 13.5 %collective-permute-start.4 = (bf16[768,256]{1,0:T(8,128)(2,1)S(1)}, bf16[768,256]{1,0:T(8,128)(2,1)S(1)}, u32[]{:S(2)}, u32[]{:S(2)}) collective-permute-start(bf16[768,256]{1,0:T(8,128)(2,1)S(1)} %shard_map.227.refs_2_.refs_3_), channel_id=1, source_target_pairs={{0,16},{8,24},{16,0},{24,8},{1,17},{9,25},{17,1},{25,9},{2,18},{10... | collective-permute-start | bytes 1179656 | tf_op jit(solution)/shard_map/ppermute | solution.py:25
  72.4 18.3 %collective-permute-start.3 = (bf16[768,256]{1,0:T(8,128)(2,1)S(1)}, bf16[768,256]{1,0:T(8,128)(2,1)}, u32[]{:S(2)}, u32[]{:S(2)}) collective-permute-start(bf16[768,256]{1,0:T(8,128)(2,1)S(1)} %shard_map.227.refs_2_.refs_3_), channel_id=1, source_target_pairs={{0,24},{8,0},{16,8},{24,16},{1,25},{9,1},{17,9},{25,17},{2,26},{10... | collective-permute-start | bytes 1179656 | tf_op jit(solution)/shard_map/ppermute | solution.py:25
  82.0 8.7 %copy-start.13 = (bf16[768,256]{1,0:T(8,128)(2,1)}, bf16[768,256]{1,0:T(8,128)(2,1)S(1)}, u32[]{:S(2)}) copy-start(bf16[768,256]{1,0:T(8,128)(2,1)S(1)} %collective-permute-done.5.refs_5_.refs_6_) | copy-start | bytes 1179652
  83.7 7.1 %copy-start.14 = (bf16[768,256]{1,0:T(8,128)(2,1)}, bf16[768,256]{1,0:T(8,128)(2,1)S(1)}, u32[]{:S(2)}) copy-start(bf16[768,256]{1,0:T(8,128)(2,1)S(1)} %collective-permute-done.4.refs_4_.refs_5_) | copy-start | bytes 1179652
  90.7 24.0 %copy-start.5 = (bf16[1,4096,128]{2,1,0:T(8,128)(2,1)S(1)}, bf16[1,4096,128]{2,1,0:T(8,128)(2,1)}, u32[]{:S(2)}) copy-start(bf16[1,4096,128]{2,1,0:T(8,128)(2,1)} %param.38) | copy-start | bytes 3145732
  92.7 1.5 collective-permute-start.6
  96.1 22.3 %copy-start.11 = (f32[8,192]{1,0:T(8,128)}, f32[8,192]{1,0:T(8,128)S(1)}, u32[]{:S(2)}) copy-start(f32[8,192]{1,0:T(8,128)S(1)} %get-tuple-element.21.refs_2_) | copy-start | bytes 18436
  112.6 2.1 %collective-permute-start.7 = (bf16[16,80,256]{2,1,0:T(8,128)(2,1)S(1)}, bf16[16,80,256]{2,1,0:T(8,128)(2,1)S(1)}, u32[]{:S(2)}, u32[]{:S(2)}) collective-permute-start(bf16[16,80,256]{2,1,0:T(8,128)(2,1)S(1)} %all_to_all.37), channel_id=1, source_target_pairs={{0,1},{1,0},{2,3},{3,2},{4,5},{5,4},{6,7},{7,6},{8,9},{9,8},{10,11... | collective-permute-start | bytes 1966088 | tf_op jit(solution)/shard_map/ppermute | solution.py:585
  116.3 1.8 %collective-permute-start.8 = (bf16[4,4,24,512]{3,2,1,0:T(8,128)(2,1)S(1)}, bf16[4,4,24,512]{3,2,1,0:T(8,128)(2,1)S(1)}, u32[]{:S(2)}, u32[]{:S(2)}) collective-permute-start(bf16[4,4,24,512]{3,2,1,0:T(8,128)(2,1)S(1)} %get-tuple-element.20), channel_id=1, source_target_pairs={{0,1},{1,0},{2,3},{3,2},{4,5},{5,4},{6,7},{7,6},{8,9},{9,8},{10,11... | collective-permute-start | bytes 1179656 | tf_op jit(solution)/shard_map/ppermute | solution.py:603
  132.5 1.9 %collective-permute-start.9 = (bf16[16,24,640]{2,1,0:T(8,128)(2,1)S(1)}, bf16[16,24,640]{2,1,0:T(8,128)(2,1)S(1)}, u32[]{:S(2)}, u32[]{:S(2)}) collective-permute-start(bf16[16,24,640]{2,1,0:T(8,128)(2,1)S(1)} %all_to_all.38), channel_id=1, source_target_pairs={{0,1},{1,0},{2,3},{3,2},{4,5},{5,4},{6,7},{7,6},{8,9},{9,8},{10,11... | collective-permute-start | bytes 1474568 | tf_op jit(solution)/shard_map/ppermute | solution.py:608

commit v2 on v1

--- a/solution.py
+++ b/solution.py
@@ -56,10 +56,10 @@
 
 
 def kernel(
-    body, outs, *args, far=(), plain=(), parts=None, far_outs=(), scratch=(), flops=0, limit=16
+    body, outs, *args, far=(), plain=(), held=(), parts=None, far_outs=(), scratch=(), flops=0, limit=16
 ):
     parts = parts or {}
-    far, plain = tuple(far), tuple(plain)
+    far, plain, held = tuple(far), tuple(plain), tuple(held)
     nears = [parts[n][0] if n in parts else args[n].shape for n in far]
 
     def run(*refs):
@@ -91,7 +91,7 @@
     if far:
         scratches.append(pltpu.SemaphoreType.DMA((len(far),)))
     args = [
-        pltpu.with_memory_space_constraint(arg, pltpu.HBM) if n in far or n in plain else arg
+        pltpu.with_memory_space_constraint(arg, pltpu.HBM) if n in far + plain + held else arg
         for n, arg in enumerate(args)
     ]
     return pl.pallas_call(
@@ -109,13 +109,10 @@
     return jnp.where(value >= count, value - count, value)
 
 
-def join_body(index, query, key, value, out):
+def spread_body(index, tokens, gain, query, key, value, out, weights):
     cols = query.shape[1]
     for place, weight in enumerate((query, key, value)):
-        out[:, place * cols : (place + 1) * cols] = weight[...]
-
-
-def spread_body(index, tokens, gain, out):
+        weights[:, place * cols : (place + 1) * cols] = weight[...]
     block = out.shape[2]
     for z in range(NZ):
         cols = slice(z * block, (z + 1) * block)
@@ -205,47 +202,36 @@
     out[...] = total.reshape(groups, rows, -1).astype(BF)
 
 
-def state_body(
-    index, arrived, factors, state, head_gain, weight, new_state, out, read, fresh, stored
-):
+def recall_body(index, arrived, factors, state, head_gain, weight, out, keys, changes):
     rows, heads, size = state.shape[:3]
     cols = heads * size
     summed = arrived[0].astype(F32)
     for z in range(1, NZ):
         summed = summed + arrived[z].astype(F32)
     summed = summed * factors[:, 0:1]
-    parts = []
+    line = lax.broadcasted_iota(jnp.int32, (rows, size), 0)
+    head_rows = []
     for h in range(heads):
-        query = unit_rows(summed[:, h * size : (h + 1) * size]) * size ** (-0.5)
+        own = slice(h * size, (h + 1) * size)
+        query = unit_rows(summed[:, own]) * size ** (-0.5)
         key = unit_rows(summed[:, cols + h * size : cols + (h + 1) * size])
         value = summed[:, 2 * cols + h * size : 2 * cols + (h + 1) * size]
-        both = jnp.sum(query * key, axis=1, keepdims=True)
-        parts.append((query.T, key.T, value, both))
-    batch = rows // stored.shape[0]
-    stores = []
-    for b in range(rows):
-        for h, (query_cols, key_cols, value, both) in enumerate(parts):
-            old = state[b, h]
-            key_col = key_cols[:, b : b + 1]
-            query_col = query_cols[:, b : b + 1]
-            fade = factors[b : b + 1, 1 + h : 2 + h]
-            recalled = jnp.sum(key_col * old, axis=0, keepdims=True)
-            asked = jnp.sum(query_col * old, axis=0, keepdims=True)
-            gate = factors[b : b + 1, 1 + heads + h : 2 + heads + h]
-            correction = gate * (value[b : b + 1] - fade * recalled)
-            fresh[b, h] = fade * old + key_col * correction
-            read[b : b + 1, h * size : (h + 1) * size] = (
-                fade * asked + both[b : b + 1] * correction
-            )
-        if (b + 1) % batch == 0:
-            group = pl.ds(b + 1 - batch, batch)
-            stores.append(
-                pltpu.make_async_copy(fresh.at[group], new_state.at[group], stored.at[b // batch])
-            )
-            stores[-1].start()
-    head_rows = []
-    for h in range(heads):
-        result = read[:, h * size : (h + 1) * size]
+        both = jnp.concatenate((key, query), axis=0).astype(BF)
+        recalled = jnp.zeros((rows, size), F32)
+        asked = jnp.zeros((rows, size), F32)
+        for b in range(0, rows, 2):
+            pair = jnp.concatenate((state[b, h], state[b + 1, h]), axis=1).astype(BF)
+            product = jnp.dot(both, pair, preferred_element_type=F32)
+            for side in range(2):
+                lanes = slice(side * size, (side + 1) * size)
+                recalled = jnp.where(line == b + side, product[:rows, lanes], recalled)
+                asked = jnp.where(line == b + side, product[rows:, lanes], asked)
+        fade = factors[:, 1 + h : 2 + h]
+        gate = factors[:, 1 + heads + h : 2 + heads + h]
+        change = gate * (value - fade * recalled)
+        keys[:, own] = key
+        changes[:, own] = change
+        result = fade * asked + jnp.sum(query * key, axis=1, keepdims=True) * change
         mean_sq = jnp.mean(result * result, axis=1, keepdims=True)
         head_rows.append(result * lax.rsqrt(mean_sq + EPS) * head_gain[...])
     left = jnp.concatenate(head_rows, axis=1).astype(BF)
@@ -253,8 +239,27 @@
     for t in range(NT):
         right = weight[:, t * block : (t + 1) * block]
         out[t] = jnp.dot(left, right, preferred_element_type=F32).astype(BF)
-    for store in stores:
-        store.wait()
+
+
+def update_body(index, keys, changes, factors, state, new_state):
+    rows, heads, size = state.shape[:3]
+    line = lax.broadcasted_iota(jnp.int32, (rows, size), 0)
+    line = jnp.concatenate((line, line, line), axis=0)
+    for h in range(heads):
+        own = slice(h * size, (h + 1) * size)
+        key, change = keys[:, own], changes[:, own]
+        key_high = key.astype(BF).astype(F32)
+        high = change.astype(BF).astype(F32)
+        left = jnp.concatenate((key_high, key - key_high, key_high), axis=0).T.astype(BF)
+        right = jnp.concatenate((high, high, change - high), axis=0)
+        for b in range(0, rows, 2):
+            pair = [jnp.where(line == b + side, right, 0.0) for side in range(2)]
+            pair = jnp.concatenate(pair, axis=1).astype(BF)
+            product = jnp.dot(left, pair, preferred_element_type=F32)
+            for side in range(2):
+                fade = factors[b + side : b + side + 1, 1 + h : 2 + h]
+                grown = product[:, side * size : (side + 1) * size]
+                new_state[b + side, h] = fade * state[b + side, h] + grown
 
 
 def middle_body(index, arrived, tokens, meta, middle, out):
@@ -263,7 +268,8 @@
     summed = arrived[0].astype(F32)
     for t in range(1, NT):
         summed = summed + arrived[t].astype(F32)
-    total = tokens[...].astype(F32) + summed
+    place = pl.multiple_of(index[2] * block, block)
+    total = tokens[:, pl.ds(place, block)].astype(F32) + summed
     middle[...] = total
     narrow = total.astype(BF)
     for z in range(NZ):
@@ -297,7 +303,7 @@
     rows, half = out.shape[2:]
     scaled = half_tokens(arrived, gain, 1 - index[3], rows)
     for step, weight in enumerate((g0, g1, g2, g3)):
-        part = jnp.dot(scaled, weight[...], preferred_element_type=F32)
+        part = jnp.dot(scaled, weight[: arrived.shape[2], :], preferred_element_type=F32)
         out[wrapped(index[1] + step, NX)] = part.reshape(NY, rows, half).astype(BF)
 
 
@@ -335,7 +341,7 @@
             out[x, y, 3 * rows :, tokens:] = jnp.zeros((8, half - tokens), BF)
     scaled = half_tokens(arrived, gain, index[3], rows)
     for step, weight in enumerate((g0, g1, g2, g3)):
-        part = jnp.dot(scaled, weight[...], preferred_element_type=F32).reshape(NY, rows, half)
+        part = jnp.dot(scaled, weight[: arrived.shape[2], :], preferred_element_type=F32).reshape(NY, rows, half)
         x = wrapped(index[1] + step, NX)
         out[x, :, 2 * rows : 3 * rows, :] = (part + away[x].astype(F32)).astype(BF)
 
@@ -422,8 +428,8 @@
             x = wrapped(index[1] + step, NX)
             left = source[x, :, :, block:].astype(F32).reshape(NY * rows, -1).astype(BF)
             size = left.shape[1]
-            lower += jnp.dot(left, weight[:size, :], preferred_element_type=F32)
-            upper += jnp.dot(left, weight[size:, :], preferred_element_type=F32)
+            lower += jnp.dot(left, weight[block : block + size, :], preferred_element_type=F32)
+            upper += jnp.dot(left, weight[block + size :, :], preferred_element_type=F32)
         dense = gate * jnp.concatenate((lower, upper), axis=1)
         for y in range(NY):
             z = 2 * y + core
@@ -474,19 +480,17 @@
         place = pl.multiple_of(index[2] * block, block)
         return ref.at[:, pl.ds(place, block)]
 
-    (own_weights,) = kernel(
-        join_body,
-        (shape(query_weight.shape[0], 3 * cols),),
+    message, own_weights = kernel(
+        spread_body,
+        (pltpu.HBM((NZ, rows, block), BF), shape(query_weight.shape[0], 3 * cols)),
+        tokens,
+        attn_gain[None],
         query_weight,
         key_weight,
         value_weight,
-        far=range(3),
+        far=range(5),
     )
     qkv_weights = from_neighbours(own_weights, "x")
-
-    (message,) = kernel(
-        spread_body, (pltpu.HBM((NZ, rows, block), BF),), tokens, attn_gain[None], far=range(2)
-    )
     spread = exchange(message, "z")
     meta, factors = kernel(
         prepare_body,
@@ -508,7 +512,7 @@
         spread,
         *qkv_weights,
         factors,
-        far=(1, 2, 3, 4),
+        held=(1, 2, 3, 4),
         plain=(5,),
         flops=2 * NZ * rows * block * 3 * cols,
     )
@@ -524,22 +528,30 @@
     )
     dense_weights = from_neighbours(packed, "x")
     arrived = exchange(part, "z")
-    new_state, attn_part = kernel(
-        state_body,
-        (shape(*delta_state.shape, dtype=F32), shape(NT, rows, block)),
+    attn_part, keys, changes = kernel(
+        recall_body,
+        (
+            shape(NT, rows, block),
+            shape(rows, cols, dtype=F32),
+            shape(rows, cols, dtype=F32),
+        ),
         arrived,
         factors,
         delta_state,
         head_gain[None],
         output_weight,
         far=(1, 3, 4),
-        far_outs=(0,),
-        scratch=(
-            pltpu.VMEM((rows, cols), F32),
-            pltpu.VMEM(delta_state.shape, F32),
-            pltpu.SemaphoreType.DMA((3,)),
-        ),
         flops=2 * rows * cols * width,
+    )
+    (new_state,) = kernel(
+        update_body,
+        (shape(*delta_state.shape, dtype=F32),),
+        keys,
+        changes,
+        factors,
+        delta_state,
+        far=range(4),
+        flops=10**8,
         limit=24,
     )
     arrived = exchange(attn_part, ("y", "c"))
@@ -549,24 +561,19 @@
         arrived,
         tokens,
         meta,
-        far=(1, 2),
-        parts={1: ((rows, block), own_block)},
     )
 
     swap = [(0, 1), (1, 0)]
     arrived = exchange(message, "z")
-    gate_up = {
-        1: ((1, block), own_block),
-        **{n: ((block, half), lambda ref, index: ref.at[:block]) for n in range(2, 6)},
-    }
+    gain_part = {1: ((1, block), own_block)}
     (away,) = kernel(
         away_body,
         (shape(NX, NY, rows, half),),
         arrived,
         ffn_gain[None],
         *dense_weights,
-        far=range(1, 6),
-        parts=gate_up,
+        far=(1,),
+        parts=gain_part,
         flops=NZ * rows * block * 2 * block,
     )
     message, route_rows = kernel(
@@ -576,8 +583,8 @@
         ffn_gain[None],
         *dense_weights,
         lax.ppermute(away, "c", swap),
-        far=range(1, 6),
-        parts=gate_up,
+        far=(1,),
+        parts=gain_part,
         flops=NZ * rows * block * 2 * block,
     )
     sides = ("x", "y")
@@ -614,15 +621,11 @@
         route_rows,
         *dense_weights,
         dense_mix[None],
-        far=range(2, 8),
-        parts={n: ((half, half), lambda ref, index: ref.at[block:]) for n in range(3, 7)},
         scratch=(pltpu.VMEM((NZ, rows, block), F32),),
         flops=2 * NZ * rows * block * block,
     )
     arrived = exchange(message, "z")
-    (mixed_out,) = kernel(
-        final_body, (shape(rows, block),), arrived, middle, far=(1,)
-    )
+    (mixed_out,) = kernel(final_body, (shape(rows, block),), arrived, middle)
     return (mixed_out, new_state)
 
 

time: 157 us -> 149 us (0.949)
  blocking collectives: 77.8 us -> 60.6 us
  waiting for transfers between devices: 27.3 us -> 34.2 us
  starting transfers between devices: 21.4 us -> 28.1 us
  Pallas kernels: 23.2 us -> 20.1 us
    all_to_all x5 -> x4, blocking collectives: 77.8 us -> 60.6 us  [exchange(): return lax.all_to_all(tiles, axes, split_axis=0, concat_axis=0, tiled=True)]
    all_to_all x2 -> x3, starting transfers between devices: 11.9 us -> 18.7 us  [exchange(): return lax.all_to_all(tiles, axes, split_axis=0, concat_axis=0, tiled=True)]
    all_to_all x2 -> x3, waiting for transfers between devices: 0.01 us -> 6.52 us  [exchange(): return lax.all_to_all(tiles, axes, split_axis=0, concat_axis=0, tiled=True)]
    pallas_call x13, Pallas kernels: 23.2 us -> 20.1 us  [kernel(): pl.pallas_call(run, out_shape=outs, in_specs=specs, out_specs=out_specs,...]
    unnamed x34 -> x30, local copies, waits for them, and re-layouts: 4.12 us -> 2.92 us
  transfers between devices with their start and end apart: 12 -> 13, of which waited for: 9 -> 11; matrix products, arithmetic and copies ran while one was open for 0% -> 0% of each run, Pallas kernels for 3% -> 5%
where the time goes in v2:
time: 149 us; the launch traced here: 147 us
  blocking collectives  60.6 us (41%)
  waiting for transfers between devices  34.2 us (23%)
  starting transfers between devices  28.1 us (19%)
  Pallas kernels  20.1 us (13%)
  local copies, waits for them, and re-layouts  2.92 us (2%)
    all_to_all x4, blocking collectives, exchange(): return lax.all_to_all(tiles, axes, split_axis=0, concat_axis=0, tiled=True)  60.6 us
    ppermute x6, waiting for transfers between devices, from_neighbours(): parts.append(lax.ppermute(shard, axis, pairs))  20.8 us
    pallas_call x13, Pallas kernels, kernel(): pl.pallas_call(run, out_shape=outs, in_specs=specs, out_specs=out_specs,...  20.1 us
    all_to_all x3, starting transfers between devices, exchange(): return lax.all_to_all(tiles, axes, split_axis=0, concat_axis=0, tiled=True)  18.7 us
    ppermute x6, starting transfers between devices, from_neighbours(): parts.append(lax.ppermute(shard, axis, pairs))  9.09 us
    all_to_all x3, waiting for transfers between devices, exchange(): return lax.all_to_all(tiles, axes, split_axis=0, concat_axis=0, tiled=True)  6.52 us
    ppermute x2, waiting for transfers between devices, per_device(): partner = lax.ppermute(arrived, 'c', swap).reshape(message.shape)  3.96 us
    ppermute x2, waiting for transfers between devices, per_device(): lax.ppermute(away, 'c', swap)  3.01 us
  transfers between devices with their start and end apart: 13, of which 11 were waited for; matrix products, arithmetic and copies ran while one was open for 0% of the time, Pallas kernels for 5%

profile of v2, /device:TPU:2, one launch (start us, length us, event | category | flops | bytes accessed | tf_op | source)
XLA Modules:
  0.0 146.8 jit_solution(16514782115299771519)
XLA Ops:
  0.6 0.0 copy-start
  0.6 1.9 %shard_map.221 = (bf16[8,24,512]{2,1,0:T(8,128)(2,1)}, bf16[128,768]{1,0:T(8,128)(2,1)S(1)}) custom-call(bf16[24,4096]{1,0:T(8,128)(2,1)} %refs_1_.2, f32[1,4096]{1,0:T(1,128)} %bitcast.35, bf16[128,256]{1,0:T(8,128)(2,1)} %refs_2_.3, bf16[128,256]{1,0:T(8,128)(2,1)} %refs_3_.3, bf16[128,256]{1,0:T(8,128)(2,1)} %refs_4_.2), custom_call_target="tpu_custom_call" | custom-call | tf_op jit(solution)/shard_map/pallas_call | solution.py:97
  2.6 0.0 copy-start.8
  2.6 8.5 %all-to-all-start = ((bf16[8,24,512]{2,1,0:T(8,128)(2,1)}), bf16[8,24,512]{2,1,0:T(8,128)(2,1)S(1)}, u32[]{:S(2)}, u32[]{:S(2)}) async-start(bf16[8,24,512]{2,1,0:T(8,128)(2,1)} %get-tuple-element.16), calls=%async_computation | async-start | bytes 393216 | tf_op jit(solution)/shard_map/all_to_all | solution.py:17
  11.1 1.5 %collective-permute-start.2 = (bf16[128,768]{1,0:T(8,128)(2,1)S(1)}, bf16[128,768]{1,0:T(8,128)(2,1)S(1)}, u32[]{:S(2)}, u32[]{:S(2)}) collective-permute-start(bf16[128,768]{1,0:T(8,128)(2,1)S(1)} %get-tuple-element.17.refs_1_), channel_id=1, source_target_pairs={{0,8},{8,16},{16,24},{24,0},{1,9},{9,17},{17,25},{25,1},{2,10},{10... | collective-permute-start | bytes 589832 | tf_op jit(solution)/shard_map/ppermute | solution.py:25
  12.6 1.1 collective-permute-start.1
  13.7 2.2 %collective-permute-start = (bf16[128,768]{1,0:T(8,128)(2,1)S(1)}, bf16[128,768]{1,0:T(8,128)(2,1)}, u32[]{:S(2)}, u32[]{:S(2)}) collective-permute-start(bf16[128,768]{1,0:T(8,128)(2,1)S(1)} %get-tuple-element.17.refs_1_), channel_id=1, source_target_pairs={{0,24},{8,0},{16,8},{24,16},{1,25},{9,1},{17,9},{25,17},{2,26},{10... | collective-permute-start | bytes 589832 | tf_op jit(solution)/shard_map/ppermute | solution.py:25
  15.8 2.3 %shard_map.222 = (bf16[8,512]{1,0:T(8,128)(2,1)S(1)}, f32[24,128]{1,0:T(8,128)S(1)}) custom-call(bf16[24,4096]{1,0:T(8,128)(2,1)} %refs_1_.2, f32[1,4096]{1,0:T(1,128)} %bitcast.36, bf16[16,4096]{1,0:T(8,128)(2,1)} %bitcast.33, bf16[16,4096]{1,0:T(8,128)(2,1)} %bitcast.34, f32[1,2]{1,0:T(1,128)} %bitcast.40, s32[2,24]{1,0:T(2,128)} %bitcast.37, ...), custom_call_target="tpu_custom_call" | custom-call | flops 100000000 | tf_op jit(solution)/shard_map/pallas_call | solution.py:97
  18.1 0.0 copy-start.9
  18.1 0.6 copy-done.9
  18.7 0.1 collective-permute-done.2.refs_4_
  18.8 3.0 %collective-permute-done.1.refs_3_ = bf16[128,768]{1,0:T(8,128)(2,1)S(1)} collective-permute-done((bf16[128,768]{1,0:T(8,128)(2,1)S(1)}, bf16[128,768]{1,0:T(8,128)(2,1)S(1)}, u32[]{:S(2)}, u32[]{:S(2)}) %collective-permute-start.1) | collective-permute-done | bytes 196640 | tf_op jit(solution)/shard_map/ppermute | solution.py:25
  21.8 0.0 copy-done.13
  21.8 0.7 copy-done.14
  22.5 1.3 collective-permute-done.refs_2_
  23.8 0.0 all-to-all-done.refs_0_
  23.8 0.0 copy-done.8
  23.8 0.7 copy-done.6
  24.5 0.9 copy-done.7
  25.4 1.7 %shard_map.223.refs_0_ = bf16[8,24,768]{2,1,0:T(8,128)(2,1)S(1)} custom-call(bf16[8,24,512]{2,1,0:T(8,128)(2,1)S(1)} %copy-done.7, bf16[128,768]{1,0:T(8,128)(2,1)} %copy-done.8, bf16[128,768]{1,0:T(8,128)(2,1)} %collective-permute-done.refs_2_, bf16[128,768]{1,0:T(8,128)(2,1)} %copy-done.14, bf16[128,768]{1,0:T(8,128)(2,1)} %copy-done.13, f32[24,128]{1,0:T(8,128)} %copy-done.9), custom_call_target="tpu_custom_call" | custom-call | flops 150994944 | tf_op jit(solution)/shard_map/pallas_call | solution.py:97
  27.1 0.0 copy-start.2
  27.1 0.0 copy-start.3
  27.1 18.9 %all_to_all.35.refs_0_ = bf16[8,24,768]{2,1,0:T(8,128)(2,1)S(1)} all-to-all(bf16[8,24,768]{2,1,0:T(8,128)(2,1)S(1)} %shard_map.223.refs_0_), channel_id=1, replica_groups=mesh['z'=8,'x'=4,'y'=4,'c'=2] {'z'}, dimensions={0} | all-to-all | bytes 589824 | tf_op jit(solution)/shard_map/all_to_all | solution.py:17
  46.1 0.0 copy-done
  46.1 2.1 %shard_map.224 = (bf16[8,24,512]{2,1,0:T(8,128)(2,1)S(1)}, f32[24,256]{1,0:T(8,128)S(1)}, f32[24,256]{1,0:T(8,128)S(1)}) custom-call(bf16[8,24,768]{2,1,0:T(8,128)(2,1)S(1)} %all_to_all.35.refs_0_, f32[24,128]{1,0:T(8,128)} %copy-done.9, f32[24,2,128,128]{3,2,1,0:T(8,128)S(1)} %copy-done, f32[1,128]{1,0:T(1,128)} %bitcast.39, bf16[256,4096]{1,0:T(8,128)(2,1)} %refs_4_.3), custom_call_target="tpu_custom_call" | custom-call | flops 50331648 | tf_op jit(solution)/shard_map/pallas_call | solution.py:97
  48.2 0.0 copy-start.10
  48.2 0.0 copy-start.11
  48.2 11.1 %all_to_all.36.refs_0_ = bf16[8,24,512]{2,1,0:T(8,128)(2,1)S(1)} all-to-all(bf16[8,24,512]{2,1,0:T(8,128)(2,1)S(1)} %get-tuple-element.19), channel_id=1, replica_groups=mesh['z'=8,'x'=4,'y'=4,'c'=2] {'y','c'}, dimensions={0} | all-to-all | bytes 393216 | tf_op jit(solution)/shard_map/all_to_all | solution.py:17
  59.3 0.0 copy-done.2
  59.3 0.0 copy-done.10
  59.3 0.0 copy-done.11
  59.3 0.0 copy-done.3
  59.3 0.7 shard_map.225
  60.0 3.4 %all-to-all-start.3 = ((bf16[8,32,512]{2,1,0:T(8,128)(2,1)}), bf16[8,32,512]{2,1,0:T(8,128)(2,1)S(1)}, u32[]{:S(2)}, u32[]{:S(2)}) async-start(bf16[8,32,512]{2,1,0:T(8,128)(2,1)} %get-tuple-element.21), calls=%async_computation.3 | async-start | bytes 524288 | tf_op jit(solution)/shard_map/all_to_all | solution.py:17
  63.4 0.0 copy-start.1
  63.5 1.2 shard_map.226.refs_2_.refs_3_
  64.6 0.2 collective-permute-start.5
  64.8 2.3 %collective-permute-start.4 = (bf16[768,256]{1,0:T(8,128)(2,1)S(1)}, bf16[768,256]{1,0:T(8,128)(2,1)S(1)}, u32[]{:S(2)}, u32[]{:S(2)}) collective-permute-start(bf16[768,256]{1,0:T(8,128)(2,1)S(1)} %shard_map.226.refs_2_.refs_3_), channel_id=1, source_target_pairs={{0,16},{8,24},{16,0},{24,8},{1,17},{9,25},{17,1},{25,9},{2,18},{10... | collective-permute-start | bytes 1179656 | tf_op jit(solution)/shard_map/ppermute | solution.py:25
  67.1 1.9 %collective-permute-start.3 = (bf16[768,256]{1,0:T(8,128)(2,1)S(1)}, bf16[768,256]{1,0:T(8,128)(2,1)S(1)}, u32[]{:S(2)}, u32[]{:S(2)}) collective-permute-start(bf16[768,256]{1,0:T(8,128)(2,1)S(1)} %shard_map.226.refs_2_.refs_3_), channel_id=1, source_target_pairs={{0,24},{8,0},{16,8},{24,16},{1,25},{9,1},{17,9},{25,17},{2,26},{10... | collective-permute-start | bytes 1179656 | tf_op jit(solution)/shard_map/ppermute | solution.py:25
  69.0 7.7 %collective-permute-done.5.refs_5_.refs_6_ = bf16[768,256]{1,0:T(8,128)(2,1)S(1)} collective-permute-done((bf16[768,256]{1,0:T(8,128)(2,1)S(1)}, bf16[768,256]{1,0:T(8,128)(2,1)S(1)}, u32[]{:S(2)}, u32[]{:S(2)}) %collective-permute-start.5) | collective-permute-done | bytes 393248 | tf_op jit(solution)/shard_map/ppermute | solution.py:25
  76.7 1.7 %collective-permute-done.4.refs_4_.refs_5_ = bf16[768,256]{1,0:T(8,128)(2,1)S(1)} collective-permute-done((bf16[768,256]{1,0:T(8,128)(2,1)S(1)}, bf16[768,256]{1,0:T(8,128)(2,1)S(1)}, u32[]{:S(2)}, u32[]{:S(2)}) %collective-permute-start.4) | collective-permute-done | bytes 393248 | tf_op jit(solution)/shard_map/ppermute | solution.py:25
  78.4 7.0 %collective-permute-done.3.refs_3_.refs_4_ = bf16[768,256]{1,0:T(8,128)(2,1)S(1)} collective-permute-done((bf16[768,256]{1,0:T(8,128)(2,1)S(1)}, bf16[768,256]{1,0:T(8,128)(2,1)S(1)}, u32[]{:S(2)}, u32[]{:S(2)}) %collective-permute-start.3) | collective-permute-done | bytes 393248 | tf_op jit(solution)/shard_map/ppermute | solution.py:25
  85.3 0.0 all-to-all-done.3.refs_0_
  85.3 1.2 shard_map.227
  86.5 0.1 collective-permute-start.6
  86.6 1.4 collective-permute-done.6.refs_6_
  88.0 1.1 shard_map.228
  89.2 16.5 %all_to_all.37 = bf16[16,80,256]{2,1,0:T(8,128)(2,1)S(1)} all-to-all(bf16[16,80,256]{2,1,0:T(8,128)(2,1)S(1)} %bitcast.27), channel_id=1, replica_groups=mesh['z'=8,'x'=4,'y'=4,'c'=2] {'x','y'}, dimensions={0} | all-to-all | bytes 1310720 | tf_op jit(solution)/shard_map/all_to_all | solution.py:17
  105.6 0.0 collective-permute-start.7
  105.6 2.1 %collective-permute-done.7 = bf16[16,80,256]{2,1,0:T(8,128)(2,1)S(1)} collective-permute-done((bf16[16,80,256]{2,1,0:T(8,128)(2,1)S(1)}, bf16[16,80,256]{2,1,0:T(8,128)(2,1)S(1)}, u32[]{:S(2)}, u32[]{:S(2)}) %collective-permute-start.7) | collective-permute-done | bytes 655392 | tf_op jit(solution)/shard_map/ppermute | solution.py:592
  107.7 0.0 copy-done.5
  107.7 0.0 copy-start.12
  107.8 1.6 %shard_map.229 = (bf16[4,4,24,512]{3,2,1,0:T(8,128)(2,1)S(1)}, bf16[96,128]{1,0:T(8,128)(2,1)S(1)}, bf16[4,24,128]{2,1,0:T(8,128)(2,1)S(1)}) custom-call(bf16[4,4,80,256]{3,2,1,0:T(8,128)(2,1)S(1)} %bitcast.21, bf16[4,4,80,256]{3,2,1,0:T(8,128)(2,1)S(1)} %bitcast.26, f32[1,4096]{1,0:T(1,128)} %bitcast.32, bf16[4096,128]{1,0:T(8,128)(2,1)S(1)} %bitcast.24, ...), custom_call_target="tpu_custom_call" | custom-call | flops 251658240 | tf_op jit(solution)/shard_map/pallas_call | solution.py:97
  109.3 0.2 collective-permute-start.8
  109.6 1.6 %collective-permute-done.8.refs_2_ = bf16[4,4,24,512]{3,2,1,0:T(8,128)(2,1)S(1)} collective-permute-done((bf16[4,4,24,512]{3,2,1,0:T(8,128)(2,1)S(1)}, bf16[4,4,24,512]{3,2,1,0:T(8,128)(2,1)S(1)}, u32[]{:S(2)}, u32[]{:S(2)}) %collective-permute-start.8) | collective-permute-done | bytes 393248 | tf_op jit(solution)/shard_map/ppermute | solution.py:610
  111.2 0.3 shard_map.230
  111.4 14.1 %all_to_all.38 = bf16[16,24,640]{2,1,0:T(8,128)(2,1)S(1)} all-to-all(bf16[16,24,640]{2,1,0:T(8,128)(2,1)S(1)} %bitcast.23), channel_id=1, replica_groups=mesh['z'=8,'x'=4,'y'=4,'c'=2] {'x','y'}, dimensions={0} | all-to-all | bytes 983040 | tf_op jit(solution)/shard_map/all_to_all | solution.py:17
  125.5 0.0 collective-permute-start.9
  125.5 1.9 %collective-permute-done.9 = bf16[16,24,640]{2,1,0:T(8,128)(2,1)S(1)} collective-permute-done((bf16[16,24,640]{2,1,0:T(8,128)(2,1)S(1)}, bf16[16,24,640]{2,1,0:T(8,128)(2,1)S(1)}, u32[]{:S(2)}, u32[]{:S(2)}) %collective-permute-start.9) | collective-permute-done | bytes 491552 | tf_op jit(solution)/shard_map/ppermute | solution.py:615
  127.4 1.2 shard_map.231
  128.6 6.8 %all-to-all-start.6 = ((bf16[8,24,512]{2,1,0:T(8,128)(2,1)}), bf16[8,24,512]{2,1,0:T(8,128)(2,1)S(1)}, u32[]{:S(2)}, u32[]{:S(2)}) async-start(bf16[8,24,512]{2,1,0:T(8,128)(2,1)} %shard_map.231), calls=%async_computation.6 | async-start | bytes 393216 | tf_op jit(solution)/shard_map/all_to_all | solution.py:17
  135.4 4.3 %shard_map.233 = f32[24,2,128,128]{3,2,1,0:T(8,128)} custom-call(f32[24,256]{1,0:T(8,128)} %copy-done.10, f32[24,256]{1,0:T(8,128)} %copy-done.11, f32[24,128]{1,0:T(8,128)} %copy-done.9, f32[24,2,128,128]{3,2,1,0:T(8,128)} %refs_3_.5), custom_call_target="tpu_custom_call" | custom-call | flops 100000000 | tf_op jit(solution)/shard_map/pallas_call | solution.py:97
  139.7 6.5 %all-to-all-done.6.refs_0_ = bf16[8,24,512]{2,1,0:T(8,128)(2,1)S(1)} async-done(((bf16[8,24,512]{2,1,0:T(8,128)(2,1)}), bf16[8,24,512]{2,1,0:T(8,128)(2,1)S(1)}, u32[]{:S(2)}, u32[]{:S(2)}) %all-to-all-start.6) | async-done | bytes 196640 | tf_op jit(solution)/shard_map/all_to_all | solution.py:17
  146.2 0.6 shard_map.232
  (9 shorter events, 0.0 us)
Async XLA Ops:
  0.6 45.4 %copy-start = (f32[24,2,128,128]{3,2,1,0:T(8,128)S(1)}, f32[24,2,128,128]{3,2,1,0:T(8,128)}, u32[]{:S(2)}) copy-start(f32[24,2,128,128]{3,2,1,0:T(8,128)} %refs_3_.5) | copy-start | bytes 9437188
  2.6 21.2 %copy-start.8 = (bf16[128,768]{1,0:T(8,128)(2,1)}, bf16[128,768]{1,0:T(8,128)(2,1)S(1)}, u32[]{:S(2)}) copy-start(bf16[128,768]{1,0:T(8,128)(2,1)S(1)} %get-tuple-element.17.refs_1_) | copy-start | bytes 589828
  2.6 21.2 %all-to-all-start = ((bf16[8,24,512]{2,1,0:T(8,128)(2,1)}), bf16[8,24,512]{2,1,0:T(8,128)(2,1)S(1)}, u32[]{:S(2)}, u32[]{:S(2)}) async-start(bf16[8,24,512]{2,1,0:T(8,128)(2,1)} %get-tuple-element.16), calls=%async_computation | async-start | bytes 393216 | tf_op jit(solution)/shard_map/all_to_all | solution.py:17
  11.1 7.8 %collective-permute-start.2 = (bf16[128,768]{1,0:T(8,128)(2,1)S(1)}, bf16[128,768]{1,0:T(8,128)(2,1)S(1)}, u32[]{:S(2)}, u32[]{:S(2)}) collective-permute-start(bf16[128,768]{1,0:T(8,128)(2,1)S(1)} %get-tuple-element.17.refs_1_), channel_id=1, source_target_pairs={{0,8},{8,16},{16,24},{24,0},{1,9},{9,17},{17,25},{25,1},{2,10},{10... | collective-permute-start | bytes 589832 | tf_op jit(solution)/shard_map/ppermute | solution.py:25
  12.6 9.3 %collective-permute-start.1 = (bf16[128,768]{1,0:T(8,128)(2,1)S(1)}, bf16[128,768]{1,0:T(8,128)(2,1)S(1)}, u32[]{:S(2)}, u32[]{:S(2)}) collective-permute-start(bf16[128,768]{1,0:T(8,128)(2,1)S(1)} %get-tuple-element.17.refs_1_), channel_id=1, source_target_pairs={{0,16},{8,24},{16,0},{24,8},{1,17},{9,25},{17,1},{25,9},{2,18},{10... | collective-permute-start | bytes 589832 | tf_op jit(solution)/shard_map/ppermute | solution.py:25
  13.7 10.1 %collective-permute-start = (bf16[128,768]{1,0:T(8,128)(2,1)S(1)}, bf16[128,768]{1,0:T(8,128)(2,1)}, u32[]{:S(2)}, u32[]{:S(2)}) collective-permute-start(bf16[128,768]{1,0:T(8,128)(2,1)S(1)} %get-tuple-element.17.refs_1_), channel_id=1, source_target_pairs={{0,24},{8,0},{16,8},{24,16},{1,25},{9,1},{17,9},{25,17},{2,26},{10... | collective-permute-start | bytes 589832 | tf_op jit(solution)/shard_map/ppermute | solution.py:25
  18.1 0.6 copy-start.9
  18.8 3.0 %copy-start.13 = (bf16[128,768]{1,0:T(8,128)(2,1)}, bf16[128,768]{1,0:T(8,128)(2,1)S(1)}, u32[]{:S(2)}) copy-start(bf16[128,768]{1,0:T(8,128)(2,1)S(1)} %collective-permute-done.2.refs_4_) | copy-start | bytes 589828
  21.8 0.7 copy-start.14
  23.8 0.7 copy-start.6
  24.5 0.9 copy-start.7
  27.1 32.2 %copy-start.2 = (bf16[8,24,768]{2,1,0:T(8,128)(2,1)}, bf16[8,24,768]{2,1,0:T(8,128)(2,1)S(1)}, u32[]{:S(2)}) copy-start(bf16[8,24,768]{2,1,0:T(8,128)(2,1)S(1)} %shard_map.223.refs_0_) | copy-start | bytes 884740
  27.1 32.2 %copy-start.3 = (bf16[24,4096]{1,0:T(8,128)(2,1)S(1)}, bf16[24,4096]{1,0:T(8,128)(2,1)}, u32[]{:S(2)}) copy-start(bf16[24,4096]{1,0:T(8,128)(2,1)} %refs_1_.2) | copy-start | bytes 589828
  48.2 11.1 %copy-start.10 = (f32[24,256]{1,0:T(8,128)}, f32[24,256]{1,0:T(8,128)S(1)}, u32[]{:S(2)}) copy-start(f32[24,256]{1,0:T(8,128)S(1)} %get-tuple-element.28.refs_0_) | copy-start | bytes 73732
  48.2 11.1 %copy-start.11 = (f32[24,256]{1,0:T(8,128)}, f32[24,256]{1,0:T(8,128)S(1)}, u32[]{:S(2)}) copy-start(f32[24,256]{1,0:T(8,128)S(1)} %get-tuple-element.29.refs_1_) | copy-start | bytes 73732
  60.0 25.3 %all-to-all-start.3 = ((bf16[8,32,512]{2,1,0:T(8,128)(2,1)}), bf16[8,32,512]{2,1,0:T(8,128)(2,1)S(1)}, u32[]{:S(2)}, u32[]{:S(2)}) async-start(bf16[8,32,512]{2,1,0:T(8,128)(2,1)} %get-tuple-element.21), calls=%async_computation.3 | async-start | bytes 524288 | tf_op jit(solution)/shard_map/all_to_all | solution.py:17
  63.4 44.3 %copy-start.1 = (bf16[1,128,4096]{2,1,0:T(8,128)(2,1)S(1)}, bf16[1,128,4096]{2,1,0:T(8,128)(2,1)}, u32[]{:S(2)}) copy-start(bf16[1,128,4096]{2,1,0:T(8,128)(2,1)} %param.39) | copy-start | bytes 3145732
  64.6 12.1 %collective-permute-start.5 = (bf16[768,256]{1,0:T(8,128)(2,1)S(1)}, bf16[768,256]{1,0:T(8,128)(2,1)S(1)}, u32[]{:S(2)}, u32[]{:S(2)}) collective-permute-start(bf16[768,256]{1,0:T(8,128)(2,1)S(1)} %shard_map.226.refs_2_.refs_3_), channel_id=1, source_target_pairs={{0,8},{8,16},{16,24},{24,0},{1,9},{9,17},{17,25},{25,1},{2,10},{10... | collective-permute-start | bytes 1179656 | tf_op jit(solution)/shard_map/ppermute | solution.py:25
  64.8 13.5 %collective-permute-start.4 = (bf16[768,256]{1,0:T(8,128)(2,1)S(1)}, bf16[768,256]{1,0:T(8,128)(2,1)S(1)}, u32[]{:S(2)}, u32[]{:S(2)}) collective-permute-start(bf16[768,256]{1,0:T(8,128)(2,1)S(1)} %shard_map.226.refs_2_.refs_3_), channel_id=1, source_target_pairs={{0,16},{8,24},{16,0},{24,8},{1,17},{9,25},{17,1},{25,9},{2,18},{10... | collective-permute-start | bytes 1179656 | tf_op jit(solution)/shard_map/ppermute | solution.py:25
  67.1 18.2 %collective-permute-start.3 = (bf16[768,256]{1,0:T(8,128)(2,1)S(1)}, bf16[768,256]{1,0:T(8,128)(2,1)S(1)}, u32[]{:S(2)}, u32[]{:S(2)}) collective-permute-start(bf16[768,256]{1,0:T(8,128)(2,1)S(1)} %shard_map.226.refs_2_.refs_3_), channel_id=1, source_target_pairs={{0,24},{8,0},{16,8},{24,16},{1,25},{9,1},{17,9},{25,17},{2,26},{10... | collective-permute-start | bytes 1179656 | tf_op jit(solution)/shard_map/ppermute | solution.py:25
  85.3 22.4 %copy-start.4 = (bf16[1,4096,128]{2,1,0:T(8,128)(2,1)S(1)}, bf16[1,4096,128]{2,1,0:T(8,128)(2,1)}, u32[]{:S(2)}) copy-start(bf16[1,4096,128]{2,1,0:T(8,128)(2,1)} %param.37) | copy-start | bytes 3145732
  85.3 22.4 %copy-start.5 = (bf16[1,4096,128]{2,1,0:T(8,128)(2,1)S(1)}, bf16[1,4096,128]{2,1,0:T(8,128)(2,1)}, u32[]{:S(2)}) copy-start(bf16[1,4096,128]{2,1,0:T(8,128)(2,1)} %param.38) | copy-start | bytes 3145732
  86.5 1.5 %collective-permute-start.6 = (bf16[4,4,24,256]{3,2,1,0:T(8,128)(2,1)S(1)}, bf16[4,4,24,256]{3,2,1,0:T(8,128)(2,1)S(1)}, u32[]{:S(2)}, u32[]{:S(2)}) collective-permute-start(bf16[4,4,24,256]{3,2,1,0:T(8,128)(2,1)S(1)} %shard_map.227), channel_id=1, source_target_pairs={{0,1},{1,0},{2,3},{3,2},{4,5},{5,4},{6,7},{7,6},{8,9},{9,8},{10,11... | collective-permute-start | bytes 589832 | tf_op jit(solution)/shard_map/ppermute | solution.py:585
  105.6 2.1 %collective-permute-start.7 = (bf16[16,80,256]{2,1,0:T(8,128)(2,1)S(1)}, bf16[16,80,256]{2,1,0:T(8,128)(2,1)S(1)}, u32[]{:S(2)}, u32[]{:S(2)}) collective-permute-start(bf16[16,80,256]{2,1,0:T(8,128)(2,1)S(1)} %all_to_all.37), channel_id=1, source_target_pairs={{0,1},{1,0},{2,3},{3,2},{4,5},{5,4},{6,7},{7,6},{8,9},{9,8},{10,11... | collective-permute-start | bytes 1966088 | tf_op jit(solution)/shard_map/ppermute | solution.py:592
  107.7 19.6 %copy-start.12 = (f32[512]{0:T(512)S(1)}, f32[512]{0:T(512)}, u32[]{:S(2)}) copy-start(f32[512]{0:T(512)} %param.43) | copy-start | bytes 6148
  109.3 1.8 %collective-permute-start.8 = (bf16[4,4,24,512]{3,2,1,0:T(8,128)(2,1)S(1)}, bf16[4,4,24,512]{3,2,1,0:T(8,128)(2,1)S(1)}, u32[]{:S(2)}, u32[]{:S(2)}) collective-permute-start(bf16[4,4,24,512]{3,2,1,0:T(8,128)(2,1)S(1)} %get-tuple-element.25), channel_id=1, source_target_pairs={{0,1},{1,0},{2,3},{3,2},{4,5},{5,4},{6,7},{7,6},{8,9},{9,8},{10,11... | collective-permute-start | bytes 1179656 | tf_op jit(solution)/shard_map/ppermute | solution.py:610
  125.5 1.9 %collective-permute-start.9 = (bf16[16,24,640]{2,1,0:T(8,128)(2,1)S(1)}, bf16[16,24,640]{2,1,0:T(8,128)(2,1)S(1)}, u32[]{:S(2)}, u32[]{:S(2)}) collective-permute-start(bf16[16,24,640]{2,1,0:T(8,128)(2,1)S(1)} %all_to_all.38), channel_id=1, source_target_pairs={{0,1},{1,0},{2,3},{3,2},{4,5},{5,4},{6,7},{7,6},{8,9},{9,8},{10,11... | collective-permute-start | bytes 1474568 | tf_op jit(solution)/shard_map/ppermute | solution.py:615
  128.6 17.6 %all-to-all-start.6 = ((bf16[8,24,512]{2,1,0:T(8,128)(2,1)}), bf16[8,24,512]{2,1,0:T(8,128)(2,1)S(1)}, u32[]{:S(2)}, u32[]{:S(2)}) async-start(bf16[8,24,512]{2,1,0:T(8,128)(2,1)} %shard_map.231), calls=%async_computation.6 | async-start | bytes 393216 | tf_op jit(solution)/shard_map/all_to_all | solution.py:17

commit v3 on v2

--- a/solution.py
+++ b/solution.py
@@ -294,21 +294,8 @@
     return slots
 
 
-def half_tokens(arrived, gain, core, rows):
-    blocks = [arrived[2 * y + core, :rows, :].astype(F32) for y in range(NY)]
-    return (jnp.concatenate(blocks, axis=0) * gain[...]).astype(BF)
-
-
-def away_body(index, arrived, gain, g0, g1, g2, g3, out):
-    rows, half = out.shape[2:]
-    scaled = half_tokens(arrived, gain, 1 - index[3], rows)
-    for step, weight in enumerate((g0, g1, g2, g3)):
-        part = jnp.dot(scaled, weight[: arrived.shape[2], :], preferred_element_type=F32)
-        out[wrapped(index[1] + step, NX)] = part.reshape(NY, rows, half).astype(BF)
-
-
-def dispatch_body(index, arrived, gain, g0, g1, g2, g3, away, out, route):
-    rows = away.shape[2]
+def dispatch_body(index, arrived, gain, g0, g1, g2, g3, after, out, route):
+    rows = arrived.shape[1] - 8
     tokens = NZ * rows
     block = arrived.shape[2]
     half = block // 2
@@ -337,17 +324,18 @@
         for y in range(NY):
             out[x, y, :rows, :] = own[:, :half]
             out[x, y, rows : 2 * rows, :] = own[:, half:]
-            out[x, y, 3 * rows :, :tokens] = square
-            out[x, y, 3 * rows :, tokens:] = jnp.zeros((8, half - tokens), BF)
-    scaled = half_tokens(arrived, gain, index[3], rows)
+            out[x, y, 4 * rows :, :tokens] = square
+            out[x, y, 4 * rows :, tokens:] = jnp.zeros((8, half - tokens), BF)
+    scaled = (wide * gain[...]).astype(BF)
     for step, weight in enumerate((g0, g1, g2, g3)):
-        part = jnp.dot(scaled, weight[: arrived.shape[2], :], preferred_element_type=F32).reshape(NY, rows, half)
+        part = jnp.dot(scaled, weight[...], preferred_element_type=F32)
         x = wrapped(index[1] + step, NX)
-        out[x, :, 2 * rows : 3 * rows, :] = (part + away[x].astype(F32)).astype(BF)
+        out[x, :, 2 * rows : 4 * rows, :] = part.reshape(NY, 2 * rows, half).astype(BF)
 
 
 def expert_body(index, arrived, partner, gain, gate, up, down, away, hidden, dense):
     rows, block = away.shape[2:]
+    size = gate.shape[1]
     half = block // 2
     width = gate.shape[0]
     slots = NX * rows
@@ -379,26 +367,34 @@
         summed = jnp.zeros((rows, half), F32)
         square = jnp.zeros((8, tokens), F32)
         for y in range(NY):
-            summed = summed + arrived[x, y, 2 * rows : 3 * rows, :].astype(F32)
             for source in (arrived, partner):
-                square = square + source[x, y, 3 * rows :, :tokens].astype(F32)
+                both = source[x, y, 2 * rows : 4 * rows, :].astype(F32)
+                summed = summed + jnp.where(index[3] == 0, both[:rows], both[rows:])
+                square = square + source[x, y, 4 * rows :, :tokens].astype(F32)
         square = square[0:1, :] + square[1:2, :]
         square = jnp.sum(jnp.where(own, square, 0.0), axis=1, keepdims=True)
         summed = summed * lax.rsqrt(square / width + EPS)
-        dense[x] = (silu(summed[:, : half // 2]) * summed[:, half // 2 :]).astype(BF)
+        result = (silu(summed[:, : half // 2]) * summed[:, half // 2 :]).astype(BF)
+        dense[x] = result
+        away[x, NY, :, :size] = result
+        away[x, NY, :, size:] = jnp.zeros((rows, block - size), BF)
 
 
 def result_body(index, hidden, dense, away, down, out):
     rows, block = away.shape[2:]
+    size = dense.shape[2]
+    own_place = pl.multiple_of(block + index[3] * size, size)
+    far_place = pl.multiple_of(block + (1 - index[3]) * size, size)
     for y in range(NY):
         place = pl.multiple_of((2 * y + index[3]) * block, block)
         part = jnp.dot(hidden[...], down[:, pl.ds(place, block)], preferred_element_type=F32)
         part = part.reshape(NX, rows, block) + away[:, y].astype(F32)
         out[:, y, :, :block] = part.astype(BF)
-        out[:, y, :, block:] = dense[...]
-
-
-def combine_body(index, arrived, partner, route, d0, d1, d2, d3, mix, out, mixed):
+        out[:, y, :, pl.ds(own_place, size)] = dense[...]
+        out[:, y, :, pl.ds(far_place, size)] = away[:, NY, :, :size]
+
+
+def combine_body(index, arrived, route, d0, d1, d2, d3, mix, out):
     rows = arrived.shape[2]
     block = out.shape[2]
     tokens = NZ * rows
@@ -419,21 +415,22 @@
         total += lax.dot_general(
             share, results, (((0,), (0,)), ((), ())), preferred_element_type=F32
         )
-    mixed[...] = total.reshape(NZ, rows, block)
     gate = 1.0 / (1.0 + jnp.exp(-mix[...]))
-    for source, core in ((arrived, index[3]), (partner, 1 - index[3])):
+    total = total.reshape(NY, 2, rows, block)
+    size = (arrived.shape[3] - block) // 2
+    for core in range(2):
         lower = jnp.zeros((NY * rows, block // 2), F32)
         upper = jnp.zeros((NY * rows, block // 2), F32)
+        lanes = slice(block + core * size, block + (core + 1) * size)
         for step, weight in enumerate((d0, d1, d2, d3)):
             x = wrapped(index[1] + step, NX)
-            left = source[x, :, :, block:].astype(F32).reshape(NY * rows, -1).astype(BF)
-            size = left.shape[1]
-            lower += jnp.dot(left, weight[block : block + size, :], preferred_element_type=F32)
-            upper += jnp.dot(left, weight[block + size :, :], preferred_element_type=F32)
+            left = arrived[x, :, :, lanes].astype(F32).reshape(NY * rows, size).astype(BF)
+            lower += jnp.dot(left, weight[:size, :], preferred_element_type=F32)
+            upper += jnp.dot(left, weight[size:, :], preferred_element_type=F32)
         dense = gate * jnp.concatenate((lower, upper), axis=1)
         for y in range(NY):
-            z = 2 * y + core
-            out[z] = (dense[y * rows : (y + 1) * rows] + mixed[z]).astype(BF)
+            own = dense[y * rows : (y + 1) * rows] + total[y, core]
+            out[2 * y + core] = own.astype(BF)
 
 
 def final_body(index, arrived, middle, out):
@@ -565,34 +562,27 @@
 
     swap = [(0, 1), (1, 0)]
     arrived = exchange(message, "z")
-    gain_part = {1: ((1, block), own_block)}
-    (away,) = kernel(
-        away_body,
-        (shape(NX, NY, rows, half),),
+    message, route_rows = kernel(
+        dispatch_body,
+        (shape(NX, NY, 4 * rows + 8, half), shape(8, NZ * rows, dtype=F32)),
         arrived,
         ffn_gain[None],
         *dense_weights,
-        far=(1,),
-        parts=gain_part,
-        flops=NZ * rows * block * 2 * block,
-    )
-    message, route_rows = kernel(
-        dispatch_body,
-        (shape(NX, NY, 3 * rows + 8, half), shape(8, NZ * rows, dtype=F32)),
-        arrived,
-        ffn_gain[None],
-        *dense_weights,
-        lax.ppermute(away, "c", swap),
-        far=(1,),
-        parts=gain_part,
-        flops=NZ * rows * block * 2 * block,
+        new_state,
+        far=range(1, 6),
+        plain=(6,),
+        parts={
+            1: ((1, block), own_block),
+            **{n: ((block, half), lambda ref, index: ref.at[:block]) for n in range(2, 6)},
+        },
+        flops=2 * NZ * rows * block * 2 * block,
     )
     sides = ("x", "y")
     arrived = exchange(message.reshape(NX * NY, -1, half), sides)
     partner = lax.ppermute(arrived, "c", swap).reshape(message.shape)
     away, hidden, dense = kernel(
         expert_body,
-        (shape(NX, NY, rows, block), shape(NX * rows, 128), shape(NX, rows, 128)),
+        (shape(NX, NY + 1, rows, block), shape(NX * rows, 128), shape(NX, rows, 128)),
         arrived.reshape(message.shape),
         partner,
         ffn_gain[None],
@@ -604,7 +594,7 @@
     )
     (message,) = kernel(
         result_body,
-        (shape(NX, NY, rows, block + 128),),
+        (shape(NX, NY, rows, block + 2 * 128),),
         hidden,
         dense,
         lax.ppermute(away, "c", swap),
@@ -612,16 +602,15 @@
         flops=NX * rows * width * 128,
     )
     arrived = exchange(message.reshape(NX * NY, rows, -1), sides)
-    partner = lax.ppermute(arrived, "c", swap).reshape(message.shape)
     (message,) = kernel(
         combine_body,
         (shape(NZ, rows, block),),
         arrived.reshape(message.shape),
-        partner,
         route_rows,
         *dense_weights,
         dense_mix[None],
-        scratch=(pltpu.VMEM((NZ, rows, block), F32),),
+        far=range(1, 7),
+        parts={n: ((half, half), lambda ref, index: ref.at[block:]) for n in range(2, 6)},
         flops=2 * NZ * rows * block * block,
     )
     arrived = exchange(message, "z")

time: 149 us -> 149 us (level)
  blocking collectives: 60.6 us -> 80.9 us
  waiting for transfers between devices: 34.2 us -> 20.6 us
  starting transfers between devices: 28.1 us -> 21.2 us
    all_to_all x4 -> x5, blocking collectives: 60.6 us -> 80.9 us  [exchange(): return lax.all_to_all(tiles, axes, split_axis=0, concat_axis=0, tiled=True)]
    all_to_all x3 -> x2, starting transfers between devices: 18.7 us -> 11.9 us  [exchange(): return lax.all_to_all(tiles, axes, split_axis=0, concat_axis=0, tiled=True)]
    all_to_all x3 -> x2, waiting for transfers between devices: 6.52 us -> 0.01 us  [exchange(): return lax.all_to_all(tiles, axes, split_axis=0, concat_axis=0, tiled=True)]
    ppermute x6, waiting for transfers between devices: 20.8 us -> 16.5 us  [from_neighbours(): parts.append(lax.ppermute(shard, axis, pairs))]
    ppermute x2 -> x1, waiting for transfers between devices: 3.96 us -> 2.38 us  [per_device(): partner = lax.ppermute(arrived, 'c', swap).reshape(message.shape)]
    ppermute x2 -> x1, waiting for transfers between devices: 3.01 us -> 1.73 us  [per_device(): lax.ppermute(away, 'c', swap)]
    unnamed x30 -> x38, local copies, waits for them, and re-layouts: 2.92 us -> 3.66 us
    pallas_call x13 -> x12, Pallas kernels: 20.1 us -> 20.7 us  [kernel(): pl.pallas_call(run, out_shape=outs, in_specs=specs, out_specs=out_specs,...]
  transfers between devices with their start and end apart: 13 -> 10, of which waited for: 11 -> 8; matrix products, arithmetic and copies ran while one was open for 0% -> 0% of each run, Pallas kernels for 5% -> 5%
where the time goes in v3:
time: 149 us; the launch traced here: 148 us
  blocking collectives  80.9 us (54%)
  starting transfers between devices  21.2 us (14%)
  Pallas kernels  20.7 us (14%)
  waiting for transfers between devices  20.6 us (14%)
  local copies, waits for them, and re-layouts  3.66 us (2%)
    all_to_all x5, blocking collectives, exchange(): return lax.all_to_all(tiles, axes, split_axis=0, concat_axis=0, tiled=True)  80.9 us
    pallas_call x12, Pallas kernels, kernel(): pl.pallas_call(run, out_shape=outs, in_specs=specs, out_specs=out_specs,...  20.7 us
    ppermute x6, waiting for transfers between devices, from_neighbours(): parts.append(lax.ppermute(shard, axis, pairs))  16.5 us
    all_to_all x2, starting transfers between devices, exchange(): return lax.all_to_all(tiles, axes, split_axis=0, concat_axis=0, tiled=True)  11.9 us
    ppermute x6, starting transfers between devices, from_neighbours(): parts.append(lax.ppermute(shard, axis, pairs))  9.09 us
    unnamed x38, local copies, waits for them, and re-layouts  3.66 us
  transfers between devices with their start and end apart: 10, of which 8 were waited for; matrix products, arithmetic and copies ran while one was open for 0% of the time, Pallas kernels for 5%

profile of v3, /device:TPU:2, one launch (start us, length us, event | category | flops | bytes accessed | tf_op | source)
XLA Modules:
  0.0 147.9 jit_solution(12293055781144891249)
XLA Ops:
  0.6 0.0 copy-start
  0.6 1.9 %shard_map.221 = (bf16[8,24,512]{2,1,0:T(8,128)(2,1)}, bf16[128,768]{1,0:T(8,128)(2,1)S(1)}) custom-call(bf16[24,4096]{1,0:T(8,128)(2,1)} %refs_1_.2, f32[1,4096]{1,0:T(1,128)} %bitcast.31, bf16[128,256]{1,0:T(8,128)(2,1)} %refs_2_.3, bf16[128,256]{1,0:T(8,128)(2,1)} %refs_3_.3, bf16[128,256]{1,0:T(8,128)(2,1)} %refs_4_.2), custom_call_target="tpu_custom_call" | custom-call | tf_op jit(solution)/shard_map/pallas_call | solution.py:97
  2.6 0.0 copy-start.9
  2.6 8.5 %all-to-all-start = ((bf16[8,24,512]{2,1,0:T(8,128)(2,1)}), bf16[8,24,512]{2,1,0:T(8,128)(2,1)S(1)}, u32[]{:S(2)}, u32[]{:S(2)}) async-start(bf16[8,24,512]{2,1,0:T(8,128)(2,1)} %get-tuple-element.16), calls=%async_computation | async-start | bytes 393216 | tf_op jit(solution)/shard_map/all_to_all | solution.py:17
  11.1 1.5 %collective-permute-start.2 = (bf16[128,768]{1,0:T(8,128)(2,1)S(1)}, bf16[128,768]{1,0:T(8,128)(2,1)S(1)}, u32[]{:S(2)}, u32[]{:S(2)}) collective-permute-start(bf16[128,768]{1,0:T(8,128)(2,1)S(1)} %get-tuple-element.17.refs_1_), channel_id=1, source_target_pairs={{0,8},{8,16},{16,24},{24,0},{1,9},{9,17},{17,25},{25,1},{2,10},{10... | collective-permute-start | bytes 589832 | tf_op jit(solution)/shard_map/ppermute | solution.py:25
  12.6 1.1 collective-permute-start.1
  13.7 2.2 %collective-permute-start = (bf16[128,768]{1,0:T(8,128)(2,1)S(1)}, bf16[128,768]{1,0:T(8,128)(2,1)}, u32[]{:S(2)}, u32[]{:S(2)}) collective-permute-start(bf16[128,768]{1,0:T(8,128)(2,1)S(1)} %get-tuple-element.17.refs_1_), channel_id=1, source_target_pairs={{0,24},{8,0},{16,8},{24,16},{1,25},{9,1},{17,9},{25,17},{2,26},{10... | collective-permute-start | bytes 589832 | tf_op jit(solution)/shard_map/ppermute | solution.py:25
  15.8 2.3 %shard_map.222 = (bf16[8,512]{1,0:T(8,128)(2,1)S(1)}, f32[24,128]{1,0:T(8,128)S(1)}) custom-call(bf16[24,4096]{1,0:T(8,128)(2,1)} %refs_1_.2, f32[1,4096]{1,0:T(1,128)} %bitcast.32, bf16[16,4096]{1,0:T(8,128)(2,1)} %bitcast.27, bf16[16,4096]{1,0:T(8,128)(2,1)} %bitcast.28, f32[1,2]{1,0:T(1,128)} %bitcast.37, s32[2,24]{1,0:T(2,128)} %bitcast.34, ...), custom_call_target="tpu_custom_call" | custom-call | flops 100000000 | tf_op jit(solution)/shard_map/pallas_call | solution.py:97
  18.1 0.0 copy-start.10
  18.1 0.6 copy-done.10
  18.7 0.1 collective-permute-done.2.refs_4_
  18.8 3.0 %collective-permute-done.1.refs_3_ = bf16[128,768]{1,0:T(8,128)(2,1)S(1)} collective-permute-done((bf16[128,768]{1,0:T(8,128)(2,1)S(1)}, bf16[128,768]{1,0:T(8,128)(2,1)S(1)}, u32[]{:S(2)}, u32[]{:S(2)}) %collective-permute-start.1) | collective-permute-done | bytes 196640 | tf_op jit(solution)/shard_map/ppermute | solution.py:25
  21.8 0.0 copy-done.17
  21.8 0.7 copy-done.18
  22.5 1.3 collective-permute-done.refs_2_
  23.8 0.0 all-to-all-done.refs_0_
  23.8 0.0 copy-done.9
  23.8 0.7 copy-done.7
  24.5 0.9 copy-done.8
  25.4 1.7 %shard_map.223.refs_0_ = bf16[8,24,768]{2,1,0:T(8,128)(2,1)S(1)} custom-call(bf16[8,24,512]{2,1,0:T(8,128)(2,1)S(1)} %copy-done.8, bf16[128,768]{1,0:T(8,128)(2,1)} %copy-done.9, bf16[128,768]{1,0:T(8,128)(2,1)} %collective-permute-done.refs_2_, bf16[128,768]{1,0:T(8,128)(2,1)} %copy-done.18, bf16[128,768]{1,0:T(8,128)(2,1)} %copy-done.17, f32[24,128]{1,0:T(8,128)} %copy-done.10), custom_call_target="tpu_custom_call" | custom-call | flops 150994944 | tf_op jit(solution)/shard_map/pallas_call | solution.py:97
  27.1 0.0 copy-start.3
  27.1 0.0 copy-start.4
  27.1 18.9 %all_to_all.35.refs_0_ = bf16[8,24,768]{2,1,0:T(8,128)(2,1)S(1)} all-to-all(bf16[8,24,768]{2,1,0:T(8,128)(2,1)S(1)} %shard_map.223.refs_0_), channel_id=1, replica_groups=mesh['z'=8,'x'=4,'y'=4,'c'=2] {'z'}, dimensions={0} | all-to-all | bytes 589824 | tf_op jit(solution)/shard_map/all_to_all | solution.py:17
  46.1 0.0 copy-done
  46.1 2.1 %shard_map.224 = (bf16[8,24,512]{2,1,0:T(8,128)(2,1)S(1)}, f32[24,256]{1,0:T(8,128)S(1)}, f32[24,256]{1,0:T(8,128)S(1)}) custom-call(bf16[8,24,768]{2,1,0:T(8,128)(2,1)S(1)} %all_to_all.35.refs_0_, f32[24,128]{1,0:T(8,128)} %copy-done.10, f32[24,2,128,128]{3,2,1,0:T(8,128)S(1)} %copy-done, f32[1,128]{1,0:T(1,128)} %bitcast.36, bf16[256,4096]{1,0:T(8,128)(2,1)} %refs_4_.3), custom_call_target="tpu_custom_call" | custom-call | flops 50331648 | tf_op jit(solution)/shard_map/pallas_call | solution.py:97
  48.2 0.0 copy-start.11
  48.2 0.0 copy-start.12
  48.2 11.1 %all_to_all.36.refs_0_ = bf16[8,24,512]{2,1,0:T(8,128)(2,1)S(1)} all-to-all(bf16[8,24,512]{2,1,0:T(8,128)(2,1)S(1)} %get-tuple-element.19), channel_id=1, replica_groups=mesh['z'=8,'x'=4,'y'=4,'c'=2] {'y','c'}, dimensions={0} | all-to-all | bytes 393216 | tf_op jit(solution)/shard_map/all_to_all | solution.py:17
  59.3 0.0 copy-done.3
  59.3 0.0 copy-done.11
  59.3 0.0 copy-done.12
  59.3 0.0 copy-done.4
  59.3 0.7 shard_map.225
  60.0 3.4 %all-to-all-start.3 = ((bf16[8,32,512]{2,1,0:T(8,128)(2,1)}), bf16[8,32,512]{2,1,0:T(8,128)(2,1)S(1)}, u32[]{:S(2)}, u32[]{:S(2)}) async-start(bf16[8,32,512]{2,1,0:T(8,128)(2,1)} %get-tuple-element.21), calls=%async_computation.3 | async-start | bytes 524288 | tf_op jit(solution)/shard_map/all_to_all | solution.py:17
  63.5 1.1 shard_map.226.refs_2_
  64.5 0.0 copy-start.2
  64.5 0.2 collective-permute-start.5
  64.8 2.3 %collective-permute-start.4 = (bf16[768,256]{1,0:T(8,128)(2,1)S(1)}, bf16[768,256]{1,0:T(8,128)(2,1)S(1)}, u32[]{:S(2)}, u32[]{:S(2)}) collective-permute-start(bf16[768,256]{1,0:T(8,128)(2,1)S(1)} %shard_map.226.refs_2_), channel_id=1, source_target_pairs={{0,16},{8,24},{16,0},{24,8},{1,17},{9,25},{17,1},{25,9},{2,18},{10... | collective-permute-start | bytes 1179656 | tf_op jit(solution)/shard_map/ppermute | solution.py:25
  67.0 1.9 %collective-permute-start.3 = (bf16[768,256]{1,0:T(8,128)(2,1)S(1)}, bf16[768,256]{1,0:T(8,128)(2,1)S(1)}, u32[]{:S(2)}, u32[]{:S(2)}) collective-permute-start(bf16[768,256]{1,0:T(8,128)(2,1)S(1)} %shard_map.226.refs_2_), channel_id=1, source_target_pairs={{0,24},{8,0},{16,8},{24,16},{1,25},{9,1},{17,9},{25,17},{2,26},{10... | collective-permute-start | bytes 1179656 | tf_op jit(solution)/shard_map/ppermute | solution.py:25
  68.9 4.3 %shard_map.227.refs_6_ = f32[24,2,128,128]{3,2,1,0:T(8,128)} custom-call(f32[24,256]{1,0:T(8,128)} %copy-done.11, f32[24,256]{1,0:T(8,128)} %copy-done.12, f32[24,128]{1,0:T(8,128)} %copy-done.10, f32[24,2,128,128]{3,2,1,0:T(8,128)} %refs_3_.5), custom_call_target="tpu_custom_call" | custom-call | flops 100000000 | tf_op jit(solution)/shard_map/pallas_call | solution.py:97
  73.2 0.0 copy-done.2
  73.2 3.5 %collective-permute-done.5.refs_5_ = bf16[768,256]{1,0:T(8,128)(2,1)S(1)} collective-permute-done((bf16[768,256]{1,0:T(8,128)(2,1)S(1)}, bf16[768,256]{1,0:T(8,128)(2,1)S(1)}, u32[]{:S(2)}, u32[]{:S(2)}) %collective-permute-start.5) | collective-permute-done | bytes 393248 | tf_op jit(solution)/shard_map/ppermute | solution.py:25
  76.6 1.7 %collective-permute-done.4.refs_4_ = bf16[768,256]{1,0:T(8,128)(2,1)S(1)} collective-permute-done((bf16[768,256]{1,0:T(8,128)(2,1)S(1)}, bf16[768,256]{1,0:T(8,128)(2,1)S(1)}, u32[]{:S(2)}, u32[]{:S(2)}) %collective-permute-start.4) | collective-permute-done | bytes 393248 | tf_op jit(solution)/shard_map/ppermute | solution.py:25
  78.3 6.9 %collective-permute-done.3.refs_3_ = bf16[768,256]{1,0:T(8,128)(2,1)S(1)} collective-permute-done((bf16[768,256]{1,0:T(8,128)(2,1)S(1)}, bf16[768,256]{1,0:T(8,128)(2,1)S(1)}, u32[]{:S(2)}, u32[]{:S(2)}) %collective-permute-start.3) | collective-permute-done | bytes 393248 | tf_op jit(solution)/shard_map/ppermute | solution.py:25
  85.2 0.0 all-to-all-done.3.refs_0_
  85.2 0.0 copy-done.14
  85.2 0.0 copy-done.15
  85.3 0.7 copy-done.16
  86.0 2.7 %shard_map.228 = (bf16[4,4,104,256]{3,2,1,0:T(8,128)(2,1)S(1)}, f32[8,192]{1,0:T(8,128)S(1)}) custom-call(bf16[8,32,512]{2,1,0:T(8,128)(2,1)S(1)} %all-to-all-done.3.refs_0_, f32[1,4096]{1,0:T(1,128)} %bitcast.29, bf16[768,256]{1,0:T(8,128)(2,1)} %copy-done.2, bf16[768,256]{1,0:T(8,128)(2,1)} %copy-done.16, bf16[768,256]{1,0:T(8,128)(2,1)} %copy-done.15, ...), custom_call_target="tpu_custom_call" | custom-call | flops 201326592 | tf_op jit(solution)/shard_map/pallas_call | solution.py:97
  88.7 0.0 copy-start.13
  88.7 18.0 %all_to_all.37 = bf16[16,104,256]{2,1,0:T(8,128)(2,1)S(1)} all-to-all(bf16[16,104,256]{2,1,0:T(8,128)(2,1)S(1)} %bitcast.26), channel_id=1, replica_groups=mesh['z'=8,'x'=4,'y'=4,'c'=2] {'x','y'}, dimensions={0} | all-to-all | bytes 1703936 | tf_op jit(solution)/shard_map/all_to_all | solution.py:17
  106.7 0.0 collective-permute-start.6
  106.7 2.4 %collective-permute-done.6 = bf16[16,104,256]{2,1,0:T(8,128)(2,1)S(1)} collective-permute-done((bf16[16,104,256]{2,1,0:T(8,128)(2,1)S(1)}, bf16[16,104,256]{2,1,0:T(8,128)(2,1)S(1)}, u32[]{:S(2)}, u32[]{:S(2)}) %collective-permute-start.6) | collective-permute-done | bytes 852000 | tf_op jit(solution)/shard_map/ppermute | solution.py:582
  109.1 0.0 copy-done.1
  109.1 0.0 copy-done.5
  109.1 0.0 copy-done.6
  109.1 1.6 %shard_map.229 = (bf16[4,5,24,512]{3,2,1,0:T(8,128)(2,1)S(1)}, bf16[96,128]{1,0:T(8,128)(2,1)S(1)}, bf16[4,24,128]{2,1,0:T(8,128)(2,1)S(1)}) custom-call(bf16[4,4,104,256]{3,2,1,0:T(8,128)(2,1)S(1)} %bitcast.20, bf16[4,4,104,256]{3,2,1,0:T(8,128)(2,1)S(1)} %bitcast.25, f32[1,4096]{1,0:T(1,128)} %bitcast.30, bf16[4096,128]{1,0:T(8,128)(2,1)S(1)} %bitcast.23, ...), custom_call_target="tpu_custom_call" | custom-call | flops 251658240 | tf_op jit(solution)/shard_map/pallas_call | solution.py:97
  110.7 0.2 collective-permute-start.7
  110.9 1.7 %collective-permute-done.7.refs_2_ = bf16[4,5,24,512]{3,2,1,0:T(8,128)(2,1)S(1)} collective-permute-done((bf16[4,5,24,512]{3,2,1,0:T(8,128)(2,1)S(1)}, bf16[4,5,24,512]{3,2,1,0:T(8,128)(2,1)S(1)}, u32[]{:S(2)}, u32[]{:S(2)}) %collective-permute-start.7) | collective-permute-done | bytes 491552 | tf_op jit(solution)/shard_map/ppermute | solution.py:600
  112.7 0.3 shard_map.230
  112.9 16.4 %all_to_all.38 = bf16[16,24,768]{2,1,0:T(8,128)(2,1)S(1)} all-to-all(bf16[16,24,768]{2,1,0:T(8,128)(2,1)S(1)} %bitcast.22), channel_id=1, replica_groups=mesh['z'=8,'x'=4,'y'=4,'c'=2] {'x','y'}, dimensions={0} | all-to-all | bytes 1179648 | tf_op jit(solution)/shard_map/all_to_all | solution.py:17
  129.3 1.5 %shard_map.231 = bf16[8,24,512]{2,1,0:T(8,128)(2,1)S(1)} custom-call(bf16[4,4,24,768]{3,2,1,0:T(8,128)(2,1)S(1)} %bitcast.21, f32[8,192]{1,0:T(8,128)} %copy-done.13, bf16[768,256]{1,0:T(8,128)(2,1)} %copy-done.2, bf16[768,256]{1,0:T(8,128)(2,1)} %copy-done.16, bf16[768,256]{1,0:T(8,128)(2,1)} %copy-done.15, bf16[768,256]{1,0:T(8,128)(2,1)} %copy-done.14, ...), custom_call_target="tpu_custom_call" | custom-call | flops 100663296 | tf_op jit(solution)/shard_map/pallas_call | solution.py:97
  130.8 16.4 %all_to_all.39.refs_0_ = bf16[8,24,512]{2,1,0:T(8,128)(2,1)S(1)} all-to-all(bf16[8,24,512]{2,1,0:T(8,128)(2,1)S(1)} %shard_map.231), channel_id=1, replica_groups=mesh['z'=8,'x'=4,'y'=4,'c'=2] {'z'}, dimensions={0} | all-to-all | bytes 393216 | tf_op jit(solution)/shard_map/all_to_all | solution.py:17
  147.2 0.6 shard_map.232
  (11 shorter events, 0.0 us)
Async XLA Ops:
  0.6 45.4 %copy-start = (f32[24,2,128,128]{3,2,1,0:T(8,128)S(1)}, f32[24,2,128,128]{3,2,1,0:T(8,128)}, u32[]{:S(2)}) copy-start(f32[24,2,128,128]{3,2,1,0:T(8,128)} %refs_3_.5) | copy-start | bytes 9437188
  2.6 21.2 %copy-start.9 = (bf16[128,768]{1,0:T(8,128)(2,1)}, bf16[128,768]{1,0:T(8,128)(2,1)S(1)}, u32[]{:S(2)}) copy-start(bf16[128,768]{1,0:T(8,128)(2,1)S(1)} %get-tuple-element.17.refs_1_) | copy-start | bytes 589828
  2.6 21.2 %all-to-all-start = ((bf16[8,24,512]{2,1,0:T(8,128)(2,1)}), bf16[8,24,512]{2,1,0:T(8,128)(2,1)S(1)}, u32[]{:S(2)}, u32[]{:S(2)}) async-start(bf16[8,24,512]{2,1,0:T(8,128)(2,1)} %get-tuple-element.16), calls=%async_computation | async-start | bytes 393216 | tf_op jit(solution)/shard_map/all_to_all | solution.py:17
  11.1 7.8 %collective-permute-start.2 = (bf16[128,768]{1,0:T(8,128)(2,1)S(1)}, bf16[128,768]{1,0:T(8,128)(2,1)S(1)}, u32[]{:S(2)}, u32[]{:S(2)}) collective-permute-start(bf16[128,768]{1,0:T(8,128)(2,1)S(1)} %get-tuple-element.17.refs_1_), channel_id=1, source_target_pairs={{0,8},{8,16},{16,24},{24,0},{1,9},{9,17},{17,25},{25,1},{2,10},{10... | collective-permute-start | bytes 589832 | tf_op jit(solution)/shard_map/ppermute | solution.py:25
  12.6 9.3 %collective-permute-start.1 = (bf16[128,768]{1,0:T(8,128)(2,1)S(1)}, bf16[128,768]{1,0:T(8,128)(2,1)S(1)}, u32[]{:S(2)}, u32[]{:S(2)}) collective-permute-start(bf16[128,768]{1,0:T(8,128)(2,1)S(1)} %get-tuple-element.17.refs_1_), channel_id=1, source_target_pairs={{0,16},{8,24},{16,0},{24,8},{1,17},{9,25},{17,1},{25,9},{2,18},{10... | collective-permute-start | bytes 589832 | tf_op jit(solution)/shard_map/ppermute | solution.py:25
  13.7 10.1 %collective-permute-start = (bf16[128,768]{1,0:T(8,128)(2,1)S(1)}, bf16[128,768]{1,0:T(8,128)(2,1)}, u32[]{:S(2)}, u32[]{:S(2)}) collective-permute-start(bf16[128,768]{1,0:T(8,128)(2,1)S(1)} %get-tuple-element.17.refs_1_), channel_id=1, source_target_pairs={{0,24},{8,0},{16,8},{24,16},{1,25},{9,1},{17,9},{25,17},{2,26},{10... | collective-permute-start | bytes 589832 | tf_op jit(solution)/shard_map/ppermute | solution.py:25
  18.1 0.6 copy-start.10
  18.8 3.0 %copy-start.17 = (bf16[128,768]{1,0:T(8,128)(2,1)}, bf16[128,768]{1,0:T(8,128)(2,1)S(1)}, u32[]{:S(2)}) copy-start(bf16[128,768]{1,0:T(8,128)(2,1)S(1)} %collective-permute-done.2.refs_4_) | copy-start | bytes 589828
  21.8 0.7 copy-start.18
  23.8 0.7 copy-start.7
  24.5 0.9 copy-start.8
  27.1 32.2 %copy-start.3 = (bf16[8,24,768]{2,1,0:T(8,128)(2,1)}, bf16[8,24,768]{2,1,0:T(8,128)(2,1)S(1)}, u32[]{:S(2)}) copy-start(bf16[8,24,768]{2,1,0:T(8,128)(2,1)S(1)} %shard_map.223.refs_0_) | copy-start | bytes 884740
  27.1 32.2 %copy-start.4 = (bf16[24,4096]{1,0:T(8,128)(2,1)S(1)}, bf16[24,4096]{1,0:T(8,128)(2,1)}, u32[]{:S(2)}) copy-start(bf16[24,4096]{1,0:T(8,128)(2,1)} %refs_1_.2) | copy-start | bytes 589828
  48.2 11.1 %copy-start.11 = (f32[24,256]{1,0:T(8,128)}, f32[24,256]{1,0:T(8,128)S(1)}, u32[]{:S(2)}) copy-start(f32[24,256]{1,0:T(8,128)S(1)} %get-tuple-element.22.refs_0_) | copy-start | bytes 73732
  48.2 11.1 %copy-start.12 = (f32[24,256]{1,0:T(8,128)}, f32[24,256]{1,0:T(8,128)S(1)}, u32[]{:S(2)}) copy-start(f32[24,256]{1,0:T(8,128)S(1)} %get-tuple-element.23.refs_1_) | copy-start | bytes 73732
  60.0 25.2 %all-to-all-start.3 = ((bf16[8,32,512]{2,1,0:T(8,128)(2,1)}), bf16[8,32,512]{2,1,0:T(8,128)(2,1)S(1)}, u32[]{:S(2)}, u32[]{:S(2)}) async-start(bf16[8,32,512]{2,1,0:T(8,128)(2,1)} %get-tuple-element.21), calls=%async_computation.3 | async-start | bytes 524288 | tf_op jit(solution)/shard_map/all_to_all | solution.py:17
  64.5 8.6 %copy-start.2 = (bf16[768,256]{1,0:T(8,128)(2,1)}, bf16[768,256]{1,0:T(8,128)(2,1)S(1)}, u32[]{:S(2)}) copy-start(bf16[768,256]{1,0:T(8,128)(2,1)S(1)} %shard_map.226.refs_2_) | copy-start | bytes 1179652
  64.5 12.1 %collective-permute-start.5 = (bf16[768,256]{1,0:T(8,128)(2,1)S(1)}, bf16[768,256]{1,0:T(8,128)(2,1)S(1)}, u32[]{:S(2)}, u32[]{:S(2)}) collective-permute-start(bf16[768,256]{1,0:T(8,128)(2,1)S(1)} %shard_map.226.refs_2_), channel_id=1, source_target_pairs={{0,8},{8,16},{16,24},{24,0},{1,9},{9,17},{17,25},{25,1},{2,10},{10... | collective-permute-start | bytes 1179656 | tf_op jit(solution)/shard_map/ppermute | solution.py:25
  64.8 13.5 %collective-permute-start.4 = (bf16[768,256]{1,0:T(8,128)(2,1)S(1)}, bf16[768,256]{1,0:T(8,128)(2,1)S(1)}, u32[]{:S(2)}, u32[]{:S(2)}) collective-permute-start(bf16[768,256]{1,0:T(8,128)(2,1)S(1)} %shard_map.226.refs_2_), channel_id=1, source_target_pairs={{0,16},{8,24},{16,0},{24,8},{1,17},{9,25},{17,1},{25,9},{2,18},{10... | collective-permute-start | bytes 1179656 | tf_op jit(solution)/shard_map/ppermute | solution.py:25
  67.0 18.2 %collective-permute-start.3 = (bf16[768,256]{1,0:T(8,128)(2,1)S(1)}, bf16[768,256]{1,0:T(8,128)(2,1)S(1)}, u32[]{:S(2)}, u32[]{:S(2)}) collective-permute-start(bf16[768,256]{1,0:T(8,128)(2,1)S(1)} %shard_map.226.refs_2_), channel_id=1, source_target_pairs={{0,24},{8,0},{16,8},{24,16},{1,25},{9,1},{17,9},{25,17},{2,26},{10... | collective-permute-start | bytes 1179656 | tf_op jit(solution)/shard_map/ppermute | solution.py:25
  76.6 8.6 %copy-start.14 = (bf16[768,256]{1,0:T(8,128)(2,1)}, bf16[768,256]{1,0:T(8,128)(2,1)S(1)}, u32[]{:S(2)}) copy-start(bf16[768,256]{1,0:T(8,128)(2,1)S(1)} %collective-permute-done.5.refs_5_) | copy-start | bytes 1179652
  78.3 7.0 %copy-start.15 = (bf16[768,256]{1,0:T(8,128)(2,1)}, bf16[768,256]{1,0:T(8,128)(2,1)S(1)}, u32[]{:S(2)}) copy-start(bf16[768,256]{1,0:T(8,128)(2,1)S(1)} %collective-permute-done.4.refs_4_) | copy-start | bytes 1179652
  85.2 0.8 copy-start.16
  86.0 23.1 %copy-start.1 = (bf16[1,128,4096]{2,1,0:T(8,128)(2,1)S(1)}, bf16[1,128,4096]{2,1,0:T(8,128)(2,1)}, u32[]{:S(2)}) copy-start(bf16[1,128,4096]{2,1,0:T(8,128)(2,1)} %param.39) | copy-start | bytes 3145732
  86.0 23.1 %copy-start.5 = (bf16[1,4096,128]{2,1,0:T(8,128)(2,1)S(1)}, bf16[1,4096,128]{2,1,0:T(8,128)(2,1)}, u32[]{:S(2)}) copy-start(bf16[1,4096,128]{2,1,0:T(8,128)(2,1)} %param.37) | copy-start | bytes 3145732
  86.0 23.1 %copy-start.6 = (bf16[1,4096,128]{2,1,0:T(8,128)(2,1)S(1)}, bf16[1,4096,128]{2,1,0:T(8,128)(2,1)}, u32[]{:S(2)}) copy-start(bf16[1,4096,128]{2,1,0:T(8,128)(2,1)} %param.38) | copy-start | bytes 3145732
  88.7 22.0 %copy-start.13 = (f32[8,192]{1,0:T(8,128)}, f32[8,192]{1,0:T(8,128)S(1)}, u32[]{:S(2)}) copy-start(f32[8,192]{1,0:T(8,128)S(1)} %get-tuple-element.28.refs_1_) | copy-start | bytes 18436
  106.7 2.4 %collective-permute-start.6 = (bf16[16,104,256]{2,1,0:T(8,128)(2,1)S(1)}, bf16[16,104,256]{2,1,0:T(8,128)(2,1)S(1)}, u32[]{:S(2)}, u32[]{:S(2)}) collective-permute-start(bf16[16,104,256]{2,1,0:T(8,128)(2,1)S(1)} %all_to_all.37), channel_id=1, source_target_pairs={{0,1},{1,0},{2,3},{3,2},{4,5},{5,4},{6,7},{7,6},{8,9},{9,8},{10,11... | collective-permute-start | bytes 2555912 | tf_op jit(solution)/shard_map/ppermute | solution.py:582
  110.7 2.0 %collective-permute-start.7 = (bf16[4,5,24,512]{3,2,1,0:T(8,128)(2,1)S(1)}, bf16[4,5,24,512]{3,2,1,0:T(8,128)(2,1)S(1)}, u32[]{:S(2)}, u32[]{:S(2)}) collective-permute-start(bf16[4,5,24,512]{3,2,1,0:T(8,128)(2,1)S(1)} %get-tuple-element.27), channel_id=1, source_target_pairs={{0,1},{1,0},{2,3},{3,2},{4,5},{5,4},{6,7},{7,6},{8,9},{9,8},{10,11... | collective-permute-start | bytes 1474568 | tf_op jit(solution)/shard_map/ppermute | solution.py:600

commit v4 on v3

--- a/solution.py
+++ b/solution.py
@@ -109,7 +109,7 @@
     return jnp.where(value >= count, value - count, value)
 
 
-def spread_body(index, tokens, gain, query, key, value, out, weights):
+def weights_and_tokens(tokens, gain, query, key, value, out, weights):
     cols = query.shape[1]
     for place, weight in enumerate((query, key, value)):
         weights[:, place * cols : (place + 1) * cols] = weight[...]
@@ -134,9 +134,11 @@
     return jnp.sum(jnp.where(same, row, 0.0), axis=1, keepdims=True)
 
 
-def prepare_body(
-    index, tokens, gain, decay_weight, beta_weight, rate, ids, prob, logit, meta, factors
+def spread_body(
+    index, tokens, gain, query, key, value, decay_weight, beta_weight, rate, ids, prob, logit,
+    out, weights, meta, factors,
 ):
+    weights_and_tokens(tokens, gain, query, key, value, out, weights)
     rows, width = tokens.shape
     block = meta.shape[1]
     wide = tokens[...].astype(F32)
@@ -190,7 +192,7 @@
     meta[...] = jnp.dot(table.astype(BF), spot, preferred_element_type=F32).astype(BF)
 
 
-def project_body(index, arrived, w0, w1, w2, w3, after, out):
+def project_body(index, arrived, w0, w1, w2, w3, out):
     groups, rows, _ = arrived.shape
     total = None
     for step, weight in enumerate((w0, w1, w2, w3)):
@@ -241,7 +243,7 @@
         out[t] = jnp.dot(left, right, preferred_element_type=F32).astype(BF)
 
 
-def update_body(index, keys, changes, factors, state, new_state):
+def update_body(keys, changes, factors, state, new_state):
     rows, heads, size = state.shape[:3]
     line = lax.broadcasted_iota(jnp.int32, (rows, size), 0)
     line = jnp.concatenate((line, line, line), axis=0)
@@ -262,6 +264,32 @@
                 new_state[b + side, h] = fade * state[b + side, h] + grown
 
 
+def updated(keys, changes, factors, state):
+    rows, heads, size = state.shape[:3]
+    step = 8
+    flat = lambda i: (i, 0)
+    deep = lambda i: (i, 0, 0, 0)
+    args = [
+        pltpu.with_memory_space_constraint(arg, pltpu.HBM)
+        for arg in (keys, changes, factors, state)
+    ]
+    return pl.pallas_call(
+        update_body,
+        name="update_body",
+        out_shape=jax.ShapeDtypeStruct(state.shape, F32),
+        grid=(rows // step,),
+        in_specs=[
+            pl.BlockSpec((step, heads * size), flat),
+            pl.BlockSpec((step, heads * size), flat),
+            pl.BlockSpec((step, factors.shape[1]), flat),
+            pl.BlockSpec((step, heads, size, size), deep),
+        ],
+        out_specs=pl.BlockSpec((step, heads, size, size), deep),
+        cost_estimate=pl.CostEstimate(flops=10**8, bytes_accessed=0, transcendentals=0),
+        compiler_params=pltpu.CompilerParams(vmem_limit_bytes=16 * MIB),
+    )(*args)
+
+
 def middle_body(index, arrived, tokens, meta, middle, out):
     block = middle.shape[1]
     rows = middle.shape[0]
@@ -294,7 +322,7 @@
     return slots
 
 
-def dispatch_body(index, arrived, gain, g0, g1, g2, g3, after, out, route):
+def dispatch_body(index, arrived, gain, g0, g1, g2, g3, out, route):
     rows = arrived.shape[1] - 8
     tokens = NZ * rows
     block = arrived.shape[2]
@@ -477,53 +505,48 @@
         place = pl.multiple_of(index[2] * block, block)
         return ref.at[:, pl.ds(place, block)]
 
-    message, own_weights = kernel(
+    message, own_weights, meta, factors = kernel(
         spread_body,
-        (pltpu.HBM((NZ, rows, block), BF), shape(query_weight.shape[0], 3 * cols)),
+        (
+            pltpu.HBM((NZ, rows, block), BF),
+            shape(query_weight.shape[0], 3 * cols),
+            shape(8, block),
+            shape(rows, 128, dtype=F32),
+        ),
         tokens,
         attn_gain[None],
         query_weight,
         key_weight,
         value_weight,
-        far=range(5),
-    )
-    qkv_weights = from_neighbours(own_weights, "x")
-    spread = exchange(message, "z")
-    meta, factors = kernel(
-        prepare_body,
-        (shape(8, block), shape(rows, 128, dtype=F32)),
-        tokens,
-        attn_gain[None],
         decay_weight.T,
         beta_weight.T,
         decay_rate[None],
         expert_ids.T,
         group_prob[None],
         expert_logit.T,
-        far=range(8),
-        flops=10**8,
-    )
+        far=range(11),
+    )
+    qkv_weights = from_neighbours(own_weights, "x")
+    spread = exchange(message, "z")
+    (packed,) = kernel(
+        pack_body,
+        (shape(block + dense_gate.shape[1] * 2, half),),
+        message,
+        dense_gate,
+        dense_up,
+        dense_down,
+        plain=(0,),
+        far=(1, 2, 3),
+    )
+    dense_weights = from_neighbours(packed, "x")
     (part,) = kernel(
         project_body,
         (shape(NZ, rows, 3 * cols),),
         spread,
         *qkv_weights,
-        factors,
         held=(1, 2, 3, 4),
-        plain=(5,),
         flops=2 * NZ * rows * block * 3 * cols,
     )
-    (packed,) = kernel(
-        pack_body,
-        (shape(block + dense_gate.shape[1] * 2, half),),
-        part,
-        dense_gate,
-        dense_up,
-        dense_down,
-        plain=(0,),
-        far=(1, 2, 3),
-    )
-    dense_weights = from_neighbours(packed, "x")
     arrived = exchange(part, "z")
     attn_part, keys, changes = kernel(
         recall_body,
@@ -540,17 +563,7 @@
         far=(1, 3, 4),
         flops=2 * rows * cols * width,
     )
-    (new_state,) = kernel(
-        update_body,
-        (shape(*delta_state.shape, dtype=F32),),
-        keys,
-        changes,
-        factors,
-        delta_state,
-        far=range(4),
-        flops=10**8,
-        limit=24,
-    )
+    new_state = updated(keys, changes, factors, delta_state)
     arrived = exchange(attn_part, ("y", "c"))
     middle, message = kernel(
         middle_body,
@@ -568,9 +581,7 @@
         arrived,
         ffn_gain[None],
         *dense_weights,
-        new_state,
         far=range(1, 6),
-        plain=(6,),
         parts={
             1: ((1, block), own_block),
             **{n: ((block, half), lambda ref, index: ref.at[:block]) for n in range(2, 6)},

time: 149 us -> 154 us (1.034)
  blocking collectives: 80.9 us -> 64.4 us
  waiting for transfers between devices: 20.6 us -> 32.3 us
  starting transfers between devices: 21.2 us -> 28.7 us
    all_to_all x5 -> x4, blocking collectives: 80.9 us -> 64.4 us  [exchange(): return lax.all_to_all(tiles, axes, split_axis=0, concat_axis=0, tiled=True)]
    all_to_all x2 -> x3, starting transfers between devices: 11.9 us -> 19.3 us  [exchange(): return lax.all_to_all(tiles, axes, split_axis=0, concat_axis=0, tiled=True)]
    ppermute x6, waiting for transfers between devices: 16.5 us -> 23.4 us  [from_neighbours(): parts.append(lax.ppermute(shard, axis, pairs))]
    pallas_call x0 -> x1, Pallas kernels: none -> 4.99 us  [updated(): pl.pallas_call(update_body, name='update_body', out_shape=jax.ShapeDtypeS...]
    all_to_all x2 -> x3, waiting for transfers between devices: 0.01 us -> 4.79 us  [exchange(): return lax.all_to_all(tiles, axes, split_axis=0, concat_axis=0, tiled=True)]
    pallas_call x12 -> x10, Pallas kernels: 20.7 us -> 16.5 us  [kernel(): pl.pallas_call(run, out_shape=outs, in_specs=specs, out_specs=out_specs,...]
    unnamed x38 -> x36, local copies, waits for them, and re-layouts: 3.66 us -> 5.13 us
  transfers between devices with their start and end apart: 10 -> 11, of which waited for: 8 -> 9; matrix products, arithmetic and copies ran while one was open for 0% -> 0% of each run, Pallas kernels for 5% -> 4%
where the time goes in v4:
time: 154 us; the launch traced here: 153 us
  blocking collectives  64.4 us (42%)
  waiting for transfers between devices  32.3 us (21%)
  starting transfers between devices  28.7 us (19%)
  Pallas kernels  21.5 us (14%)
  local copies, waits for them, and re-layouts  5.13 us (3%)
    all_to_all x4, blocking collectives, exchange(): return lax.all_to_all(tiles, axes, split_axis=0, concat_axis=0, tiled=True)  64.4 us
    ppermute x6, waiting for transfers between devices, from_neighbours(): parts.append(lax.ppermute(shard, axis, pairs))  23.4 us
    all_to_all x3, starting transfers between devices, exchange(): return lax.all_to_all(tiles, axes, split_axis=0, concat_axis=0, tiled=True)  19.3 us
    pallas_call x10, Pallas kernels, kernel(): pl.pallas_call(run, out_shape=outs, in_specs=specs, out_specs=out_specs,...  16.5 us
    ppermute x6, starting transfers between devices, from_neighbours(): parts.append(lax.ppermute(shard, axis, pairs))  9.09 us
    unnamed x36, local copies, waits for them, and re-layouts  5.13 us
    pallas_call x1, Pallas kernels, updated(): pl.pallas_call(update_body, name='update_body', out_shape=jax.ShapeDtypeS...  4.99 us
    all_to_all x3, waiting for transfers between devices, exchange(): return lax.all_to_all(tiles, axes, split_axis=0, concat_axis=0, tiled=True)  4.79 us
  transfers between devices with their start and end apart: 11, of which 9 were waited for; matrix products, arithmetic and copies ran while one was open for 0% of the time, Pallas kernels for 4%

profile of v4, /device:TPU:2, one launch (start us, length us, event | category | flops | bytes accessed | tf_op | source)
XLA Modules:
  0.0 152.9 jit_solution(13106997408540916623)
XLA Ops:
  0.6 2.9 %shard_map.221 = (bf16[8,24,512]{2,1,0:T(8,128)(2,1)}, bf16[128,768]{1,0:T(8,128)(2,1)S(1)}, bf16[8,512]{1,0:T(8,128)(2,1)S(1)}, f32[24,128]{1,0:T(8,128)S(1)}) custom-call(bf16[24,4096]{1,0:T(8,128)(2,1)} %refs_1_.2, f32[1,4096]{1,0:T(1,128)} %bitcast.31, bf16[128,256]{1,0:T(8,128)(2,1)} %refs_2_.3, bf16[128,256]{1,0:T(8,128)(2,1)} %refs_3_.2, ...), custom_call_target="tpu_custom_call" | custom-call | tf_op jit(solution)/shard_map/pallas_call | solution.py:97
  3.5 0.0 copy-start.9
  3.5 0.6 copy-done.9
  4.1 8.5 %all-to-all-start = ((bf16[8,24,512]{2,1,0:T(8,128)(2,1)}), bf16[8,24,512]{2,1,0:T(8,128)(2,1)S(1)}, u32[]{:S(2)}, u32[]{:S(2)}) async-start(bf16[8,24,512]{2,1,0:T(8,128)(2,1)} %get-tuple-element.16.refs_0_), calls=%async_computation | async-start | bytes 393216 | tf_op jit(solution)/shard_map/all_to_all | solution.py:17
  12.6 1.5 collective-permute-start.2
  14.1 1.1 collective-permute-start.1
  15.2 2.2 %collective-permute-start = (bf16[128,768]{1,0:T(8,128)(2,1)S(1)}, bf16[128,768]{1,0:T(8,128)(2,1)S(1)}, u32[]{:S(2)}, u32[]{:S(2)}) collective-permute-start(bf16[128,768]{1,0:T(8,128)(2,1)S(1)} %get-tuple-element.17.refs_1_), channel_id=1, source_target_pairs={{0,24},{8,0},{16,8},{24,16},{1,25},{9,1},{17,9},{25,17},{2,26},{10... | collective-permute-start | bytes 589832 | tf_op jit(solution)/shard_map/ppermute | solution.py:25
  17.4 3.0 %collective-permute-done.2.refs_4_ = bf16[128,768]{1,0:T(8,128)(2,1)S(1)} collective-permute-done((bf16[128,768]{1,0:T(8,128)(2,1)S(1)}, bf16[128,768]{1,0:T(8,128)(2,1)S(1)}, u32[]{:S(2)}, u32[]{:S(2)}) %collective-permute-start.2) | collective-permute-done | bytes 196640 | tf_op jit(solution)/shard_map/ppermute | solution.py:25
  20.4 3.0 %collective-permute-done.1.refs_3_ = bf16[128,768]{1,0:T(8,128)(2,1)S(1)} collective-permute-done((bf16[128,768]{1,0:T(8,128)(2,1)S(1)}, bf16[128,768]{1,0:T(8,128)(2,1)S(1)}, u32[]{:S(2)}, u32[]{:S(2)}) %collective-permute-start.1) | collective-permute-done | bytes 196640 | tf_op jit(solution)/shard_map/ppermute | solution.py:25
  23.4 1.8 %collective-permute-done.refs_2_ = bf16[128,768]{1,0:T(8,128)(2,1)S(1)} collective-permute-done((bf16[128,768]{1,0:T(8,128)(2,1)S(1)}, bf16[128,768]{1,0:T(8,128)(2,1)S(1)}, u32[]{:S(2)}, u32[]{:S(2)}) %collective-permute-start) | collective-permute-done | bytes 196640 | tf_op jit(solution)/shard_map/ppermute | solution.py:25
  25.2 0.0 all-to-all-done.refs_0_
  25.2 0.0 copy-done.6
  25.2 0.0 copy-done.15
  25.2 0.0 copy-done.16
  25.3 0.6 copy-done.17
  25.9 1.7 %shard_map.222 = bf16[8,24,768]{2,1,0:T(8,128)(2,1)S(1)} custom-call(bf16[8,24,512]{2,1,0:T(8,128)(2,1)S(1)} %all-to-all-done.refs_0_, bf16[128,768]{1,0:T(8,128)(2,1)} %copy-done.6, bf16[128,768]{1,0:T(8,128)(2,1)} %copy-done.17, bf16[128,768]{1,0:T(8,128)(2,1)} %copy-done.16, bf16[128,768]{1,0:T(8,128)(2,1)} %copy-done.15), custom_call_target="tpu_custom_call" | custom-call | flops 150994944 | tf_op jit(solution)/shard_map/pallas_call | solution.py:97
  27.6 0.0 copy-start.5
  27.6 18.9 %all_to_all.35.refs_0_ = bf16[8,24,768]{2,1,0:T(8,128)(2,1)S(1)} all-to-all(bf16[8,24,768]{2,1,0:T(8,128)(2,1)S(1)} %shard_map.222), channel_id=1, replica_groups=mesh['z'=8,'x'=4,'y'=4,'c'=2] {'z'}, dimensions={0} | all-to-all | bytes 589824 | tf_op jit(solution)/shard_map/all_to_all | solution.py:17
  46.5 1.9 %copy-done = f32[24,2,128,128]{3,2,1,0:T(8,128)S(1)} copy-done((f32[24,2,128,128]{3,2,1,0:T(8,128)S(1)}, f32[24,2,128,128]{3,2,1,0:T(8,128)}, u32[]{:S(2)}) %copy-start) | copy-done | bytes 3145752
  48.4 2.1 %shard_map.223 = (bf16[8,24,512]{2,1,0:T(8,128)(2,1)S(1)}, f32[24,256]{1,0:T(8,128)S(1)}, f32[24,256]{1,0:T(8,128)S(1)}) custom-call(bf16[8,24,768]{2,1,0:T(8,128)(2,1)S(1)} %all_to_all.35.refs_0_, f32[24,128]{1,0:T(8,128)} %copy-done.9, f32[24,2,128,128]{3,2,1,0:T(8,128)S(1)} %copy-done, f32[1,128]{1,0:T(1,128)} %bitcast.35, bf16[256,4096]{1,0:T(8,128)(2,1)} %refs_4_.3), custom_call_target="tpu_custom_call" | custom-call | flops 50331648 | tf_op jit(solution)/shard_map/pallas_call | solution.py:97
  50.6 0.0 copy-start.10
  50.6 0.0 copy-start.11
  50.6 0.0 copy-start.1
  50.6 0.0 copy-start.3
  50.6 0.0 copy-start.4
  50.6 11.3 %all_to_all.36.refs_0_ = bf16[8,24,512]{2,1,0:T(8,128)(2,1)S(1)} all-to-all(bf16[8,24,512]{2,1,0:T(8,128)(2,1)S(1)} %get-tuple-element.19), channel_id=1, replica_groups=mesh['z'=8,'x'=4,'y'=4,'c'=2] {'y','c'}, dimensions={0} | all-to-all | bytes 393216 | tf_op jit(solution)/shard_map/all_to_all | solution.py:17
  61.9 0.0 copy-done.5
  61.9 0.8 shard_map.224
  62.7 0.0 copy-done.10
  62.7 0.0 copy-done.11
  62.7 0.6 copy-done.7
  63.3 4.1 %all-to-all-start.3 = ((bf16[8,32,512]{2,1,0:T(8,128)(2,1)}), bf16[8,32,512]{2,1,0:T(8,128)(2,1)}, u32[]{:S(2)}, u32[]{:S(2)}) async-start(bf16[8,32,512]{2,1,0:T(8,128)(2,1)} %get-tuple-element.21), calls=%async_computation.3 | async-start | bytes 524288 | tf_op jit(solution)/shard_map/all_to_all | solution.py:17
  67.4 1.1 shard_map.225.refs_2_
  68.5 0.0 copy-start.2
  68.5 0.2 collective-permute-start.5
  68.7 1.8 %collective-permute-start.4 = (bf16[768,256]{1,0:T(8,128)(2,1)S(1)}, bf16[768,256]{1,0:T(8,128)(2,1)S(1)}, u32[]{:S(2)}, u32[]{:S(2)}) collective-permute-start(bf16[768,256]{1,0:T(8,128)(2,1)S(1)} %shard_map.225.refs_2_), channel_id=1, source_target_pairs={{0,16},{8,24},{16,0},{24,8},{1,17},{9,25},{17,1},{25,9},{2,18},{10... | collective-permute-start | bytes 1179656 | tf_op jit(solution)/shard_map/ppermute | solution.py:25
  70.4 2.4 %collective-permute-start.3 = (bf16[768,256]{1,0:T(8,128)(2,1)S(1)}, bf16[768,256]{1,0:T(8,128)(2,1)}, u32[]{:S(2)}, u32[]{:S(2)}) collective-permute-start(bf16[768,256]{1,0:T(8,128)(2,1)S(1)} %shard_map.225.refs_2_), channel_id=1, source_target_pairs={{0,24},{8,0},{16,8},{24,16},{1,25},{9,1},{17,9},{25,17},{2,26},{10... | collective-permute-start | bytes 1179656 | tf_op jit(solution)/shard_map/ppermute | solution.py:25
  72.8 7.7 %collective-permute-done.5.refs_5_ = bf16[768,256]{1,0:T(8,128)(2,1)S(1)} collective-permute-done((bf16[768,256]{1,0:T(8,128)(2,1)S(1)}, bf16[768,256]{1,0:T(8,128)(2,1)S(1)}, u32[]{:S(2)}, u32[]{:S(2)}) %collective-permute-start.5) | collective-permute-done | bytes 393248 | tf_op jit(solution)/shard_map/ppermute | solution.py:25
  80.5 1.6 %collective-permute-done.4.refs_4_ = bf16[768,256]{1,0:T(8,128)(2,1)S(1)} collective-permute-done((bf16[768,256]{1,0:T(8,128)(2,1)S(1)}, bf16[768,256]{1,0:T(8,128)(2,1)S(1)}, u32[]{:S(2)}, u32[]{:S(2)}) %collective-permute-start.4) | collective-permute-done | bytes 393248 | tf_op jit(solution)/shard_map/ppermute | solution.py:25
  82.2 0.0 copy-done.13
  82.2 0.7 copy-done.14
  82.9 6.2 %collective-permute-done.3.refs_3_ = bf16[768,256]{1,0:T(8,128)(2,1)} collective-permute-done((bf16[768,256]{1,0:T(8,128)(2,1)S(1)}, bf16[768,256]{1,0:T(8,128)(2,1)}, u32[]{:S(2)}, u32[]{:S(2)}) %collective-permute-start.3) | collective-permute-done | bytes 393248 | tf_op jit(solution)/shard_map/ppermute | solution.py:25
  89.1 0.0 all-to-all-done.3.refs_0_
  89.1 0.0 copy-done.2
  89.1 3.4 %shard_map.226 = (bf16[4,4,104,256]{3,2,1,0:T(8,128)(2,1)S(1)}, f32[8,192]{1,0:T(8,128)S(1)}) custom-call(bf16[8,32,512]{2,1,0:T(8,128)(2,1)} %all-to-all-done.3.refs_0_, f32[1,4096]{1,0:T(1,128)} %bitcast.29, bf16[768,256]{1,0:T(8,128)(2,1)} %copy-done.2, bf16[768,256]{1,0:T(8,128)(2,1)} %collective-permute-done.3.refs_3_, bf16[768,256]{1,0:T(8,128)(2,1)} %copy-done.14, ...), custom_call_target="tpu_custom_call" | custom-call | flops 201326592 | tf_op jit(solution)/shard_map/pallas_call | solution.py:97
  92.5 0.0 copy-start.12
  92.5 0.6 copy-done.12
  93.1 17.8 %all_to_all.37 = bf16[16,104,256]{2,1,0:T(8,128)(2,1)S(1)} all-to-all(bf16[16,104,256]{2,1,0:T(8,128)(2,1)S(1)} %bitcast.26), channel_id=1, replica_groups=mesh['z'=8,'x'=4,'y'=4,'c'=2] {'x','y'}, dimensions={0} | all-to-all | bytes 1703936 | tf_op jit(solution)/shard_map/all_to_all | solution.py:17
  110.9 0.0 collective-permute-start.6
  110.9 2.4 %collective-permute-done.6 = bf16[16,104,256]{2,1,0:T(8,128)(2,1)S(1)} collective-permute-done((bf16[16,104,256]{2,1,0:T(8,128)(2,1)S(1)}, bf16[16,104,256]{2,1,0:T(8,128)(2,1)S(1)}, u32[]{:S(2)}, u32[]{:S(2)}) %collective-permute-start.6) | collective-permute-done | bytes 852000 | tf_op jit(solution)/shard_map/ppermute | solution.py:593
  113.3 0.0 copy-done.1
  113.3 0.0 copy-done.3
  113.3 0.0 copy-done.4
  113.3 1.6 %shard_map.227 = (bf16[4,5,24,512]{3,2,1,0:T(8,128)(2,1)S(1)}, bf16[96,128]{1,0:T(8,128)(2,1)S(1)}, bf16[4,24,128]{2,1,0:T(8,128)(2,1)S(1)}) custom-call(bf16[4,4,104,256]{3,2,1,0:T(8,128)(2,1)S(1)} %bitcast.20, bf16[4,4,104,256]{3,2,1,0:T(8,128)(2,1)S(1)} %bitcast.25, f32[1,4096]{1,0:T(1,128)} %bitcast.30, bf16[4096,128]{1,0:T(8,128)(2,1)S(1)} %bitcast.23, ...), custom_call_target="tpu_custom_call" | custom-call | flops 251658240 | tf_op jit(solution)/shard_map/pallas_call | solution.py:97
  114.8 0.2 collective-permute-start.7
  115.1 1.7 %collective-permute-done.7.refs_2_ = bf16[4,5,24,512]{3,2,1,0:T(8,128)(2,1)S(1)} collective-permute-done((bf16[4,5,24,512]{3,2,1,0:T(8,128)(2,1)S(1)}, bf16[4,5,24,512]{3,2,1,0:T(8,128)(2,1)S(1)}, u32[]{:S(2)}, u32[]{:S(2)}) %collective-permute-start.7) | collective-permute-done | bytes 491552 | tf_op jit(solution)/shard_map/ppermute | solution.py:611
  116.8 0.3 shard_map.228
  117.1 16.4 %all_to_all.38 = bf16[16,24,768]{2,1,0:T(8,128)(2,1)S(1)} all-to-all(bf16[16,24,768]{2,1,0:T(8,128)(2,1)S(1)} %bitcast.22), channel_id=1, replica_groups=mesh['z'=8,'x'=4,'y'=4,'c'=2] {'x','y'}, dimensions={0} | all-to-all | bytes 1179648 | tf_op jit(solution)/shard_map/all_to_all | solution.py:17
  133.5 2.2 %shard_map.229 = bf16[8,24,512]{2,1,0:T(8,128)(2,1)} custom-call(bf16[4,4,24,768]{3,2,1,0:T(8,128)(2,1)S(1)} %bitcast.21, f32[8,192]{1,0:T(8,128)} %copy-done.12, bf16[768,256]{1,0:T(8,128)(2,1)} %copy-done.2, bf16[768,256]{1,0:T(8,128)(2,1)} %collective-permute-done.3.refs_3_, bf16[768,256]{1,0:T(8,128)(2,1)} %copy-done.14, bf16[768,256]{1,0:T(8,128)(2,1)} %copy-done.13, ...), custom_call_target="tpu_custom_call" | custom-call | flops 100663296 | tf_op jit(solution)/shard_map/pallas_call | solution.py:97
  135.6 6.8 %all-to-all-start.6 = ((bf16[8,24,512]{2,1,0:T(8,128)(2,1)}), bf16[8,24,512]{2,1,0:T(8,128)(2,1)S(1)}, u32[]{:S(2)}, u32[]{:S(2)}) async-start(bf16[8,24,512]{2,1,0:T(8,128)(2,1)} %shard_map.229), calls=%async_computation.6 | async-start | bytes 393216 | tf_op jit(solution)/shard_map/all_to_all | solution.py:17
  142.5 5.0 %update_body.1 = f32[24,2,128,128]{3,2,1,0:T(8,128)} custom-call(f32[24,256]{1,0:T(8,128)} %copy-done.10, f32[24,256]{1,0:T(8,128)} %copy-done.11, f32[24,128]{1,0:T(8,128)} %copy-done.9, f32[24,2,128,128]{3,2,1,0:T(8,128)} %state.1), custom_call_target="tpu_custom_call" | custom-call | flops 100000000 | tf_op jit(solution)/shard_map/update_body/pallas_call | solution.py:276
  147.5 4.8 %all-to-all-done.6.refs_0_ = bf16[8,24,512]{2,1,0:T(8,128)(2,1)S(1)} async-done(((bf16[8,24,512]{2,1,0:T(8,128)(2,1)}), bf16[8,24,512]{2,1,0:T(8,128)(2,1)S(1)}, u32[]{:S(2)}, u32[]{:S(2)}) %all-to-all-start.6) | async-done | bytes 196640 | tf_op jit(solution)/shard_map/all_to_all | solution.py:17
  152.2 0.0 copy-done.8
  152.2 0.6 shard_map.230
  (9 shorter events, 0.0 us)
Async XLA Ops:
  3.5 0.6 copy-start.9
  4.1 21.1 %copy-start.6 = (bf16[128,768]{1,0:T(8,128)(2,1)}, bf16[128,768]{1,0:T(8,128)(2,1)S(1)}, u32[]{:S(2)}) copy-start(bf16[128,768]{1,0:T(8,128)(2,1)S(1)} %get-tuple-element.17.refs_1_) | copy-start | bytes 589828
  4.1 21.1 %all-to-all-start = ((bf16[8,24,512]{2,1,0:T(8,128)(2,1)}), bf16[8,24,512]{2,1,0:T(8,128)(2,1)S(1)}, u32[]{:S(2)}, u32[]{:S(2)}) async-start(bf16[8,24,512]{2,1,0:T(8,128)(2,1)} %get-tuple-element.16.refs_0_), calls=%async_computation | async-start | bytes 393216 | tf_op jit(solution)/shard_map/all_to_all | solution.py:17
  12.6 7.8 %collective-permute-start.2 = (bf16[128,768]{1,0:T(8,128)(2,1)S(1)}, bf16[128,768]{1,0:T(8,128)(2,1)S(1)}, u32[]{:S(2)}, u32[]{:S(2)}) collective-permute-start(bf16[128,768]{1,0:T(8,128)(2,1)S(1)} %get-tuple-element.17.refs_1_), channel_id=1, source_target_pairs={{0,8},{8,16},{16,24},{24,0},{1,9},{9,17},{17,25},{25,1},{2,10},{10... | collective-permute-start | bytes 589832 | tf_op jit(solution)/shard_map/ppermute | solution.py:25
  14.1 9.3 %collective-permute-start.1 = (bf16[128,768]{1,0:T(8,128)(2,1)S(1)}, bf16[128,768]{1,0:T(8,128)(2,1)S(1)}, u32[]{:S(2)}, u32[]{:S(2)}) collective-permute-start(bf16[128,768]{1,0:T(8,128)(2,1)S(1)} %get-tuple-element.17.refs_1_), channel_id=1, source_target_pairs={{0,16},{8,24},{16,0},{24,8},{1,17},{9,25},{17,1},{25,9},{2,18},{10... | collective-permute-start | bytes 589832 | tf_op jit(solution)/shard_map/ppermute | solution.py:25
  15.2 10.0 %collective-permute-start = (bf16[128,768]{1,0:T(8,128)(2,1)S(1)}, bf16[128,768]{1,0:T(8,128)(2,1)S(1)}, u32[]{:S(2)}, u32[]{:S(2)}) collective-permute-start(bf16[128,768]{1,0:T(8,128)(2,1)S(1)} %get-tuple-element.17.refs_1_), channel_id=1, source_target_pairs={{0,24},{8,0},{16,8},{24,16},{1,25},{9,1},{17,9},{25,17},{2,26},{10... | collective-permute-start | bytes 589832 | tf_op jit(solution)/shard_map/ppermute | solution.py:25
  20.4 4.9 %copy-start.15 = (bf16[128,768]{1,0:T(8,128)(2,1)}, bf16[128,768]{1,0:T(8,128)(2,1)S(1)}, u32[]{:S(2)}) copy-start(bf16[128,768]{1,0:T(8,128)(2,1)S(1)} %collective-permute-done.2.refs_4_) | copy-start | bytes 589828
  23.4 1.9 %copy-start.16 = (bf16[128,768]{1,0:T(8,128)(2,1)}, bf16[128,768]{1,0:T(8,128)(2,1)S(1)}, u32[]{:S(2)}) copy-start(bf16[128,768]{1,0:T(8,128)(2,1)S(1)} %collective-permute-done.1.refs_3_) | copy-start | bytes 589828
  25.2 0.7 copy-start.17
  27.6 34.4 %copy-start.5 = (bf16[24,4096]{1,0:T(8,128)(2,1)S(1)}, bf16[24,4096]{1,0:T(8,128)(2,1)}, u32[]{:S(2)}) copy-start(bf16[24,4096]{1,0:T(8,128)(2,1)} %refs_1_.2) | copy-start | bytes 589828
  46.5 1.9 %copy-start = (f32[24,2,128,128]{3,2,1,0:T(8,128)S(1)}, f32[24,2,128,128]{3,2,1,0:T(8,128)}, u32[]{:S(2)}) copy-start(f32[24,2,128,128]{3,2,1,0:T(8,128)} %state.1) | copy-start | bytes 9437188
  50.6 12.1 %copy-start.10 = (f32[24,256]{1,0:T(8,128)}, f32[24,256]{1,0:T(8,128)S(1)}, u32[]{:S(2)}) copy-start(f32[24,256]{1,0:T(8,128)S(1)} %get-tuple-element.28.keys) | copy-start | bytes 73732
  50.6 12.1 %copy-start.11 = (f32[24,256]{1,0:T(8,128)}, f32[24,256]{1,0:T(8,128)S(1)}, u32[]{:S(2)}) copy-start(f32[24,256]{1,0:T(8,128)S(1)} %get-tuple-element.29.changes) | copy-start | bytes 73732
  50.6 62.7 %copy-start.1 = (bf16[1,128,4096]{2,1,0:T(8,128)(2,1)S(1)}, bf16[1,128,4096]{2,1,0:T(8,128)(2,1)}, u32[]{:S(2)}) copy-start(bf16[1,128,4096]{2,1,0:T(8,128)(2,1)} %param.39) | copy-start | bytes 3145732
  50.6 62.7 %copy-start.3 = (bf16[1,4096,128]{2,1,0:T(8,128)(2,1)S(1)}, bf16[1,4096,128]{2,1,0:T(8,128)(2,1)}, u32[]{:S(2)}) copy-start(bf16[1,4096,128]{2,1,0:T(8,128)(2,1)} %param.37) | copy-start | bytes 3145732
  50.6 62.7 %copy-start.4 = (bf16[1,4096,128]{2,1,0:T(8,128)(2,1)S(1)}, bf16[1,4096,128]{2,1,0:T(8,128)(2,1)}, u32[]{:S(2)}) copy-start(bf16[1,4096,128]{2,1,0:T(8,128)(2,1)} %param.38) | copy-start | bytes 3145732
  62.7 0.6 copy-start.7
  63.3 25.8 %all-to-all-start.3 = ((bf16[8,32,512]{2,1,0:T(8,128)(2,1)}), bf16[8,32,512]{2,1,0:T(8,128)(2,1)}, u32[]{:S(2)}, u32[]{:S(2)}) async-start(bf16[8,32,512]{2,1,0:T(8,128)(2,1)} %get-tuple-element.21), calls=%async_computation.3 | async-start | bytes 524288 | tf_op jit(solution)/shard_map/all_to_all | solution.py:17
  68.5 20.7 %copy-start.2 = (bf16[768,256]{1,0:T(8,128)(2,1)}, bf16[768,256]{1,0:T(8,128)(2,1)S(1)}, u32[]{:S(2)}) copy-start(bf16[768,256]{1,0:T(8,128)(2,1)S(1)} %shard_map.225.refs_2_) | copy-start | bytes 1179652
  68.5 12.1 %collective-permute-start.5 = (bf16[768,256]{1,0:T(8,128)(2,1)S(1)}, bf16[768,256]{1,0:T(8,128)(2,1)S(1)}, u32[]{:S(2)}, u32[]{:S(2)}) collective-permute-start(bf16[768,256]{1,0:T(8,128)(2,1)S(1)} %shard_map.225.refs_2_), channel_id=1, source_target_pairs={{0,8},{8,16},{16,24},{24,0},{1,9},{9,17},{17,25},{25,1},{2,10},{10... | collective-permute-start | bytes 1179656 | tf_op jit(solution)/shard_map/ppermute | solution.py:25
  68.7 13.5 %collective-permute-start.4 = (bf16[768,256]{1,0:T(8,128)(2,1)S(1)}, bf16[768,256]{1,0:T(8,128)(2,1)S(1)}, u32[]{:S(2)}, u32[]{:S(2)}) collective-permute-start(bf16[768,256]{1,0:T(8,128)(2,1)S(1)} %shard_map.225.refs_2_), channel_id=1, source_target_pairs={{0,16},{8,24},{16,0},{24,8},{1,17},{9,25},{17,1},{25,9},{2,18},{10... | collective-permute-start | bytes 1179656 | tf_op jit(solution)/shard_map/ppermute | solution.py:25
  70.4 18.7 %collective-permute-start.3 = (bf16[768,256]{1,0:T(8,128)(2,1)S(1)}, bf16[768,256]{1,0:T(8,128)(2,1)}, u32[]{:S(2)}, u32[]{:S(2)}) collective-permute-start(bf16[768,256]{1,0:T(8,128)(2,1)S(1)} %shard_map.225.refs_2_), channel_id=1, source_target_pairs={{0,24},{8,0},{16,8},{24,16},{1,25},{9,1},{17,9},{25,17},{2,26},{10... | collective-permute-start | bytes 1179656 | tf_op jit(solution)/shard_map/ppermute | solution.py:25
  80.5 1.6 %copy-start.13 = (bf16[768,256]{1,0:T(8,128)(2,1)}, bf16[768,256]{1,0:T(8,128)(2,1)S(1)}, u32[]{:S(2)}) copy-start(bf16[768,256]{1,0:T(8,128)(2,1)S(1)} %collective-permute-done.5.refs_5_) | copy-start | bytes 1179652
  82.2 0.8 copy-start.14
  92.5 0.6 copy-start.12
  110.9 2.4 %collective-permute-start.6 = (bf16[16,104,256]{2,1,0:T(8,128)(2,1)S(1)}, bf16[16,104,256]{2,1,0:T(8,128)(2,1)S(1)}, u32[]{:S(2)}, u32[]{:S(2)}) collective-permute-start(bf16[16,104,256]{2,1,0:T(8,128)(2,1)S(1)} %all_to_all.37), channel_id=1, source_target_pairs={{0,1},{1,0},{2,3},{3,2},{4,5},{5,4},{6,7},{7,6},{8,9},{9,8},{10,11... | collective-permute-start | bytes 2555912 | tf_op jit(solution)/shard_map/ppermute | solution.py:593
  114.8 2.0 %collective-permute-start.7 = (bf16[4,5,24,512]{3,2,1,0:T(8,128)(2,1)S(1)}, bf16[4,5,24,512]{3,2,1,0:T(8,128)(2,1)S(1)}, u32[]{:S(2)}, u32[]{:S(2)}) collective-permute-start(bf16[4,5,24,512]{3,2,1,0:T(8,128)(2,1)S(1)} %get-tuple-element.25), channel_id=1, source_target_pairs={{0,1},{1,0},{2,3},{3,2},{4,5},{5,4},{6,7},{7,6},{8,9},{9,8},{10,11... | collective-permute-start | bytes 1474568 | tf_op jit(solution)/shard_map/ppermute | solution.py:611
  135.6 16.6 %all-to-all-start.6 = ((bf16[8,24,512]{2,1,0:T(8,128)(2,1)}), bf16[8,24,512]{2,1,0:T(8,128)(2,1)S(1)}, u32[]{:S(2)}, u32[]{:S(2)}) async-start(bf16[8,24,512]{2,1,0:T(8,128)(2,1)} %shard_map.229), calls=%async_computation.6 | async-start | bytes 393216 | tf_op jit(solution)/shard_map/all_to_all | solution.py:17
  142.5 9.8 %copy-start.8 = (f32[24,512]{1,0:T(8,128)S(1)}, f32[24,512]{1,0:T(8,128)}, u32[]{:S(2)}) copy-start(f32[24,512]{1,0:T(8,128)} %copy-done.7) | copy-start | bytes 147460

commit v5 on v3

--- a/solution.py
+++ b/solution.py
@@ -109,7 +109,7 @@
     return jnp.where(value >= count, value - count, value)
 
 
-def spread_body(index, tokens, gain, query, key, value, out, weights):
+def weights_and_tokens(tokens, gain, query, key, value, out, weights):
     cols = query.shape[1]
     for place, weight in enumerate((query, key, value)):
         weights[:, place * cols : (place + 1) * cols] = weight[...]
@@ -134,9 +134,19 @@
     return jnp.sum(jnp.where(same, row, 0.0), axis=1, keepdims=True)
 
 
-def prepare_body(
-    index, tokens, gain, decay_weight, beta_weight, rate, ids, prob, logit, meta, factors
+def spread_body(
+    index, tokens, gain, query, key, value, decay_weight, beta_weight, rate, ids, prob, logit,
+    far_out, far_weights, far_meta, far_factors, out, weights, meta, factors, stored,
 ):
+    stores = [
+        pltpu.make_async_copy(near, far, stored.at[place])
+        for place, (near, far) in enumerate(
+            ((out, far_out), (weights, far_weights), (meta, far_meta), (factors, far_factors))
+        )
+    ]
+    weights_and_tokens(tokens, gain, query, key, value, out, weights)
+    stores[0].start()
+    stores[1].start()
     rows, width = tokens.shape
     block = meta.shape[1]
     wide = tokens[...].astype(F32)
@@ -188,9 +198,13 @@
     spot = lane == lax.broadcasted_iota(jnp.int32, shape, 0) + index[0] * rows
     spot = jnp.where(spot, 1.0, 0.0).astype(BF)
     meta[...] = jnp.dot(table.astype(BF), spot, preferred_element_type=F32).astype(BF)
-
-
-def project_body(index, arrived, w0, w1, w2, w3, after, out):
+    stores[2].start()
+    stores[3].start()
+    for store in stores:
+        store.wait()
+
+
+def project_body(index, arrived, w0, w1, w2, w3, out):
     groups, rows, _ = arrived.shape
     total = None
     for step, weight in enumerate((w0, w1, w2, w3)):
@@ -477,60 +491,59 @@
         place = pl.multiple_of(index[2] * block, block)
         return ref.at[:, pl.ds(place, block)]
 
-    message, own_weights = kernel(
+    first = (
+        shape(NZ, rows, block),
+        shape(query_weight.shape[0], 3 * cols),
+        shape(8, block),
+        shape(rows, 128, dtype=F32),
+    )
+    message, own_weights, meta, factors = kernel(
         spread_body,
-        (pltpu.HBM((NZ, rows, block), BF), shape(query_weight.shape[0], 3 * cols)),
+        tuple(pltpu.HBM(made.shape, made.dtype) for made in first),
         tokens,
         attn_gain[None],
         query_weight,
         key_weight,
         value_weight,
-        far=range(5),
-    )
-    qkv_weights = from_neighbours(own_weights, "x")
-    spread = exchange(message, "z")
-    meta, factors = kernel(
-        prepare_body,
-        (shape(8, block), shape(rows, 128, dtype=F32)),
-        tokens,
-        attn_gain[None],
         decay_weight.T,
         beta_weight.T,
         decay_rate[None],
         expert_ids.T,
         group_prob[None],
         expert_logit.T,
-        far=range(8),
-        flops=10**8,
-    )
+        far=range(11),
+        far_outs=range(4),
+        scratch=[pltpu.VMEM(made.shape, made.dtype) for made in first]
+        + [pltpu.SemaphoreType.DMA((4,))],
+    )
+    qkv_weights = from_neighbours(own_weights, "x")
+    spread = exchange(message, "z")
+    (packed,) = kernel(
+        pack_body,
+        (shape(block + dense_gate.shape[1] * 2, half),),
+        message,
+        dense_gate,
+        dense_up,
+        dense_down,
+        plain=(0,),
+        far=(1, 2, 3),
+    )
+    dense_weights = from_neighbours(packed, "x")
     (part,) = kernel(
         project_body,
         (shape(NZ, rows, 3 * cols),),
         spread,
         *qkv_weights,
-        factors,
         held=(1, 2, 3, 4),
-        plain=(5,),
         flops=2 * NZ * rows * block * 3 * cols,
     )
-    (packed,) = kernel(
-        pack_body,
-        (shape(block + dense_gate.shape[1] * 2, half),),
-        part,
-        dense_gate,
-        dense_up,
-        dense_down,
-        plain=(0,),
-        far=(1, 2, 3),
-    )
-    dense_weights = from_neighbours(packed, "x")
     arrived = exchange(part, "z")
     attn_part, keys, changes = kernel(
         recall_body,
         (
             shape(NT, rows, block),
-            shape(rows, cols, dtype=F32),
-            shape(rows, cols, dtype=F32),
+            pltpu.HBM((rows, cols), F32),
+            pltpu.HBM((rows, cols), F32),
         ),
         arrived,
         factors,
@@ -569,8 +582,8 @@
         ffn_gain[None],
         *dense_weights,
         new_state,
+        plain=(6,),
         far=range(1, 6),
-        plain=(6,),
         parts={
             1: ((1, block), own_block),
             **{n: ((block, half), lambda ref, index: ref.at[:block]) for n in range(2, 6)},

time: 149 us -> 150 us (level)
  waiting for transfers between devices: 20.6 us -> 24.1 us
    ppermute x6, waiting for transfers between devices: 16.5 us -> 20 us  [from_neighbours(): parts.append(lax.ppermute(shard, axis, pairs))]
    pallas_call x12 -> x11, Pallas kernels: 20.7 us -> 19.7 us  [kernel(): pl.pallas_call(run, out_shape=outs, in_specs=specs, out_specs=out_specs,...]
    unnamed x38 -> x28, local copies, waits for them, and re-layouts: 3.66 us -> 3.34 us
  transfers between devices with their start and end apart: 10 -> 10, of which waited for: 8 -> 8; matrix products, arithmetic and copies ran while one was open for 0% -> 0% of each run, Pallas kernels for 5% -> 4%
where the time goes in v5:
time: 150 us
  blocking collectives  80.6 us (54%)
  waiting for transfers between devices  24.1 us (16%)
  starting transfers between devices  21.2 us (14%)
  Pallas kernels  19.7 us (13%)
  local copies, waits for them, and re-layouts  3.34 us (2%)
    all_to_all x5, blocking collectives, exchange(): return lax.all_to_all(tiles, axes, split_axis=0, concat_axis=0, tiled=True)  80.6 us
    ppermute x6, waiting for transfers between devices, from_neighbours(): parts.append(lax.ppermute(shard, axis, pairs))  20 us
    pallas_call x11, Pallas kernels, kernel(): pl.pallas_call(run, out_shape=outs, in_specs=specs, out_specs=out_specs,...  19.7 us
    all_to_all x2, starting transfers between devices, exchange(): return lax.all_to_all(tiles, axes, split_axis=0, concat_axis=0, tiled=True)  11.9 us
    ppermute x6, starting transfers between devices, from_neighbours(): parts.append(lax.ppermute(shard, axis, pairs))  9.09 us
    unnamed x28, local copies, waits for them, and re-layouts  3.34 us
  transfers between devices with their start and end apart: 10, of which 8 were waited for; matrix products, arithmetic and copies ran while one was open for 0% of the time, Pallas kernels for 4%

profile of v5, /device:TPU:2, one launch (start us, length us, event | category | flops | bytes accessed | tf_op | source)
XLA Modules:
  0.0 149.7 jit_solution(5615554089871913894)
XLA Ops:
  0.6 3.0 %shard_map.221 = (bf16[8,24,512]{2,1,0:T(8,128)(2,1)}, bf16[128,768]{1,0:T(8,128)(2,1)}, bf16[8,512]{1,0:T(8,128)(2,1)}, f32[24,128]{1,0:T(8,128)}) custom-call(bf16[24,4096]{1,0:T(8,128)(2,1)} %refs_1_.2, f32[1,4096]{1,0:T(1,128)} %bitcast.31, bf16[128,256]{1,0:T(8,128)(2,1)} %refs_2_.3, bf16[128,256]{1,0:T(8,128)(2,1)} %refs_3_.3, ...), custom_call_target="tpu_custom_call" | custom-call | tf_op jit(solution)/shard_map/pallas_call | solution.py:97
  3.6 8.5 %all-to-all-start = ((bf16[8,24,512]{2,1,0:T(8,128)(2,1)}), bf16[8,24,512]{2,1,0:T(8,128)(2,1)S(1)}, u32[]{:S(2)}, u32[]{:S(2)}) async-start(bf16[8,24,512]{2,1,0:T(8,128)(2,1)} %get-tuple-element.16.refs_0_), calls=%async_computation | async-start | bytes 393216 | tf_op jit(solution)/shard_map/all_to_all | solution.py:17
  12.1 1.5 collective-permute-start.2
  13.6 1.1 collective-permute-start.1
  14.7 2.2 %collective-permute-start = (bf16[128,768]{1,0:T(8,128)(2,1)}, bf16[128,768]{1,0:T(8,128)(2,1)S(1)}, u32[]{:S(2)}, u32[]{:S(2)}) collective-permute-start(bf16[128,768]{1,0:T(8,128)(2,1)} %get-tuple-element.17.refs_1_), channel_id=1, source_target_pairs={{0,24},{8,0},{16,8},{24,16},{1,25},{9,1},{17,9},{25,17},{2,26},{10... | collective-permute-start | bytes 589832 | tf_op jit(solution)/shard_map/ppermute | solution.py:25
  16.9 3.2 %collective-permute-done.2.refs_4_ = bf16[128,768]{1,0:T(8,128)(2,1)S(1)} collective-permute-done((bf16[128,768]{1,0:T(8,128)(2,1)}, bf16[128,768]{1,0:T(8,128)(2,1)S(1)}, u32[]{:S(2)}, u32[]{:S(2)}) %collective-permute-start.2) | collective-permute-done | bytes 196640 | tf_op jit(solution)/shard_map/ppermute | solution.py:25
  20.1 0.0 copy-start.11
  20.1 3.0 %collective-permute-done.1.refs_3_ = bf16[128,768]{1,0:T(8,128)(2,1)S(1)} collective-permute-done((bf16[128,768]{1,0:T(8,128)(2,1)}, bf16[128,768]{1,0:T(8,128)(2,1)S(1)}, u32[]{:S(2)}, u32[]{:S(2)}) %collective-permute-start.1) | collective-permute-done | bytes 196640 | tf_op jit(solution)/shard_map/ppermute | solution.py:25
  23.1 0.0 copy-start.12
  23.1 1.8 %collective-permute-done.refs_2_ = bf16[128,768]{1,0:T(8,128)(2,1)S(1)} collective-permute-done((bf16[128,768]{1,0:T(8,128)(2,1)}, bf16[128,768]{1,0:T(8,128)(2,1)S(1)}, u32[]{:S(2)}, u32[]{:S(2)}) %collective-permute-start) | collective-permute-done | bytes 196640 | tf_op jit(solution)/shard_map/ppermute | solution.py:25
  24.9 0.0 copy-start.13
  24.9 0.0 all-to-all-done.refs_0_
  24.9 0.0 copy-done.11
  24.9 0.0 copy-done.12
  24.9 0.7 copy-done.13
  25.6 1.7 %shard_map.222 = bf16[8,24,768]{2,1,0:T(8,128)(2,1)S(1)} custom-call(bf16[8,24,512]{2,1,0:T(8,128)(2,1)S(1)} %all-to-all-done.refs_0_, bf16[128,768]{1,0:T(8,128)(2,1)} %get-tuple-element.17.refs_1_, bf16[128,768]{1,0:T(8,128)(2,1)} %copy-done.13, bf16[128,768]{1,0:T(8,128)(2,1)} %copy-done.12, bf16[128,768]{1,0:T(8,128)(2,1)} %copy-done.11), custom_call_target="tpu_custom_call" | custom-call | flops 150994944 | tf_op jit(solution)/shard_map/pallas_call | solution.py:97
  27.3 0.0 copy-start.5
  27.3 0.0 copy-start.7
  27.3 18.9 %all_to_all.35.refs_0_ = bf16[8,24,768]{2,1,0:T(8,128)(2,1)S(1)} all-to-all(bf16[8,24,768]{2,1,0:T(8,128)(2,1)S(1)} %shard_map.222), channel_id=1, replica_groups=mesh['z'=8,'x'=4,'y'=4,'c'=2] {'z'}, dimensions={0} | all-to-all | bytes 589824 | tf_op jit(solution)/shard_map/all_to_all | solution.py:17
  46.2 0.0 copy-start
  46.3 1.9 %copy-done = f32[24,2,128,128]{3,2,1,0:T(8,128)S(1)} copy-done((f32[24,2,128,128]{3,2,1,0:T(8,128)S(1)}, f32[24,2,128,128]{3,2,1,0:T(8,128)}, u32[]{:S(2)}) %copy-start) | copy-done | bytes 3145752
  48.1 2.3 %shard_map.223 = (bf16[8,24,512]{2,1,0:T(8,128)(2,1)S(1)}, f32[24,256]{1,0:T(8,128)}, f32[24,256]{1,0:T(8,128)}) custom-call(bf16[8,24,768]{2,1,0:T(8,128)(2,1)S(1)} %all_to_all.35.refs_0_, f32[24,128]{1,0:T(8,128)} %get-tuple-element.18.refs_1_.refs_2_, f32[24,2,128,128]{3,2,1,0:T(8,128)S(1)} %copy-done, f32[1,128]{1,0:T(1,128)} %bitcast.35, ...), custom_call_target="tpu_custom_call" | custom-call | flops 50331648 | tf_op jit(solution)/shard_map/pallas_call | solution.py:97
  50.4 11.1 %all_to_all.36.refs_0_ = bf16[8,24,512]{2,1,0:T(8,128)(2,1)S(1)} all-to-all(bf16[8,24,512]{2,1,0:T(8,128)(2,1)S(1)} %get-tuple-element.19), channel_id=1, replica_groups=mesh['z'=8,'x'=4,'y'=4,'c'=2] {'y','c'}, dimensions={0} | all-to-all | bytes 393216 | tf_op jit(solution)/shard_map/all_to_all | solution.py:17
  61.5 0.0 copy-done.5
  61.5 0.0 copy-done.7
  61.5 0.8 shard_map.224
  62.3 3.4 %all-to-all-start.3 = ((bf16[8,32,512]{2,1,0:T(8,128)(2,1)}), bf16[8,32,512]{2,1,0:T(8,128)(2,1)S(1)}, u32[]{:S(2)}, u32[]{:S(2)}) async-start(bf16[8,32,512]{2,1,0:T(8,128)(2,1)} %get-tuple-element.21), calls=%async_computation.3 | async-start | bytes 524288 | tf_op jit(solution)/shard_map/all_to_all | solution.py:17
  65.7 1.1 shard_map.225.refs_2_
  66.8 0.0 copy-start.2
  66.8 0.2 collective-permute-start.5
  67.0 1.8 %collective-permute-start.4 = (bf16[768,256]{1,0:T(8,128)(2,1)S(1)}, bf16[768,256]{1,0:T(8,128)(2,1)S(1)}, u32[]{:S(2)}, u32[]{:S(2)}) collective-permute-start(bf16[768,256]{1,0:T(8,128)(2,1)S(1)} %shard_map.225.refs_2_), channel_id=1, source_target_pairs={{0,16},{8,24},{16,0},{24,8},{1,17},{9,25},{17,1},{25,9},{2,18},{10... | collective-permute-start | bytes 1179656 | tf_op jit(solution)/shard_map/ppermute | solution.py:25
  68.7 2.4 %collective-permute-start.3 = (bf16[768,256]{1,0:T(8,128)(2,1)S(1)}, bf16[768,256]{1,0:T(8,128)(2,1)S(1)}, u32[]{:S(2)}, u32[]{:S(2)}) collective-permute-start(bf16[768,256]{1,0:T(8,128)(2,1)S(1)} %shard_map.225.refs_2_), channel_id=1, source_target_pairs={{0,24},{8,0},{16,8},{24,16},{1,25},{9,1},{17,9},{25,17},{2,26},{10... | collective-permute-start | bytes 1179656 | tf_op jit(solution)/shard_map/ppermute | solution.py:25
  71.1 4.3 %shard_map.226.refs_6_ = f32[24,2,128,128]{3,2,1,0:T(8,128)} custom-call(f32[24,256]{1,0:T(8,128)} %get-tuple-element.22.refs_0_, f32[24,256]{1,0:T(8,128)} %get-tuple-element.23.refs_1_, f32[24,128]{1,0:T(8,128)} %get-tuple-element.18.refs_1_.refs_2_, f32[24,2,128,128]{3,2,1,0:T(8,128)} %refs_3_.5), custom_call_target="tpu_custom_call" | custom-call | flops 100000000 | tf_op jit(solution)/shard_map/pallas_call | solution.py:97
  75.4 0.0 copy-done.2
  75.4 3.5 %collective-permute-done.5.refs_5_ = bf16[768,256]{1,0:T(8,128)(2,1)S(1)} collective-permute-done((bf16[768,256]{1,0:T(8,128)(2,1)S(1)}, bf16[768,256]{1,0:T(8,128)(2,1)S(1)}, u32[]{:S(2)}, u32[]{:S(2)}) %collective-permute-start.5) | collective-permute-done | bytes 393248 | tf_op jit(solution)/shard_map/ppermute | solution.py:25
  78.8 0.0 copy-start.8
  78.8 1.6 %collective-permute-done.4.refs_4_ = bf16[768,256]{1,0:T(8,128)(2,1)S(1)} collective-permute-done((bf16[768,256]{1,0:T(8,128)(2,1)S(1)}, bf16[768,256]{1,0:T(8,128)(2,1)S(1)}, u32[]{:S(2)}, u32[]{:S(2)}) %collective-permute-start.4) | collective-permute-done | bytes 393248 | tf_op jit(solution)/shard_map/ppermute | solution.py:25
  80.5 0.0 copy-start.9
  80.5 6.8 %collective-permute-done.3.refs_3_ = bf16[768,256]{1,0:T(8,128)(2,1)S(1)} collective-permute-done((bf16[768,256]{1,0:T(8,128)(2,1)S(1)}, bf16[768,256]{1,0:T(8,128)(2,1)S(1)}, u32[]{:S(2)}, u32[]{:S(2)}) %collective-permute-start.3) | collective-permute-done | bytes 393248 | tf_op jit(solution)/shard_map/ppermute | solution.py:25
  87.3 0.0 copy-start.10
  87.3 0.0 all-to-all-done.3.refs_0_
  87.3 0.0 copy-done.8
  87.3 0.0 copy-done.9
  87.3 0.7 copy-done.10
  88.1 0.0 copy-start.1
  88.1 0.0 copy-start.3
  88.1 0.0 copy-start.4
  88.1 2.7 %shard_map.227 = (bf16[4,4,104,256]{3,2,1,0:T(8,128)(2,1)S(1)}, f32[8,192]{1,0:T(8,128)S(1)}) custom-call(bf16[8,32,512]{2,1,0:T(8,128)(2,1)S(1)} %all-to-all-done.3.refs_0_, f32[1,4096]{1,0:T(1,128)} %bitcast.29, bf16[768,256]{1,0:T(8,128)(2,1)} %copy-done.2, bf16[768,256]{1,0:T(8,128)(2,1)} %copy-done.10, bf16[768,256]{1,0:T(8,128)(2,1)} %copy-done.9, ...), custom_call_target="tpu_custom_call" | custom-call | flops 201326592 | tf_op jit(solution)/shard_map/pallas_call | solution.py:97
  90.7 0.0 copy-start.6
  90.8 17.8 %all_to_all.37 = bf16[16,104,256]{2,1,0:T(8,128)(2,1)S(1)} all-to-all(bf16[16,104,256]{2,1,0:T(8,128)(2,1)S(1)} %bitcast.26), channel_id=1, replica_groups=mesh['z'=8,'x'=4,'y'=4,'c'=2] {'x','y'}, dimensions={0} | all-to-all | bytes 1703936 | tf_op jit(solution)/shard_map/all_to_all | solution.py:17
  108.6 0.0 collective-permute-start.6
  108.6 2.4 %collective-permute-done.6 = bf16[16,104,256]{2,1,0:T(8,128)(2,1)S(1)} collective-permute-done((bf16[16,104,256]{2,1,0:T(8,128)(2,1)S(1)}, bf16[16,104,256]{2,1,0:T(8,128)(2,1)S(1)}, u32[]{:S(2)}, u32[]{:S(2)}) %collective-permute-start.6) | collective-permute-done | bytes 852000 | tf_op jit(solution)/shard_map/ppermute | solution.py:595
  110.9 0.0 copy-done.1
  110.9 0.0 copy-done.3
  110.9 0.0 copy-done.4
  111.0 1.6 %shard_map.228 = (bf16[4,5,24,512]{3,2,1,0:T(8,128)(2,1)S(1)}, bf16[96,128]{1,0:T(8,128)(2,1)S(1)}, bf16[4,24,128]{2,1,0:T(8,128)(2,1)S(1)}) custom-call(bf16[4,4,104,256]{3,2,1,0:T(8,128)(2,1)S(1)} %bitcast.20, bf16[4,4,104,256]{3,2,1,0:T(8,128)(2,1)S(1)} %bitcast.25, f32[1,4096]{1,0:T(1,128)} %bitcast.30, bf16[4096,128]{1,0:T(8,128)(2,1)S(1)} %bitcast.23, ...), custom_call_target="tpu_custom_call" | custom-call | flops 251658240 | tf_op jit(solution)/shard_map/pallas_call | solution.py:97
  112.6 0.0 copy-done.6
  112.6 0.2 collective-permute-start.7
  112.8 1.7 %collective-permute-done.7.refs_2_ = bf16[4,5,24,512]{3,2,1,0:T(8,128)(2,1)S(1)} collective-permute-done((bf16[4,5,24,512]{3,2,1,0:T(8,128)(2,1)S(1)}, bf16[4,5,24,512]{3,2,1,0:T(8,128)(2,1)S(1)}, u32[]{:S(2)}, u32[]{:S(2)}) %collective-permute-start.7) | collective-permute-done | bytes 491552 | tf_op jit(solution)/shard_map/ppermute | solution.py:613
  114.5 0.3 shard_map.229
  114.8 16.4 %all_to_all.38 = bf16[16,24,768]{2,1,0:T(8,128)(2,1)S(1)} all-to-all(bf16[16,24,768]{2,1,0:T(8,128)(2,1)S(1)} %bitcast.22), channel_id=1, replica_groups=mesh['z'=8,'x'=4,'y'=4,'c'=2] {'x','y'}, dimensions={0} | all-to-all | bytes 1179648 | tf_op jit(solution)/shard_map/all_to_all | solution.py:17
  131.2 1.5 shard_map.230
  132.7 16.4 %all_to_all.39.refs_0_ = bf16[8,24,512]{2,1,0:T(8,128)(2,1)S(1)} all-to-all(bf16[8,24,512]{2,1,0:T(8,128)(2,1)S(1)} %shard_map.230), channel_id=1, replica_groups=mesh['z'=8,'x'=4,'y'=4,'c'=2] {'z'}, dimensions={0} | all-to-all | bytes 393216 | tf_op jit(solution)/shard_map/all_to_all | solution.py:17
  149.1 0.6 shard_map.231
Async XLA Ops:
  3.6 21.3 %all-to-all-start = ((bf16[8,24,512]{2,1,0:T(8,128)(2,1)}), bf16[8,24,512]{2,1,0:T(8,128)(2,1)S(1)}, u32[]{:S(2)}, u32[]{:S(2)}) async-start(bf16[8,24,512]{2,1,0:T(8,128)(2,1)} %get-tuple-element.16.refs_0_), calls=%async_computation | async-start | bytes 393216 | tf_op jit(solution)/shard_map/all_to_all | solution.py:17
  12.1 8.0 %collective-permute-start.2 = (bf16[128,768]{1,0:T(8,128)(2,1)}, bf16[128,768]{1,0:T(8,128)(2,1)S(1)}, u32[]{:S(2)}, u32[]{:S(2)}) collective-permute-start(bf16[128,768]{1,0:T(8,128)(2,1)} %get-tuple-element.17.refs_1_), channel_id=1, source_target_pairs={{0,8},{8,16},{16,24},{24,0},{1,9},{9,17},{17,25},{25,1},{2,10},{10... | collective-permute-start | bytes 589832 | tf_op jit(solution)/shard_map/ppermute | solution.py:25
  13.6 9.5 %collective-permute-start.1 = (bf16[128,768]{1,0:T(8,128)(2,1)}, bf16[128,768]{1,0:T(8,128)(2,1)S(1)}, u32[]{:S(2)}, u32[]{:S(2)}) collective-permute-start(bf16[128,768]{1,0:T(8,128)(2,1)} %get-tuple-element.17.refs_1_), channel_id=1, source_target_pairs={{0,16},{8,24},{16,0},{24,8},{1,17},{9,25},{17,1},{25,9},{2,18},{10... | collective-permute-start | bytes 589832 | tf_op jit(solution)/shard_map/ppermute | solution.py:25
  14.7 10.2 %collective-permute-start = (bf16[128,768]{1,0:T(8,128)(2,1)}, bf16[128,768]{1,0:T(8,128)(2,1)S(1)}, u32[]{:S(2)}, u32[]{:S(2)}) collective-permute-start(bf16[128,768]{1,0:T(8,128)(2,1)} %get-tuple-element.17.refs_1_), channel_id=1, source_target_pairs={{0,24},{8,0},{16,8},{24,16},{1,25},{9,1},{17,9},{25,17},{2,26},{10... | collective-permute-start | bytes 589832 | tf_op jit(solution)/shard_map/ppermute | solution.py:25
  20.1 4.9 %copy-start.11 = (bf16[128,768]{1,0:T(8,128)(2,1)}, bf16[128,768]{1,0:T(8,128)(2,1)S(1)}, u32[]{:S(2)}) copy-start(bf16[128,768]{1,0:T(8,128)(2,1)S(1)} %collective-permute-done.2.refs_4_) | copy-start | bytes 589828
  23.1 1.9 %copy-start.12 = (bf16[128,768]{1,0:T(8,128)(2,1)}, bf16[128,768]{1,0:T(8,128)(2,1)S(1)}, u32[]{:S(2)}) copy-start(bf16[128,768]{1,0:T(8,128)(2,1)S(1)} %collective-permute-done.1.refs_3_) | copy-start | bytes 589828
  24.9 0.7 copy-start.13
  27.3 34.2 %copy-start.5 = (bf16[24,4096]{1,0:T(8,128)(2,1)S(1)}, bf16[24,4096]{1,0:T(8,128)(2,1)}, u32[]{:S(2)}) copy-start(bf16[24,4096]{1,0:T(8,128)(2,1)} %refs_1_.2) | copy-start | bytes 589828
  27.3 34.2 %copy-start.7 = (bf16[8,512]{1,0:T(8,128)(2,1)S(1)}, bf16[8,512]{1,0:T(8,128)(2,1)}, u32[]{:S(2)}) copy-start(bf16[8,512]{1,0:T(8,128)(2,1)} %get-tuple-element.20.refs_2_) | copy-start | bytes 24580
  46.2 1.9 %copy-start = (f32[24,2,128,128]{3,2,1,0:T(8,128)S(1)}, f32[24,2,128,128]{3,2,1,0:T(8,128)}, u32[]{:S(2)}) copy-start(f32[24,2,128,128]{3,2,1,0:T(8,128)} %refs_3_.5) | copy-start | bytes 9437188
  62.3 25.0 %all-to-all-start.3 = ((bf16[8,32,512]{2,1,0:T(8,128)(2,1)}), bf16[8,32,512]{2,1,0:T(8,128)(2,1)S(1)}, u32[]{:S(2)}, u32[]{:S(2)}) async-start(bf16[8,32,512]{2,1,0:T(8,128)(2,1)} %get-tuple-element.21), calls=%async_computation.3 | async-start | bytes 524288 | tf_op jit(solution)/shard_map/all_to_all | solution.py:17
  66.8 8.6 %copy-start.2 = (bf16[768,256]{1,0:T(8,128)(2,1)}, bf16[768,256]{1,0:T(8,128)(2,1)S(1)}, u32[]{:S(2)}) copy-start(bf16[768,256]{1,0:T(8,128)(2,1)S(1)} %shard_map.225.refs_2_) | copy-start | bytes 1179652
  66.8 12.1 %collective-permute-start.5 = (bf16[768,256]{1,0:T(8,128)(2,1)S(1)}, bf16[768,256]{1,0:T(8,128)(2,1)S(1)}, u32[]{:S(2)}, u32[]{:S(2)}) collective-permute-start(bf16[768,256]{1,0:T(8,128)(2,1)S(1)} %shard_map.225.refs_2_), channel_id=1, source_target_pairs={{0,8},{8,16},{16,24},{24,0},{1,9},{9,17},{17,25},{25,1},{2,10},{10... | collective-permute-start | bytes 1179656 | tf_op jit(solution)/shard_map/ppermute | solution.py:25
  67.0 13.5 %collective-permute-start.4 = (bf16[768,256]{1,0:T(8,128)(2,1)S(1)}, bf16[768,256]{1,0:T(8,128)(2,1)S(1)}, u32[]{:S(2)}, u32[]{:S(2)}) collective-permute-start(bf16[768,256]{1,0:T(8,128)(2,1)S(1)} %shard_map.225.refs_2_), channel_id=1, source_target_pairs={{0,16},{8,24},{16,0},{24,8},{1,17},{9,25},{17,1},{25,9},{2,18},{10... | collective-permute-start | bytes 1179656 | tf_op jit(solution)/shard_map/ppermute | solution.py:25
  68.7 18.5 %collective-permute-start.3 = (bf16[768,256]{1,0:T(8,128)(2,1)S(1)}, bf16[768,256]{1,0:T(8,128)(2,1)S(1)}, u32[]{:S(2)}, u32[]{:S(2)}) collective-permute-start(bf16[768,256]{1,0:T(8,128)(2,1)S(1)} %shard_map.225.refs_2_), channel_id=1, source_target_pairs={{0,24},{8,0},{16,8},{24,16},{1,25},{9,1},{17,9},{25,17},{2,26},{10... | collective-permute-start | bytes 1179656 | tf_op jit(solution)/shard_map/ppermute | solution.py:25
  78.8 8.5 %copy-start.8 = (bf16[768,256]{1,0:T(8,128)(2,1)}, bf16[768,256]{1,0:T(8,128)(2,1)S(1)}, u32[]{:S(2)}) copy-start(bf16[768,256]{1,0:T(8,128)(2,1)S(1)} %collective-permute-done.5.refs_5_) | copy-start | bytes 1179652
  80.5 6.8 %copy-start.9 = (bf16[768,256]{1,0:T(8,128)(2,1)}, bf16[768,256]{1,0:T(8,128)(2,1)S(1)}, u32[]{:S(2)}) copy-start(bf16[768,256]{1,0:T(8,128)(2,1)S(1)} %collective-permute-done.4.refs_4_) | copy-start | bytes 1179652
  87.3 0.8 copy-start.10
  88.1 22.9 %copy-start.1 = (bf16[1,128,4096]{2,1,0:T(8,128)(2,1)S(1)}, bf16[1,128,4096]{2,1,0:T(8,128)(2,1)}, u32[]{:S(2)}) copy-start(bf16[1,128,4096]{2,1,0:T(8,128)(2,1)} %param.39) | copy-start | bytes 3145732
  88.1 22.9 %copy-start.3 = (bf16[1,4096,128]{2,1,0:T(8,128)(2,1)S(1)}, bf16[1,4096,128]{2,1,0:T(8,128)(2,1)}, u32[]{:S(2)}) copy-start(bf16[1,4096,128]{2,1,0:T(8,128)(2,1)} %param.37) | copy-start | bytes 3145732
  88.1 22.9 %copy-start.4 = (bf16[1,4096,128]{2,1,0:T(8,128)(2,1)S(1)}, bf16[1,4096,128]{2,1,0:T(8,128)(2,1)}, u32[]{:S(2)}) copy-start(bf16[1,4096,128]{2,1,0:T(8,128)(2,1)} %param.38) | copy-start | bytes 3145732
  90.7 21.8 %copy-start.6 = (f32[8,192]{1,0:T(8,128)}, f32[8,192]{1,0:T(8,128)S(1)}, u32[]{:S(2)}) copy-start(f32[8,192]{1,0:T(8,128)S(1)} %get-tuple-element.28.refs_1_) | copy-start | bytes 18436
  108.6 2.4 %collective-permute-start.6 = (bf16[16,104,256]{2,1,0:T(8,128)(2,1)S(1)}, bf16[16,104,256]{2,1,0:T(8,128)(2,1)S(1)}, u32[]{:S(2)}, u32[]{:S(2)}) collective-permute-start(bf16[16,104,256]{2,1,0:T(8,128)(2,1)S(1)} %all_to_all.37), channel_id=1, source_target_pairs={{0,1},{1,0},{2,3},{3,2},{4,5},{5,4},{6,7},{7,6},{8,9},{9,8},{10,11... | collective-permute-start | bytes 2555912 | tf_op jit(solution)/shard_map/ppermute | solution.py:595
  112.6 2.0 %collective-permute-start.7 = (bf16[4,5,24,512]{3,2,1,0:T(8,128)(2,1)S(1)}, bf16[4,5,24,512]{3,2,1,0:T(8,128)(2,1)S(1)}, u32[]{:S(2)}, u32[]{:S(2)}) collective-permute-start(bf16[4,5,24,512]{3,2,1,0:T(8,128)(2,1)S(1)} %get-tuple-element.27), channel_id=1, source_target_pairs={{0,1},{1,0},{2,3},{3,2},{4,5},{5,4},{6,7},{7,6},{8,9},{9,8},{10,11... | collective-permute-start | bytes 1474568 | tf_op jit(solution)/shard_map/ppermute | solution.py:613

commit v6 on v5

--- a/solution.py
+++ b/solution.py
@@ -110,13 +110,14 @@
 
 
 def weights_and_tokens(tokens, gain, query, key, value, out, weights):
+    rows = tokens.shape[0]
     cols = query.shape[1]
     for place, weight in enumerate((query, key, value)):
         weights[:, place * cols : (place + 1) * cols] = weight[...]
     block = out.shape[2]
     for z in range(NZ):
         cols = slice(z * block, (z + 1) * block)
-        out[z] = (tokens[:, cols].astype(F32) * gain[:, cols]).astype(BF)
+        out[z, :rows, :] = (tokens[:, cols].astype(F32) * gain[:, cols]).astype(BF)
 
 
 def pack_body(index, after, gate, up, down, out):
@@ -136,19 +137,18 @@
 
 def spread_body(
     index, tokens, gain, query, key, value, decay_weight, beta_weight, rate, ids, prob, logit,
-    far_out, far_weights, far_meta, far_factors, out, weights, meta, factors, stored,
+    far_out, far_weights, far_factors, out, weights, factors, stored,
 ):
     stores = [
         pltpu.make_async_copy(near, far, stored.at[place])
         for place, (near, far) in enumerate(
-            ((out, far_out), (weights, far_weights), (meta, far_meta), (factors, far_factors))
+            ((weights, far_weights), (out, far_out), (factors, far_factors))
         )
     ]
     weights_and_tokens(tokens, gain, query, key, value, out, weights)
     stores[0].start()
-    stores[1].start()
     rows, width = tokens.shape
-    block = meta.shape[1]
+    block = out.shape[2]
     wide = tokens[...].astype(F32)
     row_scale = lax.rsqrt(jnp.sum(wide * wide, axis=1, keepdims=True) / width + EPS)
     gained = (wide * gain[...]).astype(BF)
@@ -197,20 +197,27 @@
     lane = lax.broadcasted_iota(jnp.int32, shape, 1)
     spot = lane == lax.broadcasted_iota(jnp.int32, shape, 0) + index[0] * rows
     spot = jnp.where(spot, 1.0, 0.0).astype(BF)
-    meta[...] = jnp.dot(table.astype(BF), spot, preferred_element_type=F32).astype(BF)
+    meta = jnp.dot(table.astype(BF), spot, preferred_element_type=F32).astype(BF)
+    for z in range(NZ):
+        out[z, rows:, :] = meta
+    stores[1].start()
     stores[2].start()
-    stores[3].start()
     for store in stores:
         store.wait()
 
 
-def project_body(index, arrived, w0, w1, w2, w3, out):
-    groups, rows, _ = arrived.shape
+def project_body(index, arrived, w0, w1, w2, w3, out, route):
+    groups, rows, _ = out.shape
+    tokens = groups * rows
+    routing = arrived[0, rows:, :tokens].astype(F32)
+    for z in range(1, groups):
+        routing = routing + arrived[z, rows:, :tokens].astype(F32)
+    route[...] = routing
     total = None
     for step, weight in enumerate((w0, w1, w2, w3)):
         size = weight.shape[0]
         place = pl.multiple_of(wrapped(index[1] + step, NX) * size, size)
-        left = arrived[:, :, pl.ds(place, size)].astype(F32).reshape(groups * rows, size).astype(BF)
+        left = arrived[:, :rows, pl.ds(place, size)].astype(F32).reshape(tokens, size).astype(BF)
         part = jnp.dot(left, weight[...], preferred_element_type=F32)
         total = part if total is None else total + part
     out[...] = total.reshape(groups, rows, -1).astype(BF)
@@ -276,9 +283,8 @@
                 new_state[b + side, h] = fade * state[b + side, h] + grown
 
 
-def middle_body(index, arrived, tokens, meta, middle, out):
+def middle_body(index, arrived, tokens, middle, out):
     block = middle.shape[1]
-    rows = middle.shape[0]
     summed = arrived[0].astype(F32)
     for t in range(1, NT):
         summed = summed + arrived[t].astype(F32)
@@ -287,8 +293,7 @@
     middle[...] = total
     narrow = total.astype(BF)
     for z in range(NZ):
-        out[z, :rows, :] = narrow
-        out[z, rows:, :] = meta[...]
+        out[z] = narrow
 
 
 def slots_of(route, zi):
@@ -308,27 +313,25 @@
     return slots
 
 
-def dispatch_body(index, arrived, gain, g0, g1, g2, g3, after, out, route):
-    rows = arrived.shape[1] - 8
+def dispatch_body(index, arrived, gain, g0, g1, g2, g3, route, after, out):
+    rows = arrived.shape[1]
     tokens = NZ * rows
     block = arrived.shape[2]
     half = block // 2
-    wide = arrived[:, :rows, :].astype(F32).reshape(tokens, block)
+    wide = arrived[...].astype(F32).reshape(tokens, block)
     narrow = wide.astype(BF)
-    routing = arrived[0, rows:, :tokens].astype(F32)
-    for z in range(1, NZ):
-        routing = routing + arrived[z, rows:, :tokens].astype(F32)
-    route[...] = routing
+    routing = route[...]
     slot0, slot1 = slots_of(routing, index[0])
     place = lax.broadcasted_iota(jnp.int32, (NX * rows, tokens), 0)
     picks = jnp.where((place == slot0) | (place == slot1), 1.0, 0.0).astype(BF)
     chosen = jnp.dot(picks, narrow, preferred_element_type=F32).astype(BF)
-    square = lax.dot_general(
-        jnp.ones((8, block), F32),
-        wide * wide,
-        (((1,), (1,)), ((), ())),
-        precision=lax.Precision.HIGHEST,
-        preferred_element_type=F32,
+    square = wide * wide
+    high = square.astype(BF)
+    ones = jnp.ones((8, block), BF)
+    over_block = (((1,), (1,)), ((), ()))
+    square = sum(
+        lax.dot_general(ones, part, over_block, preferred_element_type=F32)
+        for part in (high, (square - high.astype(F32)).astype(BF))
     )
     high = square.astype(BF).astype(F32)
     first = lax.broadcasted_iota(jnp.int32, square.shape, 0) == 0
@@ -492,12 +495,11 @@
         return ref.at[:, pl.ds(place, block)]
 
     first = (
-        shape(NZ, rows, block),
+        shape(NZ, rows + 8, block),
         shape(query_weight.shape[0], 3 * cols),
-        shape(8, block),
         shape(rows, 128, dtype=F32),
     )
-    message, own_weights, meta, factors = kernel(
+    message, own_weights, factors = kernel(
         spread_body,
         tuple(pltpu.HBM(made.shape, made.dtype) for made in first),
         tokens,
@@ -512,9 +514,9 @@
         group_prob[None],
         expert_logit.T,
         far=range(11),
-        far_outs=range(4),
+        far_outs=range(3),
         scratch=[pltpu.VMEM(made.shape, made.dtype) for made in first]
-        + [pltpu.SemaphoreType.DMA((4,))],
+        + [pltpu.SemaphoreType.DMA((3,))],
     )
     qkv_weights = from_neighbours(own_weights, "x")
     spread = exchange(message, "z")
@@ -529,9 +531,9 @@
         far=(1, 2, 3),
     )
     dense_weights = from_neighbours(packed, "x")
-    (part,) = kernel(
+    part, route_rows = kernel(
         project_body,
-        (shape(NZ, rows, 3 * cols),),
+        (shape(NZ, rows, 3 * cols), pltpu.HBM((8, NZ * rows), F32)),
         spread,
         *qkv_weights,
         held=(1, 2, 3, 4),
@@ -567,23 +569,23 @@
     arrived = exchange(attn_part, ("y", "c"))
     middle, message = kernel(
         middle_body,
-        (shape(rows, block, dtype=F32), shape(NZ, rows + 8, block)),
+        (shape(rows, block, dtype=F32), shape(NZ, rows, block)),
         arrived,
         tokens,
-        meta,
     )
 
     swap = [(0, 1), (1, 0)]
     arrived = exchange(message, "z")
-    message, route_rows = kernel(
+    (message,) = kernel(
         dispatch_body,
-        (shape(NX, NY, 4 * rows + 8, half), shape(8, NZ * rows, dtype=F32)),
+        (shape(NX, NY, 4 * rows + 8, half),),
         arrived,
         ffn_gain[None],
         *dense_weights,
+        route_rows,
         new_state,
-        plain=(6,),
-        far=range(1, 6),
+        plain=(7,),
+        far=range(1, 7),
         parts={
             1: ((1, block), own_block),
             **{n: ((block, half), lambda ref, index: ref.at[:block]) for n in range(2, 6)},

time: 150 us -> 139 us (0.927)
  blocking collectives: 80.6 us -> 67.1 us
  starting transfers between devices: 21.2 us -> 25.7 us
  waiting for transfers between devices: 24.1 us -> 20.9 us
    all_to_all x5 -> x4, blocking collectives: 80.6 us -> 67.1 us  [exchange(): return lax.all_to_all(tiles, axes, split_axis=0, concat_axis=0, tiled=True)]
    ppermute x6, waiting for transfers between devices: 20 us -> 15.4 us  [from_neighbours(): parts.append(lax.ppermute(shard, axis, pairs))]
    all_to_all x2 -> x3, starting transfers between devices: 11.9 us -> 16.3 us  [exchange(): return lax.all_to_all(tiles, axes, split_axis=0, concat_axis=0, tiled=True)]
    unnamed x28 -> x24, local copies, waits for them, and re-layouts: 3.34 us -> 3.33 us
  transfers between devices with their start and end apart: 10 -> 11, of which waited for: 8 -> 7; matrix products, arithmetic and copies ran while one was open for 0% -> 0% of each run, Pallas kernels for 4% -> 4%
where the time goes in v6:
time: 139 us
  blocking collectives  67.1 us (48%)
  starting transfers between devices  25.7 us (18%)
  waiting for transfers between devices  20.9 us (15%)
  Pallas kernels  20.8 us (15%)
  local copies, waits for them, and re-layouts  3.33 us (2%)
    all_to_all x4, blocking collectives, exchange(): return lax.all_to_all(tiles, axes, split_axis=0, concat_axis=0, tiled=True)  67.1 us
    pallas_call x11, Pallas kernels, kernel(): pl.pallas_call(run, out_shape=outs, in_specs=specs, out_specs=out_specs,...  20.8 us
    all_to_all x3, starting transfers between devices, exchange(): return lax.all_to_all(tiles, axes, split_axis=0, concat_axis=0, tiled=True)  16.3 us
    ppermute x6, waiting for transfers between devices, from_neighbours(): parts.append(lax.ppermute(shard, axis, pairs))  15.4 us
    ppermute x6, starting transfers between devices, from_neighbours(): parts.append(lax.ppermute(shard, axis, pairs))  9.09 us
    unnamed x24, local copies, waits for them, and re-layouts  3.33 us
  transfers between devices with their start and end apart: 11, of which 7 were waited for; matrix products, arithmetic and copies ran while one was open for 0% of the time, Pallas kernels for 4%

profile of v6, /device:TPU:2, one launch (start us, length us, event | category | flops | bytes accessed | tf_op | source)
XLA Modules:
  0.0 138.6 jit_solution(17725402645838384932)
XLA Ops:
  0.6 3.1 %shard_map.221 = (bf16[8,32,512]{2,1,0:T(8,128)(2,1)}, bf16[128,768]{1,0:T(8,128)(2,1)}, f32[24,128]{1,0:T(8,128)}) custom-call(bf16[24,4096]{1,0:T(8,128)(2,1)} %refs_1_.2, f32[1,4096]{1,0:T(1,128)} %bitcast.31, bf16[128,256]{1,0:T(8,128)(2,1)} %refs_2_.3, bf16[128,256]{1,0:T(8,128)(2,1)} %refs_3_.3, bf16[128,256]{1,0:T(8,128)(2,1)} %refs_4_.2, ...), custom_call_target="tpu_custom_call" | custom-call | tf_op jit(solution)/shard_map/pallas_call | solution.py:97
  3.7 8.5 %all-to-all-start = ((bf16[8,32,512]{2,1,0:T(8,128)(2,1)}), bf16[8,32,512]{2,1,0:T(8,128)(2,1)S(1)}, u32[]{:S(2)}, u32[]{:S(2)}) async-start(bf16[8,32,512]{2,1,0:T(8,128)(2,1)} %get-tuple-element.15.refs_0_), calls=%async_computation | async-start | bytes 524288 | tf_op jit(solution)/shard_map/all_to_all | solution.py:17
  12.2 1.5 %collective-permute-start.2 = (bf16[128,768]{1,0:T(8,128)(2,1)}, bf16[128,768]{1,0:T(8,128)(2,1)S(1)}, u32[]{:S(2)}, u32[]{:S(2)}) collective-permute-start(bf16[128,768]{1,0:T(8,128)(2,1)} %get-tuple-element.16.refs_1_), channel_id=1, source_target_pairs={{0,8},{8,16},{16,24},{24,0},{1,9},{9,17},{17,25},{25,1},{2,10},{10... | collective-permute-start | bytes 589832 | tf_op jit(solution)/shard_map/ppermute | solution.py:25
  13.7 1.1 collective-permute-start.1
  14.8 2.2 %collective-permute-start = (bf16[128,768]{1,0:T(8,128)(2,1)}, bf16[128,768]{1,0:T(8,128)(2,1)S(1)}, u32[]{:S(2)}, u32[]{:S(2)}) collective-permute-start(bf16[128,768]{1,0:T(8,128)(2,1)} %get-tuple-element.16.refs_1_), channel_id=1, source_target_pairs={{0,24},{8,0},{16,8},{24,16},{1,25},{9,1},{17,9},{25,17},{2,26},{10... | collective-permute-start | bytes 589832 | tf_op jit(solution)/shard_map/ppermute | solution.py:25
  17.0 3.2 %collective-permute-done.2.refs_4_ = bf16[128,768]{1,0:T(8,128)(2,1)S(1)} collective-permute-done((bf16[128,768]{1,0:T(8,128)(2,1)}, bf16[128,768]{1,0:T(8,128)(2,1)S(1)}, u32[]{:S(2)}, u32[]{:S(2)}) %collective-permute-start.2) | collective-permute-done | bytes 196640 | tf_op jit(solution)/shard_map/ppermute | solution.py:25
  20.2 0.0 copy-start.9
  20.2 3.0 %collective-permute-done.1.refs_3_ = bf16[128,768]{1,0:T(8,128)(2,1)S(1)} collective-permute-done((bf16[128,768]{1,0:T(8,128)(2,1)}, bf16[128,768]{1,0:T(8,128)(2,1)S(1)}, u32[]{:S(2)}, u32[]{:S(2)}) %collective-permute-start.1) | collective-permute-done | bytes 196640 | tf_op jit(solution)/shard_map/ppermute | solution.py:25
  23.2 0.0 copy-start.10
  23.2 1.8 %collective-permute-done.refs_2_ = bf16[128,768]{1,0:T(8,128)(2,1)S(1)} collective-permute-done((bf16[128,768]{1,0:T(8,128)(2,1)}, bf16[128,768]{1,0:T(8,128)(2,1)S(1)}, u32[]{:S(2)}, u32[]{:S(2)}) %collective-permute-start) | collective-permute-done | bytes 196640 | tf_op jit(solution)/shard_map/ppermute | solution.py:25
  25.0 0.0 copy-start.11
  25.0 0.0 all-to-all-done.refs_0_
  25.0 0.0 copy-done.9
  25.0 0.0 copy-done.10
  25.0 0.7 copy-done.11
  25.7 2.2 %shard_map.222 = (bf16[8,24,768]{2,1,0:T(8,128)(2,1)S(1)}, f32[8,192]{1,0:T(8,128)}) custom-call(bf16[8,32,512]{2,1,0:T(8,128)(2,1)S(1)} %all-to-all-done.refs_0_, bf16[128,768]{1,0:T(8,128)(2,1)} %get-tuple-element.16.refs_1_, bf16[128,768]{1,0:T(8,128)(2,1)} %copy-done.11, bf16[128,768]{1,0:T(8,128)(2,1)} %copy-done.10, bf16[128,768]{1,0:T(8,128)(2,1)} %copy-done.9), custom_call_target="tpu_custom_call" | custom-call | flops 150994944 | tf_op jit(solution)/shard_map/pallas_call | solution.py:97
  27.9 18.8 %all_to_all.35.refs_0_ = bf16[8,24,768]{2,1,0:T(8,128)(2,1)S(1)} all-to-all(bf16[8,24,768]{2,1,0:T(8,128)(2,1)S(1)} %get-tuple-element.17), channel_id=1, replica_groups=mesh['z'=8,'x'=4,'y'=4,'c'=2] {'z'}, dimensions={0} | all-to-all | bytes 589824 | tf_op jit(solution)/shard_map/all_to_all | solution.py:17
  46.7 0.0 copy-start
  46.7 1.9 %copy-done = f32[24,2,128,128]{3,2,1,0:T(8,128)S(1)} copy-done((f32[24,2,128,128]{3,2,1,0:T(8,128)S(1)}, f32[24,2,128,128]{3,2,1,0:T(8,128)}, u32[]{:S(2)}) %copy-start) | copy-done | bytes 3145752
  48.6 0.0 copy-start.5
  48.6 2.8 %shard_map.223 = (bf16[8,24,512]{2,1,0:T(8,128)(2,1)}, f32[24,256]{1,0:T(8,128)}, f32[24,256]{1,0:T(8,128)}) custom-call(bf16[8,24,768]{2,1,0:T(8,128)(2,1)S(1)} %all_to_all.35.refs_0_, f32[24,128]{1,0:T(8,128)} %get-tuple-element.18.refs_1_.refs_2_, f32[24,2,128,128]{3,2,1,0:T(8,128)S(1)} %copy-done, f32[1,128]{1,0:T(1,128)} %bitcast.35, ...), custom_call_target="tpu_custom_call" | custom-call | flops 50331648 | tf_op jit(solution)/shard_map/pallas_call | solution.py:97
  51.5 4.5 %all-to-all-start.2 = ((bf16[8,24,512]{2,1,0:T(8,128)(2,1)}), bf16[8,24,512]{2,1,0:T(8,128)(2,1)S(1)}, u32[]{:S(2)}, u32[]{:S(2)}) async-start(bf16[8,24,512]{2,1,0:T(8,128)(2,1)} %get-tuple-element.19), calls=%async_computation.2 | async-start | bytes 393216 | tf_op jit(solution)/shard_map/all_to_all | solution.py:17
  55.9 1.1 shard_map.225.refs_2_
  57.0 0.0 copy-start.2
  57.0 0.2 collective-permute-start.5
  57.2 1.8 %collective-permute-start.4 = (bf16[768,256]{1,0:T(8,128)(2,1)S(1)}, bf16[768,256]{1,0:T(8,128)(2,1)S(1)}, u32[]{:S(2)}, u32[]{:S(2)}) collective-permute-start(bf16[768,256]{1,0:T(8,128)(2,1)S(1)} %shard_map.225.refs_2_), channel_id=1, source_target_pairs={{0,16},{8,24},{16,0},{24,8},{1,17},{9,25},{17,1},{25,9},{2,18},{10... | collective-permute-start | bytes 1179656 | tf_op jit(solution)/shard_map/ppermute | solution.py:25
  59.0 2.4 %collective-permute-start.3 = (bf16[768,256]{1,0:T(8,128)(2,1)S(1)}, bf16[768,256]{1,0:T(8,128)(2,1)S(1)}, u32[]{:S(2)}, u32[]{:S(2)}) collective-permute-start(bf16[768,256]{1,0:T(8,128)(2,1)S(1)} %shard_map.225.refs_2_), channel_id=1, source_target_pairs={{0,24},{8,0},{16,8},{24,16},{1,25},{9,1},{17,9},{25,17},{2,26},{10... | collective-permute-start | bytes 1179656 | tf_op jit(solution)/shard_map/ppermute | solution.py:25
  61.4 1.4 %all-to-all-done.2.refs_0_ = bf16[8,24,512]{2,1,0:T(8,128)(2,1)S(1)} async-done(((bf16[8,24,512]{2,1,0:T(8,128)(2,1)}), bf16[8,24,512]{2,1,0:T(8,128)(2,1)S(1)}, u32[]{:S(2)}, u32[]{:S(2)}) %all-to-all-start.2) | async-done | bytes 196640 | tf_op jit(solution)/shard_map/all_to_all | solution.py:17
  62.7 0.0 copy-done.5
  62.7 0.7 shard_map.224
  63.5 3.4 %all-to-all-start.3 = ((bf16[8,24,512]{2,1,0:T(8,128)(2,1)}), bf16[8,24,512]{2,1,0:T(8,128)(2,1)S(1)}, u32[]{:S(2)}, u32[]{:S(2)}) async-start(bf16[8,24,512]{2,1,0:T(8,128)(2,1)} %get-tuple-element.20), calls=%async_computation.3 | async-start | bytes 393216 | tf_op jit(solution)/shard_map/all_to_all | solution.py:17
  66.9 4.3 %shard_map.226.refs_7_ = f32[24,2,128,128]{3,2,1,0:T(8,128)} custom-call(f32[24,256]{1,0:T(8,128)} %get-tuple-element.22.refs_0_, f32[24,256]{1,0:T(8,128)} %get-tuple-element.23.refs_1_, f32[24,128]{1,0:T(8,128)} %get-tuple-element.18.refs_1_.refs_2_, f32[24,2,128,128]{3,2,1,0:T(8,128)} %refs_3_.5), custom_call_target="tpu_custom_call" | custom-call | flops 100000000 | tf_op jit(solution)/shard_map/pallas_call | solution.py:97
  71.1 0.0 copy-done.2
  71.2 0.0 collective-permute-done.5.refs_5_
  71.2 0.0 copy-start.6
  71.2 0.0 collective-permute-done.4.refs_4_
  71.2 0.0 copy-start.7
  71.2 7.3 %collective-permute-done.3.refs_3_ = bf16[768,256]{1,0:T(8,128)(2,1)S(1)} collective-permute-done((bf16[768,256]{1,0:T(8,128)(2,1)S(1)}, bf16[768,256]{1,0:T(8,128)(2,1)S(1)}, u32[]{:S(2)}, u32[]{:S(2)}) %collective-permute-start.3) | collective-permute-done | bytes 393248 | tf_op jit(solution)/shard_map/ppermute | solution.py:25
  78.5 0.0 copy-start.8
  78.5 0.0 all-to-all-done.3.refs_0_
  78.5 0.0 copy-done.6
  78.5 0.0 copy-done.7
  78.5 0.7 copy-done.8
  79.3 0.0 copy-start.1
  79.3 0.0 copy-start.3
  79.3 0.0 copy-start.4
  79.3 2.7 %shard_map.227 = bf16[4,4,104,256]{3,2,1,0:T(8,128)(2,1)S(1)} custom-call(bf16[8,24,512]{2,1,0:T(8,128)(2,1)S(1)} %all-to-all-done.3.refs_0_, f32[1,4096]{1,0:T(1,128)} %bitcast.29, bf16[768,256]{1,0:T(8,128)(2,1)} %copy-done.2, bf16[768,256]{1,0:T(8,128)(2,1)} %copy-done.8, bf16[768,256]{1,0:T(8,128)(2,1)} %copy-done.7, bf16[768,256]{1,0:T(8,128)(2,1)} %copy-done.6, ...), custom_call_target="tpu_custom_call" | custom-call | flops 201326592 | tf_op jit(solution)/shard_map/pallas_call | solution.py:97
  81.9 19.8 %all_to_all.36 = bf16[16,104,256]{2,1,0:T(8,128)(2,1)S(1)} all-to-all(bf16[16,104,256]{2,1,0:T(8,128)(2,1)S(1)} %bitcast.21), channel_id=1, replica_groups=mesh['z'=8,'x'=4,'y'=4,'c'=2] {'x','y'}, dimensions={0} | all-to-all | bytes 1703936 | tf_op jit(solution)/shard_map/all_to_all | solution.py:17
  101.7 0.0 collective-permute-start.6
  101.7 2.4 %collective-permute-done.6 = bf16[16,104,256]{2,1,0:T(8,128)(2,1)S(1)} collective-permute-done((bf16[16,104,256]{2,1,0:T(8,128)(2,1)S(1)}, bf16[16,104,256]{2,1,0:T(8,128)(2,1)S(1)}, u32[]{:S(2)}, u32[]{:S(2)}) %collective-permute-start.6) | collective-permute-done | bytes 852000 | tf_op jit(solution)/shard_map/ppermute | solution.py:597
  104.1 0.0 copy-done.1
  104.1 0.0 copy-done.3
  104.1 0.0 copy-done.4
  104.1 1.6 %shard_map.228 = (bf16[4,5,24,512]{3,2,1,0:T(8,128)(2,1)S(1)}, bf16[96,128]{1,0:T(8,128)(2,1)S(1)}, bf16[4,24,128]{2,1,0:T(8,128)(2,1)S(1)}) custom-call(bf16[4,4,104,256]{3,2,1,0:T(8,128)(2,1)S(1)} %bitcast.20, bf16[4,4,104,256]{3,2,1,0:T(8,128)(2,1)S(1)} %bitcast.26, f32[1,4096]{1,0:T(1,128)} %bitcast.30, bf16[4096,128]{1,0:T(8,128)(2,1)S(1)} %bitcast.24, ...), custom_call_target="tpu_custom_call" | custom-call | flops 251658240 | tf_op jit(solution)/shard_map/pallas_call | solution.py:97
  105.7 0.2 collective-permute-start.7
  105.9 1.7 %collective-permute-done.7.refs_2_ = bf16[4,5,24,512]{3,2,1,0:T(8,128)(2,1)S(1)} collective-permute-done((bf16[4,5,24,512]{3,2,1,0:T(8,128)(2,1)S(1)}, bf16[4,5,24,512]{3,2,1,0:T(8,128)(2,1)S(1)}, u32[]{:S(2)}, u32[]{:S(2)}) %collective-permute-start.7) | collective-permute-done | bytes 491552 | tf_op jit(solution)/shard_map/ppermute | solution.py:615
  107.6 0.3 shard_map.229
  107.9 16.4 %all_to_all.37 = bf16[16,24,768]{2,1,0:T(8,128)(2,1)S(1)} all-to-all(bf16[16,24,768]{2,1,0:T(8,128)(2,1)S(1)} %bitcast.23), channel_id=1, replica_groups=mesh['z'=8,'x'=4,'y'=4,'c'=2] {'x','y'}, dimensions={0} | all-to-all | bytes 1179648 | tf_op jit(solution)/shard_map/all_to_all | solution.py:17
  124.3 1.5 %shard_map.230 = bf16[8,24,512]{2,1,0:T(8,128)(2,1)S(1)} custom-call(bf16[4,4,24,768]{3,2,1,0:T(8,128)(2,1)S(1)} %bitcast.22, f32[8,192]{1,0:T(8,128)} %get-tuple-element.21.refs_6_.refs_1_, bf16[768,256]{1,0:T(8,128)(2,1)} %copy-done.2, bf16[768,256]{1,0:T(8,128)(2,1)} %copy-done.8, bf16[768,256]{1,0:T(8,128)(2,1)} %copy-done.7, ...), custom_call_target="tpu_custom_call" | custom-call | flops 100663296 | tf_op jit(solution)/shard_map/pallas_call | solution.py:97
  125.8 12.2 %all_to_all.38.refs_0_ = bf16[8,24,512]{2,1,0:T(8,128)(2,1)S(1)} all-to-all(bf16[8,24,512]{2,1,0:T(8,128)(2,1)S(1)} %shard_map.230), channel_id=1, replica_groups=mesh['z'=8,'x'=4,'y'=4,'c'=2] {'z'}, dimensions={0} | all-to-all | bytes 393216 | tf_op jit(solution)/shard_map/all_to_all | solution.py:17
  137.9 0.6 shard_map.231
Async XLA Ops:
  3.7 21.3 %all-to-all-start = ((bf16[8,32,512]{2,1,0:T(8,128)(2,1)}), bf16[8,32,512]{2,1,0:T(8,128)(2,1)S(1)}, u32[]{:S(2)}, u32[]{:S(2)}) async-start(bf16[8,32,512]{2,1,0:T(8,128)(2,1)} %get-tuple-element.15.refs_0_), calls=%async_computation | async-start | bytes 524288 | tf_op jit(solution)/shard_map/all_to_all | solution.py:17
  12.2 8.0 %collective-permute-start.2 = (bf16[128,768]{1,0:T(8,128)(2,1)}, bf16[128,768]{1,0:T(8,128)(2,1)S(1)}, u32[]{:S(2)}, u32[]{:S(2)}) collective-permute-start(bf16[128,768]{1,0:T(8,128)(2,1)} %get-tuple-element.16.refs_1_), channel_id=1, source_target_pairs={{0,8},{8,16},{16,24},{24,0},{1,9},{9,17},{17,25},{25,1},{2,10},{10... | collective-permute-start | bytes 589832 | tf_op jit(solution)/shard_map/ppermute | solution.py:25
  13.7 9.5 %collective-permute-start.1 = (bf16[128,768]{1,0:T(8,128)(2,1)}, bf16[128,768]{1,0:T(8,128)(2,1)S(1)}, u32[]{:S(2)}, u32[]{:S(2)}) collective-permute-start(bf16[128,768]{1,0:T(8,128)(2,1)} %get-tuple-element.16.refs_1_), channel_id=1, source_target_pairs={{0,16},{8,24},{16,0},{24,8},{1,17},{9,25},{17,1},{25,9},{2,18},{10... | collective-permute-start | bytes 589832 | tf_op jit(solution)/shard_map/ppermute | solution.py:25
  14.8 10.2 %collective-permute-start = (bf16[128,768]{1,0:T(8,128)(2,1)}, bf16[128,768]{1,0:T(8,128)(2,1)S(1)}, u32[]{:S(2)}, u32[]{:S(2)}) collective-permute-start(bf16[128,768]{1,0:T(8,128)(2,1)} %get-tuple-element.16.refs_1_), channel_id=1, source_target_pairs={{0,24},{8,0},{16,8},{24,16},{1,25},{9,1},{17,9},{25,17},{2,26},{10... | collective-permute-start | bytes 589832 | tf_op jit(solution)/shard_map/ppermute | solution.py:25
  20.2 4.9 %copy-start.9 = (bf16[128,768]{1,0:T(8,128)(2,1)}, bf16[128,768]{1,0:T(8,128)(2,1)S(1)}, u32[]{:S(2)}) copy-start(bf16[128,768]{1,0:T(8,128)(2,1)S(1)} %collective-permute-done.2.refs_4_) | copy-start | bytes 589828
  23.2 1.9 %copy-start.10 = (bf16[128,768]{1,0:T(8,128)(2,1)}, bf16[128,768]{1,0:T(8,128)(2,1)S(1)}, u32[]{:S(2)}) copy-start(bf16[128,768]{1,0:T(8,128)(2,1)S(1)} %collective-permute-done.1.refs_3_) | copy-start | bytes 589828
  25.0 0.7 copy-start.11
  46.7 1.9 %copy-start = (f32[24,2,128,128]{3,2,1,0:T(8,128)S(1)}, f32[24,2,128,128]{3,2,1,0:T(8,128)}, u32[]{:S(2)}) copy-start(f32[24,2,128,128]{3,2,1,0:T(8,128)} %refs_3_.5) | copy-start | bytes 9437188
  48.6 14.1 %copy-start.5 = (bf16[24,4096]{1,0:T(8,128)(2,1)S(1)}, bf16[24,4096]{1,0:T(8,128)(2,1)}, u32[]{:S(2)}) copy-start(bf16[24,4096]{1,0:T(8,128)(2,1)} %refs_1_.2) | copy-start | bytes 589828
  51.5 11.3 %all-to-all-start.2 = ((bf16[8,24,512]{2,1,0:T(8,128)(2,1)}), bf16[8,24,512]{2,1,0:T(8,128)(2,1)S(1)}, u32[]{:S(2)}, u32[]{:S(2)}) async-start(bf16[8,24,512]{2,1,0:T(8,128)(2,1)} %get-tuple-element.19), calls=%async_computation.2 | async-start | bytes 393216 | tf_op jit(solution)/shard_map/all_to_all | solution.py:17
  57.0 14.1 %copy-start.2 = (bf16[768,256]{1,0:T(8,128)(2,1)}, bf16[768,256]{1,0:T(8,128)(2,1)S(1)}, u32[]{:S(2)}) copy-start(bf16[768,256]{1,0:T(8,128)(2,1)S(1)} %shard_map.225.refs_2_) | copy-start | bytes 1179652
  57.0 14.1 %collective-permute-start.5 = (bf16[768,256]{1,0:T(8,128)(2,1)S(1)}, bf16[768,256]{1,0:T(8,128)(2,1)S(1)}, u32[]{:S(2)}, u32[]{:S(2)}) collective-permute-start(bf16[768,256]{1,0:T(8,128)(2,1)S(1)} %shard_map.225.refs_2_), channel_id=1, source_target_pairs={{0,8},{8,16},{16,24},{24,0},{1,9},{9,17},{17,25},{25,1},{2,10},{10... | collective-permute-start | bytes 1179656 | tf_op jit(solution)/shard_map/ppermute | solution.py:25
  57.2 14.0 %collective-permute-start.4 = (bf16[768,256]{1,0:T(8,128)(2,1)S(1)}, bf16[768,256]{1,0:T(8,128)(2,1)S(1)}, u32[]{:S(2)}, u32[]{:S(2)}) collective-permute-start(bf16[768,256]{1,0:T(8,128)(2,1)S(1)} %shard_map.225.refs_2_), channel_id=1, source_target_pairs={{0,16},{8,24},{16,0},{24,8},{1,17},{9,25},{17,1},{25,9},{2,18},{10... | collective-permute-start | bytes 1179656 | tf_op jit(solution)/shard_map/ppermute | solution.py:25
  59.0 19.5 %collective-permute-start.3 = (bf16[768,256]{1,0:T(8,128)(2,1)S(1)}, bf16[768,256]{1,0:T(8,128)(2,1)S(1)}, u32[]{:S(2)}, u32[]{:S(2)}) collective-permute-start(bf16[768,256]{1,0:T(8,128)(2,1)S(1)} %shard_map.225.refs_2_), channel_id=1, source_target_pairs={{0,24},{8,0},{16,8},{24,16},{1,25},{9,1},{17,9},{25,17},{2,26},{10... | collective-permute-start | bytes 1179656 | tf_op jit(solution)/shard_map/ppermute | solution.py:25
  63.5 15.0 %all-to-all-start.3 = ((bf16[8,24,512]{2,1,0:T(8,128)(2,1)}), bf16[8,24,512]{2,1,0:T(8,128)(2,1)S(1)}, u32[]{:S(2)}, u32[]{:S(2)}) async-start(bf16[8,24,512]{2,1,0:T(8,128)(2,1)} %get-tuple-element.20), calls=%async_computation.3 | async-start | bytes 393216 | tf_op jit(solution)/shard_map/all_to_all | solution.py:17
  71.2 7.3 %copy-start.6 = (bf16[768,256]{1,0:T(8,128)(2,1)}, bf16[768,256]{1,0:T(8,128)(2,1)S(1)}, u32[]{:S(2)}) copy-start(bf16[768,256]{1,0:T(8,128)(2,1)S(1)} %collective-permute-done.5.refs_5_) | copy-start | bytes 1179652
  71.2 7.3 %copy-start.7 = (bf16[768,256]{1,0:T(8,128)(2,1)}, bf16[768,256]{1,0:T(8,128)(2,1)S(1)}, u32[]{:S(2)}) copy-start(bf16[768,256]{1,0:T(8,128)(2,1)S(1)} %collective-permute-done.4.refs_4_) | copy-start | bytes 1179652
  78.5 0.8 copy-start.8
  79.3 24.8 %copy-start.1 = (bf16[1,128,4096]{2,1,0:T(8,128)(2,1)S(1)}, bf16[1,128,4096]{2,1,0:T(8,128)(2,1)}, u32[]{:S(2)}) copy-start(bf16[1,128,4096]{2,1,0:T(8,128)(2,1)} %param.39) | copy-start | bytes 3145732
  79.3 24.8 %copy-start.3 = (bf16[1,4096,128]{2,1,0:T(8,128)(2,1)S(1)}, bf16[1,4096,128]{2,1,0:T(8,128)(2,1)}, u32[]{:S(2)}) copy-start(bf16[1,4096,128]{2,1,0:T(8,128)(2,1)} %param.37) | copy-start | bytes 3145732
  79.3 24.8 %copy-start.4 = (bf16[1,4096,128]{2,1,0:T(8,128)(2,1)S(1)}, bf16[1,4096,128]{2,1,0:T(8,128)(2,1)}, u32[]{:S(2)}) copy-start(bf16[1,4096,128]{2,1,0:T(8,128)(2,1)} %param.38) | copy-start | bytes 3145732
  101.7 2.4 %collective-permute-start.6 = (bf16[16,104,256]{2,1,0:T(8,128)(2,1)S(1)}, bf16[16,104,256]{2,1,0:T(8,128)(2,1)S(1)}, u32[]{:S(2)}, u32[]{:S(2)}) collective-permute-start(bf16[16,104,256]{2,1,0:T(8,128)(2,1)S(1)} %all_to_all.36), channel_id=1, source_target_pairs={{0,1},{1,0},{2,3},{3,2},{4,5},{5,4},{6,7},{7,6},{8,9},{9,8},{10,11... | collective-permute-start | bytes 2555912 | tf_op jit(solution)/shard_map/ppermute | solution.py:597
  105.7 2.0 %collective-permute-start.7 = (bf16[4,5,24,512]{3,2,1,0:T(8,128)(2,1)S(1)}, bf16[4,5,24,512]{3,2,1,0:T(8,128)(2,1)S(1)}, u32[]{:S(2)}, u32[]{:S(2)}) collective-permute-start(bf16[4,5,24,512]{3,2,1,0:T(8,128)(2,1)S(1)} %get-tuple-element.26), channel_id=1, source_target_pairs={{0,1},{1,0},{2,3},{3,2},{4,5},{5,4},{6,7},{7,6},{8,9},{9,8},{10,11... | collective-permute-start | bytes 1474568 | tf_op jit(solution)/shard_map/ppermute | solution.py:615

commit v7 on v6

--- a/solution.py
+++ b/solution.py
@@ -157,19 +157,20 @@
     factor_lane = lax.broadcasted_iota(jnp.int32, factors.shape, 1)
     table = jnp.where(factor_lane == 0, row_scale, 0.0)
 
-    def own_heads(weight):
-        product = lax.dot_general(gained, weight[...], over_width, preferred_element_type=F32)
-        lane = lax.broadcasted_iota(jnp.int32, product.shape, 1)
-        columns = []
-        for h in range(heads):
-            own = lane == index[2] * heads + h
-            columns.append(jnp.sum(jnp.where(own, product, 0.0), axis=1, keepdims=True) * row_scale)
-        return columns
-
-    for h, column in enumerate(own_heads(decay_weight)):
+    both = jnp.concatenate((decay_weight[...], beta_weight[...]), axis=0)
+    product = lax.dot_general(gained, both, over_width, preferred_element_type=F32)
+    product_lane = lax.broadcasted_iota(jnp.int32, product.shape, 1)
+
+    def own_head(place):
+        own = jnp.where(product_lane == place, product, 0.0)
+        return jnp.sum(own, axis=1, keepdims=True) * row_scale
+
+    for h in range(heads):
+        place = index[2] * heads + h
+        column = own_head(place)
         soft = jnp.maximum(column, 0.0) + jnp.log1p(jnp.exp(-jnp.abs(column)))
         table = jnp.where(factor_lane == 1 + h, jnp.exp(-rate[:, h : h + 1] * soft), table)
-    for h, column in enumerate(own_heads(beta_weight)):
+        column = own_head(decay_weight.shape[0] + place)
         table = jnp.where(factor_lane == 1 + heads + h, 1.0 / (1.0 + jnp.exp(-column)), table)
     factors[...] = table
 
@@ -206,13 +207,9 @@
         store.wait()
 
 
-def project_body(index, arrived, w0, w1, w2, w3, out, route):
+def project_body(index, arrived, w0, w1, w2, w3, out):
     groups, rows, _ = out.shape
     tokens = groups * rows
-    routing = arrived[0, rows:, :tokens].astype(F32)
-    for z in range(1, groups):
-        routing = routing + arrived[z, rows:, :tokens].astype(F32)
-    route[...] = routing
     total = None
     for step, weight in enumerate((w0, w1, w2, w3)):
         size = weight.shape[0]
@@ -262,8 +259,13 @@
         out[t] = jnp.dot(left, right, preferred_element_type=F32).astype(BF)
 
 
-def update_body(index, keys, changes, factors, state, new_state):
+def update_body(index, keys, changes, factors, state, spread, new_state, route):
     rows, heads, size = state.shape[:3]
+    tokens = route.shape[1]
+    routing = spread[0, :, :tokens].astype(F32)
+    for z in range(1, NZ):
+        routing = routing + spread[z, :, :tokens].astype(F32)
+    route[...] = routing
     line = lax.broadcasted_iota(jnp.int32, (rows, size), 0)
     line = jnp.concatenate((line, line, line), axis=0)
     for h in range(heads):
@@ -313,7 +315,7 @@
     return slots
 
 
-def dispatch_body(index, arrived, gain, g0, g1, g2, g3, route, after, out):
+def dispatch_body(index, arrived, gain, g0, g1, g2, g3, route, out):
     rows = arrived.shape[1]
     tokens = NZ * rows
     block = arrived.shape[2]
@@ -531,9 +533,9 @@
         far=(1, 2, 3),
     )
     dense_weights = from_neighbours(packed, "x")
-    part, route_rows = kernel(
+    (part,) = kernel(
         project_body,
-        (shape(NZ, rows, 3 * cols), pltpu.HBM((8, NZ * rows), F32)),
+        (shape(NZ, rows, 3 * cols),),
         spread,
         *qkv_weights,
         held=(1, 2, 3, 4),
@@ -555,14 +557,16 @@
         far=(1, 3, 4),
         flops=2 * rows * cols * width,
     )
-    (new_state,) = kernel(
+    new_state, route_rows = kernel(
         update_body,
-        (shape(*delta_state.shape, dtype=F32),),
+        (shape(*delta_state.shape, dtype=F32), pltpu.HBM((8, NZ * rows), F32)),
         keys,
         changes,
         factors,
         delta_state,
-        far=range(4),
+        spread,
+        far=range(5),
+        parts={4: ((NZ, 8, block), lambda ref, index: ref.at[:, rows:])},
         flops=10**8,
         limit=24,
     )
@@ -583,8 +587,6 @@
         ffn_gain[None],
         *dense_weights,
         route_rows,
-        new_state,
-        plain=(7,),
         far=range(1, 7),
         parts={
             1: ((1, block), own_block),

time: 139 us -> 137 us (0.986)
  waiting for transfers between devices: 20.9 us -> 18.8 us
    ppermute x6, waiting for transfers between devices: 15.4 us -> 13.2 us  [from_neighbours(): parts.append(lax.ppermute(shard, axis, pairs))]
  transfers between devices with their start and end apart: 11 -> 11, of which waited for: 7 -> 8; matrix products, arithmetic and copies ran while one was open for 0% -> 0% of each run, Pallas kernels for 4% -> 5%
where the time goes in v7:
time: 137 us; the launch traced here: 136 us
  blocking collectives  67.3 us (49%)
  starting transfers between devices  26.3 us (19%)
  Pallas kernels  20.6 us (15%)
  waiting for transfers between devices  18.8 us (14%)
  local copies, waits for them, and re-layouts  2.32 us (2%)
    all_to_all x4, blocking collectives, exchange(): return lax.all_to_all(tiles, axes, split_axis=0, concat_axis=0, tiled=True)  67.3 us
    pallas_call x11, Pallas kernels, kernel(): pl.pallas_call(run, out_shape=outs, in_specs=specs, out_specs=out_specs,...  20.6 us
    all_to_all x3, starting transfers between devices, exchange(): return lax.all_to_all(tiles, axes, split_axis=0, concat_axis=0, tiled=True)  17 us
    ppermute x6, waiting for transfers between devices, from_neighbours(): parts.append(lax.ppermute(shard, axis, pairs))  13.2 us
    ppermute x6, starting transfers between devices, from_neighbours(): parts.append(lax.ppermute(shard, axis, pairs))  9.08 us
  transfers between devices with their start and end apart: 11, of which 8 were waited for; matrix products, arithmetic and copies ran while one was open for 0% of the time, Pallas kernels for 5%

profile of v7, /device:TPU:2, one launch (start us, length us, event | category | flops | bytes accessed | tf_op | source)
XLA Modules:
  0.0 136.2 jit_solution(16318403170289945346)
XLA Ops:
  0.6 0.0 copy-start
  0.6 2.9 %shard_map.221 = (bf16[8,32,512]{2,1,0:T(8,128)(2,1)}, bf16[128,768]{1,0:T(8,128)(2,1)}, f32[24,128]{1,0:T(8,128)}) custom-call(bf16[24,4096]{1,0:T(8,128)(2,1)} %refs_1_.2, f32[1,4096]{1,0:T(1,128)} %bitcast.31, bf16[128,256]{1,0:T(8,128)(2,1)} %refs_2_.3, bf16[128,256]{1,0:T(8,128)(2,1)} %refs_3_.3, bf16[128,256]{1,0:T(8,128)(2,1)} %refs_4_.2, ...), custom_call_target="tpu_custom_call" | custom-call | tf_op jit(solution)/shard_map/pallas_call | solution.py:97
  3.5 8.5 %all-to-all-start = ((bf16[8,32,512]{2,1,0:T(8,128)(2,1)}), bf16[8,32,512]{2,1,0:T(8,128)(2,1)S(1)}, u32[]{:S(2)}, u32[]{:S(2)}) async-start(bf16[8,32,512]{2,1,0:T(8,128)(2,1)} %get-tuple-element.15.refs_0_), calls=%async_computation | async-start | bytes 524288 | tf_op jit(solution)/shard_map/all_to_all | solution.py:17
  12.0 1.5 %collective-permute-start.2 = (bf16[128,768]{1,0:T(8,128)(2,1)}, bf16[128,768]{1,0:T(8,128)(2,1)S(1)}, u32[]{:S(2)}, u32[]{:S(2)}) collective-permute-start(bf16[128,768]{1,0:T(8,128)(2,1)} %get-tuple-element.16.refs_1_), channel_id=1, source_target_pairs={{0,8},{8,16},{16,24},{24,0},{1,9},{9,17},{17,25},{25,1},{2,10},{10... | collective-permute-start | bytes 589832 | tf_op jit(solution)/shard_map/ppermute | solution.py:25
  13.5 1.1 collective-permute-start.1
  14.6 2.2 %collective-permute-start = (bf16[128,768]{1,0:T(8,128)(2,1)}, bf16[128,768]{1,0:T(8,128)(2,1)}, u32[]{:S(2)}, u32[]{:S(2)}) collective-permute-start(bf16[128,768]{1,0:T(8,128)(2,1)} %get-tuple-element.16.refs_1_), channel_id=1, source_target_pairs={{0,24},{8,0},{16,8},{24,16},{1,25},{9,1},{17,9},{25,17},{2,26},{10... | collective-permute-start | bytes 589832 | tf_op jit(solution)/shard_map/ppermute | solution.py:25
  16.8 3.2 %collective-permute-done.2.refs_4_ = bf16[128,768]{1,0:T(8,128)(2,1)S(1)} collective-permute-done((bf16[128,768]{1,0:T(8,128)(2,1)}, bf16[128,768]{1,0:T(8,128)(2,1)S(1)}, u32[]{:S(2)}, u32[]{:S(2)}) %collective-permute-start.2) | collective-permute-done | bytes 196640 | tf_op jit(solution)/shard_map/ppermute | solution.py:25
  20.0 0.0 copy-start.10
  20.0 3.0 %collective-permute-done.1.refs_3_ = bf16[128,768]{1,0:T(8,128)(2,1)S(1)} collective-permute-done((bf16[128,768]{1,0:T(8,128)(2,1)}, bf16[128,768]{1,0:T(8,128)(2,1)S(1)}, u32[]{:S(2)}, u32[]{:S(2)}) %collective-permute-start.1) | collective-permute-done | bytes 196640 | tf_op jit(solution)/shard_map/ppermute | solution.py:25
  23.0 0.0 copy-done.10
  23.0 0.0 copy-start.11
  23.0 0.7 copy-done.11
  23.7 1.3 collective-permute-done.refs_2_
  25.0 0.0 all-to-all-done.refs_0_.refs_4_
  25.0 0.0 copy-start.3
  25.0 1.8 %shard_map.222 = bf16[8,24,768]{2,1,0:T(8,128)(2,1)S(1)} custom-call(bf16[8,32,512]{2,1,0:T(8,128)(2,1)S(1)} %all-to-all-done.refs_0_.refs_4_, bf16[128,768]{1,0:T(8,128)(2,1)} %get-tuple-element.16.refs_1_, bf16[128,768]{1,0:T(8,128)(2,1)} %collective-permute-done.refs_2_, bf16[128,768]{1,0:T(8,128)(2,1)} %copy-done.11, bf16[128,768]{1,0:T(8,128)(2,1)} %copy-done.10), custom_call_target="tpu_custom_call" | custom-call | flops 150994944 | tf_op jit(solution)/shard_map/pallas_call | solution.py:97
  26.7 18.8 %all_to_all.35.refs_0_ = bf16[8,24,768]{2,1,0:T(8,128)(2,1)S(1)} all-to-all(bf16[8,24,768]{2,1,0:T(8,128)(2,1)S(1)} %shard_map.222), channel_id=1, replica_groups=mesh['z'=8,'x'=4,'y'=4,'c'=2] {'z'}, dimensions={0} | all-to-all | bytes 589824 | tf_op jit(solution)/shard_map/all_to_all | solution.py:17
  45.5 0.0 copy-done
  45.5 2.3 %shard_map.223 = (bf16[8,24,512]{2,1,0:T(8,128)(2,1)S(1)}, f32[24,256]{1,0:T(8,128)}, f32[24,256]{1,0:T(8,128)}) custom-call(bf16[8,24,768]{2,1,0:T(8,128)(2,1)S(1)} %all_to_all.35.refs_0_, f32[24,128]{1,0:T(8,128)} %get-tuple-element.17.refs_1_.refs_2_, f32[24,2,128,128]{3,2,1,0:T(8,128)S(1)} %copy-done, f32[1,128]{1,0:T(1,128)} %bitcast.35, ...), custom_call_target="tpu_custom_call" | custom-call | flops 50331648 | tf_op jit(solution)/shard_map/pallas_call | solution.py:97
  47.8 0.0 copy-done.3
  47.8 0.0 copy-start.7
  47.8 0.7 copy-done.7
  48.5 4.5 %all-to-all-start.2 = ((bf16[8,24,512]{2,1,0:T(8,128)(2,1)}), bf16[8,24,512]{2,1,0:T(8,128)(2,1)S(1)}, u32[]{:S(2)}, u32[]{:S(2)}) async-start(bf16[8,24,512]{2,1,0:T(8,128)(2,1)} %copy-done.7), calls=%async_computation.2 | async-start | bytes 393216 | tf_op jit(solution)/shard_map/all_to_all | solution.py:17
  53.0 1.1 shard_map.225.refs_2_
  54.1 0.0 copy-start.2
  54.1 0.2 collective-permute-start.5
  54.3 2.3 %collective-permute-start.4 = (bf16[768,256]{1,0:T(8,128)(2,1)S(1)}, bf16[768,256]{1,0:T(8,128)(2,1)}, u32[]{:S(2)}, u32[]{:S(2)}) collective-permute-start(bf16[768,256]{1,0:T(8,128)(2,1)S(1)} %shard_map.225.refs_2_), channel_id=1, source_target_pairs={{0,16},{8,24},{16,0},{24,8},{1,17},{9,25},{17,1},{25,9},{2,18},{10... | collective-permute-start | bytes 1179656 | tf_op jit(solution)/shard_map/ppermute | solution.py:25
  56.6 1.8 %collective-permute-start.3 = (bf16[768,256]{1,0:T(8,128)(2,1)S(1)}, bf16[768,256]{1,0:T(8,128)(2,1)}, u32[]{:S(2)}, u32[]{:S(2)}) collective-permute-start(bf16[768,256]{1,0:T(8,128)(2,1)S(1)} %shard_map.225.refs_2_), channel_id=1, source_target_pairs={{0,24},{8,0},{16,8},{24,16},{1,25},{9,1},{17,9},{25,17},{2,26},{10... | collective-permute-start | bytes 1179656 | tf_op jit(solution)/shard_map/ppermute | solution.py:25
  58.4 1.4 %all-to-all-done.2.refs_0_ = bf16[8,24,512]{2,1,0:T(8,128)(2,1)S(1)} async-done(((bf16[8,24,512]{2,1,0:T(8,128)(2,1)}), bf16[8,24,512]{2,1,0:T(8,128)(2,1)S(1)}, u32[]{:S(2)}, u32[]{:S(2)}) %all-to-all-start.2) | async-done | bytes 196640 | tf_op jit(solution)/shard_map/all_to_all | solution.py:17
  59.8 0.0 copy-start.6
  59.8 0.9 copy-done.6
  60.7 0.7 shard_map.224
  61.4 0.0 copy-start.8
  61.4 4.0 %all-to-all-start.3 = ((bf16[8,24,512]{2,1,0:T(8,128)(2,1)}), bf16[8,24,512]{2,1,0:T(8,128)(2,1)}, u32[]{:S(2)}, u32[]{:S(2)}) async-start(bf16[8,24,512]{2,1,0:T(8,128)(2,1)} %get-tuple-element.19), calls=%async_computation.3 | async-start | bytes 393216 | tf_op jit(solution)/shard_map/all_to_all | solution.py:17
  65.5 0.0 copy-done.8
  65.5 0.0 copy-start.1
  65.5 0.0 copy-start.4
  65.5 0.0 copy-start.5
  65.5 4.5 %shard_map.226 = (f32[24,2,128,128]{3,2,1,0:T(8,128)}, f32[8,192]{1,0:T(8,128)}) custom-call(f32[24,256]{1,0:T(8,128)} %get-tuple-element.20.refs_0_, f32[24,256]{1,0:T(8,128)} %get-tuple-element.21.refs_1_, f32[24,128]{1,0:T(8,128)} %get-tuple-element.17.refs_1_.refs_2_, f32[24,2,128,128]{3,2,1,0:T(8,128)} %refs_3_.5, bf16[8,32,512]{2,1,0:T(8,128)(2,1)} %copy-done.3), custom_call_target="tpu_custom_call" | custom-call | flops 100000000 | tf_op jit(solution)/shard_map/pallas_call | solution.py:97
  70.1 0.0 collective-permute-done.5.refs_5_
  70.1 0.0 collective-permute-done.4.refs_4_
  70.1 5.7 %collective-permute-done.3.refs_3_ = bf16[768,256]{1,0:T(8,128)(2,1)} collective-permute-done((bf16[768,256]{1,0:T(8,128)(2,1)S(1)}, bf16[768,256]{1,0:T(8,128)(2,1)}, u32[]{:S(2)}, u32[]{:S(2)}) %collective-permute-start.3) | collective-permute-done | bytes 393248 | tf_op jit(solution)/shard_map/ppermute | solution.py:25
  75.8 0.1 all-to-all-done.3.refs_0_
  75.9 0.0 copy-done.2
  75.9 3.4 %shard_map.227 = bf16[4,4,104,256]{3,2,1,0:T(8,128)(2,1)S(1)} custom-call(bf16[8,24,512]{2,1,0:T(8,128)(2,1)} %all-to-all-done.3.refs_0_, f32[1,4096]{1,0:T(1,128)} %bitcast.29, bf16[768,256]{1,0:T(8,128)(2,1)} %copy-done.2, bf16[768,256]{1,0:T(8,128)(2,1)} %collective-permute-done.3.refs_3_, bf16[768,256]{1,0:T(8,128)(2,1)} %collective-permute-done.4.refs_4_, ...), custom_call_target="tpu_custom_call" | custom-call | flops 201326592 | tf_op jit(solution)/shard_map/pallas_call | solution.py:97
  79.4 19.9 %all_to_all.36 = bf16[16,104,256]{2,1,0:T(8,128)(2,1)S(1)} all-to-all(bf16[16,104,256]{2,1,0:T(8,128)(2,1)S(1)} %bitcast.21), channel_id=1, replica_groups=mesh['z'=8,'x'=4,'y'=4,'c'=2] {'x','y'}, dimensions={0} | all-to-all | bytes 1703936 | tf_op jit(solution)/shard_map/all_to_all | solution.py:17
  99.3 0.0 collective-permute-start.6
  99.3 2.4 %collective-permute-done.6 = bf16[16,104,256]{2,1,0:T(8,128)(2,1)S(1)} collective-permute-done((bf16[16,104,256]{2,1,0:T(8,128)(2,1)S(1)}, bf16[16,104,256]{2,1,0:T(8,128)(2,1)S(1)}, u32[]{:S(2)}, u32[]{:S(2)}) %collective-permute-start.6) | collective-permute-done | bytes 852000 | tf_op jit(solution)/shard_map/ppermute | solution.py:599
  101.7 0.0 copy-done.1
  101.7 0.0 copy-done.4
  101.7 0.0 copy-done.5
  101.7 1.6 %shard_map.228 = (bf16[4,5,24,512]{3,2,1,0:T(8,128)(2,1)S(1)}, bf16[96,128]{1,0:T(8,128)(2,1)S(1)}, bf16[4,24,128]{2,1,0:T(8,128)(2,1)S(1)}) custom-call(bf16[4,4,104,256]{3,2,1,0:T(8,128)(2,1)S(1)} %bitcast.20, bf16[4,4,104,256]{3,2,1,0:T(8,128)(2,1)S(1)} %bitcast.26, f32[1,4096]{1,0:T(1,128)} %bitcast.30, bf16[4096,128]{1,0:T(8,128)(2,1)S(1)} %bitcast.24, ...), custom_call_target="tpu_custom_call" | custom-call | flops 251658240 | tf_op jit(solution)/shard_map/pallas_call | solution.py:97
  103.2 0.0 copy-start.9
  103.3 0.2 collective-permute-start.7
  103.5 1.7 %collective-permute-done.7.refs_2_ = bf16[4,5,24,512]{3,2,1,0:T(8,128)(2,1)S(1)} collective-permute-done((bf16[4,5,24,512]{3,2,1,0:T(8,128)(2,1)S(1)}, bf16[4,5,24,512]{3,2,1,0:T(8,128)(2,1)S(1)}, u32[]{:S(2)}, u32[]{:S(2)}) %collective-permute-start.7) | collective-permute-done | bytes 491552 | tf_op jit(solution)/shard_map/ppermute | solution.py:617
  105.2 0.3 shard_map.229
  105.5 16.4 %all_to_all.37 = bf16[16,24,768]{2,1,0:T(8,128)(2,1)S(1)} all-to-all(bf16[16,24,768]{2,1,0:T(8,128)(2,1)S(1)} %bitcast.23), channel_id=1, replica_groups=mesh['z'=8,'x'=4,'y'=4,'c'=2] {'x','y'}, dimensions={0} | all-to-all | bytes 1179648 | tf_op jit(solution)/shard_map/all_to_all | solution.py:17
  121.9 1.5 %shard_map.230 = bf16[8,24,512]{2,1,0:T(8,128)(2,1)S(1)} custom-call(bf16[4,4,24,768]{3,2,1,0:T(8,128)(2,1)S(1)} %bitcast.22, f32[8,192]{1,0:T(8,128)} %get-tuple-element.22.refs_6_.refs_1_, bf16[768,256]{1,0:T(8,128)(2,1)} %copy-done.2, bf16[768,256]{1,0:T(8,128)(2,1)} %collective-permute-done.3.refs_3_, bf16[768,256]{1,0:T(8,128)(2,1)} %collective-permute-done.4.refs_4_, ...), custom_call_target="tpu_custom_call" | custom-call | flops 100663296 | tf_op jit(solution)/shard_map/pallas_call | solution.py:97
  123.4 12.2 %all_to_all.38.refs_0_ = bf16[8,24,512]{2,1,0:T(8,128)(2,1)S(1)} all-to-all(bf16[8,24,512]{2,1,0:T(8,128)(2,1)S(1)} %shard_map.230), channel_id=1, replica_groups=mesh['z'=8,'x'=4,'y'=4,'c'=2] {'z'}, dimensions={0} | all-to-all | bytes 393216 | tf_op jit(solution)/shard_map/all_to_all | solution.py:17
  135.5 0.0 copy-done.9
  135.5 0.6 shard_map.231
Async XLA Ops:
  0.6 44.9 %copy-start = (f32[24,2,128,128]{3,2,1,0:T(8,128)S(1)}, f32[24,2,128,128]{3,2,1,0:T(8,128)}, u32[]{:S(2)}) copy-start(f32[24,2,128,128]{3,2,1,0:T(8,128)} %refs_3_.5) | copy-start | bytes 9437188
  3.5 21.4 %all-to-all-start = ((bf16[8,32,512]{2,1,0:T(8,128)(2,1)}), bf16[8,32,512]{2,1,0:T(8,128)(2,1)S(1)}, u32[]{:S(2)}, u32[]{:S(2)}) async-start(bf16[8,32,512]{2,1,0:T(8,128)(2,1)} %get-tuple-element.15.refs_0_), calls=%async_computation | async-start | bytes 524288 | tf_op jit(solution)/shard_map/all_to_all | solution.py:17
  12.0 8.0 %collective-permute-start.2 = (bf16[128,768]{1,0:T(8,128)(2,1)}, bf16[128,768]{1,0:T(8,128)(2,1)S(1)}, u32[]{:S(2)}, u32[]{:S(2)}) collective-permute-start(bf16[128,768]{1,0:T(8,128)(2,1)} %get-tuple-element.16.refs_1_), channel_id=1, source_target_pairs={{0,8},{8,16},{16,24},{24,0},{1,9},{9,17},{17,25},{25,1},{2,10},{10... | collective-permute-start | bytes 589832 | tf_op jit(solution)/shard_map/ppermute | solution.py:25
  13.5 9.5 %collective-permute-start.1 = (bf16[128,768]{1,0:T(8,128)(2,1)}, bf16[128,768]{1,0:T(8,128)(2,1)S(1)}, u32[]{:S(2)}, u32[]{:S(2)}) collective-permute-start(bf16[128,768]{1,0:T(8,128)(2,1)} %get-tuple-element.16.refs_1_), channel_id=1, source_target_pairs={{0,16},{8,24},{16,0},{24,8},{1,17},{9,25},{17,1},{25,9},{2,18},{10... | collective-permute-start | bytes 589832 | tf_op jit(solution)/shard_map/ppermute | solution.py:25
  14.6 10.3 %collective-permute-start = (bf16[128,768]{1,0:T(8,128)(2,1)}, bf16[128,768]{1,0:T(8,128)(2,1)}, u32[]{:S(2)}, u32[]{:S(2)}) collective-permute-start(bf16[128,768]{1,0:T(8,128)(2,1)} %get-tuple-element.16.refs_1_), channel_id=1, source_target_pairs={{0,24},{8,0},{16,8},{24,16},{1,25},{9,1},{17,9},{25,17},{2,26},{10... | collective-permute-start | bytes 589832 | tf_op jit(solution)/shard_map/ppermute | solution.py:25
  20.0 3.0 %copy-start.10 = (bf16[128,768]{1,0:T(8,128)(2,1)}, bf16[128,768]{1,0:T(8,128)(2,1)S(1)}, u32[]{:S(2)}) copy-start(bf16[128,768]{1,0:T(8,128)(2,1)S(1)} %collective-permute-done.2.refs_4_) | copy-start | bytes 589828
  23.0 0.7 copy-start.11
  25.0 22.9 %copy-start.3 = (bf16[8,32,512]{2,1,0:T(8,128)(2,1)}, bf16[8,32,512]{2,1,0:T(8,128)(2,1)S(1)}, u32[]{:S(2)}) copy-start(bf16[8,32,512]{2,1,0:T(8,128)(2,1)S(1)} %all-to-all-done.refs_0_.refs_4_) | copy-start | bytes 786436
  47.8 0.7 copy-start.7
  48.5 11.3 %all-to-all-start.2 = ((bf16[8,24,512]{2,1,0:T(8,128)(2,1)}), bf16[8,24,512]{2,1,0:T(8,128)(2,1)S(1)}, u32[]{:S(2)}, u32[]{:S(2)}) async-start(bf16[8,24,512]{2,1,0:T(8,128)(2,1)} %copy-done.7), calls=%async_computation.2 | async-start | bytes 393216 | tf_op jit(solution)/shard_map/all_to_all | solution.py:17
  54.1 21.9 %copy-start.2 = (bf16[768,256]{1,0:T(8,128)(2,1)}, bf16[768,256]{1,0:T(8,128)(2,1)S(1)}, u32[]{:S(2)}) copy-start(bf16[768,256]{1,0:T(8,128)(2,1)S(1)} %shard_map.225.refs_2_) | copy-start | bytes 1179652
  54.1 16.0 %collective-permute-start.5 = (bf16[768,256]{1,0:T(8,128)(2,1)S(1)}, bf16[768,256]{1,0:T(8,128)(2,1)}, u32[]{:S(2)}, u32[]{:S(2)}) collective-permute-start(bf16[768,256]{1,0:T(8,128)(2,1)S(1)} %shard_map.225.refs_2_), channel_id=1, source_target_pairs={{0,8},{8,16},{16,24},{24,0},{1,9},{9,17},{17,25},{25,1},{2,10},{10... | collective-permute-start | bytes 1179656 | tf_op jit(solution)/shard_map/ppermute | solution.py:25
  54.3 15.8 %collective-permute-start.4 = (bf16[768,256]{1,0:T(8,128)(2,1)S(1)}, bf16[768,256]{1,0:T(8,128)(2,1)}, u32[]{:S(2)}, u32[]{:S(2)}) collective-permute-start(bf16[768,256]{1,0:T(8,128)(2,1)S(1)} %shard_map.225.refs_2_), channel_id=1, source_target_pairs={{0,16},{8,24},{16,0},{24,8},{1,17},{9,25},{17,1},{25,9},{2,18},{10... | collective-permute-start | bytes 1179656 | tf_op jit(solution)/shard_map/ppermute | solution.py:25
  56.6 19.2 %collective-permute-start.3 = (bf16[768,256]{1,0:T(8,128)(2,1)S(1)}, bf16[768,256]{1,0:T(8,128)(2,1)}, u32[]{:S(2)}, u32[]{:S(2)}) collective-permute-start(bf16[768,256]{1,0:T(8,128)(2,1)S(1)} %shard_map.225.refs_2_), channel_id=1, source_target_pairs={{0,24},{8,0},{16,8},{24,16},{1,25},{9,1},{17,9},{25,17},{2,26},{10... | collective-permute-start | bytes 1179656 | tf_op jit(solution)/shard_map/ppermute | solution.py:25
  59.8 0.9 copy-start.6
  61.4 4.0 %copy-start.8 = (f32[24,512]{1,0:T(8,128)}, f32[24,512]{1,0:T(8,128)S(1)}, u32[]{:S(2)}) copy-start(f32[24,512]{1,0:T(8,128)S(1)} %get-tuple-element.26.refs_1_) | copy-start | bytes 147460
  61.4 14.5 %all-to-all-start.3 = ((bf16[8,24,512]{2,1,0:T(8,128)(2,1)}), bf16[8,24,512]{2,1,0:T(8,128)(2,1)}, u32[]{:S(2)}, u32[]{:S(2)}) async-start(bf16[8,24,512]{2,1,0:T(8,128)(2,1)} %get-tuple-element.19), calls=%async_computation.3 | async-start | bytes 393216 | tf_op jit(solution)/shard_map/all_to_all | solution.py:17
  65.5 36.2 %copy-start.1 = (bf16[1,128,4096]{2,1,0:T(8,128)(2,1)S(1)}, bf16[1,128,4096]{2,1,0:T(8,128)(2,1)}, u32[]{:S(2)}) copy-start(bf16[1,128,4096]{2,1,0:T(8,128)(2,1)} %param.39) | copy-start | bytes 3145732
  65.5 36.2 %copy-start.4 = (bf16[1,4096,128]{2,1,0:T(8,128)(2,1)S(1)}, bf16[1,4096,128]{2,1,0:T(8,128)(2,1)}, u32[]{:S(2)}) copy-start(bf16[1,4096,128]{2,1,0:T(8,128)(2,1)} %param.37) | copy-start | bytes 3145732
  65.5 36.2 %copy-start.5 = (bf16[1,4096,128]{2,1,0:T(8,128)(2,1)S(1)}, bf16[1,4096,128]{2,1,0:T(8,128)(2,1)}, u32[]{:S(2)}) copy-start(bf16[1,4096,128]{2,1,0:T(8,128)(2,1)} %param.38) | copy-start | bytes 3145732
  99.3 2.4 %collective-permute-start.6 = (bf16[16,104,256]{2,1,0:T(8,128)(2,1)S(1)}, bf16[16,104,256]{2,1,0:T(8,128)(2,1)S(1)}, u32[]{:S(2)}, u32[]{:S(2)}) collective-permute-start(bf16[16,104,256]{2,1,0:T(8,128)(2,1)S(1)} %all_to_all.36), channel_id=1, source_target_pairs={{0,1},{1,0},{2,3},{3,2},{4,5},{5,4},{6,7},{7,6},{8,9},{9,8},{10,11... | collective-permute-start | bytes 2555912 | tf_op jit(solution)/shard_map/ppermute | solution.py:599
  103.2 32.3 %copy-start.9 = (f32[24,512]{1,0:T(8,128)S(1)}, f32[24,512]{1,0:T(8,128)}, u32[]{:S(2)}) copy-start(f32[24,512]{1,0:T(8,128)} %copy-done.8) | copy-start | bytes 147460
  103.3 2.0 %collective-permute-start.7 = (bf16[4,5,24,512]{3,2,1,0:T(8,128)(2,1)S(1)}, bf16[4,5,24,512]{3,2,1,0:T(8,128)(2,1)S(1)}, u32[]{:S(2)}, u32[]{:S(2)}) collective-permute-start(bf16[4,5,24,512]{3,2,1,0:T(8,128)(2,1)S(1)} %get-tuple-element.25), channel_id=1, source_target_pairs={{0,1},{1,0},{2,3},{3,2},{4,5},{5,4},{6,7},{7,6},{8,9},{9,8},{10,11... | collective-permute-start | bytes 1474568 | tf_op jit(solution)/shard_map/ppermute | solution.py:617

commit v8 on v7

--- a/solution.py
+++ b/solution.py
@@ -227,23 +227,29 @@
     for z in range(1, NZ):
         summed = summed + arrived[z].astype(F32)
     summed = summed * factors[:, 0:1]
-    line = lax.broadcasted_iota(jnp.int32, (rows, size), 0)
+    line = lax.broadcasted_iota(jnp.int32, (8, size), 0)
     head_rows = []
     for h in range(heads):
         own = slice(h * size, (h + 1) * size)
         query = unit_rows(summed[:, own]) * size ** (-0.5)
         key = unit_rows(summed[:, cols + h * size : cols + (h + 1) * size])
         value = summed[:, 2 * cols + h * size : 2 * cols + (h + 1) * size]
-        both = jnp.concatenate((key, query), axis=0).astype(BF)
-        recalled = jnp.zeros((rows, size), F32)
-        asked = jnp.zeros((rows, size), F32)
-        for b in range(0, rows, 2):
-            pair = jnp.concatenate((state[b, h], state[b + 1, h]), axis=1).astype(BF)
-            product = jnp.dot(both, pair, preferred_element_type=F32)
-            for side in range(2):
-                lanes = slice(side * size, (side + 1) * size)
-                recalled = jnp.where(line == b + side, product[:rows, lanes], recalled)
-                asked = jnp.where(line == b + side, product[rows:, lanes], asked)
+        groups = []
+        for first in range(0, rows, 8):
+            some = slice(first, first + 8)
+            both = jnp.concatenate((key[some], query[some]), axis=0).astype(BF)
+            recalled = jnp.zeros((8, size), F32)
+            asked = jnp.zeros((8, size), F32)
+            for b in range(0, 8, 2):
+                pair = (state[first + b, h], state[first + b + 1, h])
+                pair = jnp.concatenate(pair, axis=1).astype(BF)
+                product = jnp.dot(both, pair, preferred_element_type=F32)
+                for side in range(2):
+                    lanes = slice(side * size, (side + 1) * size)
+                    recalled = jnp.where(line == b + side, product[:8, lanes], recalled)
+                    asked = jnp.where(line == b + side, product[8:, lanes], asked)
+            groups.append((recalled, asked))
+        recalled, asked = (jnp.concatenate(part, axis=0) for part in zip(*groups))
         fade = factors[:, 1 + h : 2 + h]
         gate = factors[:, 1 + heads + h : 2 + heads + h]
         change = gate * (value - fade * recalled)

time: 137 us -> 137 us (level)
  no operation moved by 1% of the time
where the time goes in v8:
time: 137 us; the launch traced here: 136 us
  blocking collectives  67.3 us (49%)
  starting transfers between devices  26.3 us (19%)
  Pallas kernels  20.6 us (15%)
  waiting for transfers between devices  18.8 us (14%)
  local copies, waits for them, and re-layouts  2.32 us (2%)
    all_to_all x4, blocking collectives, exchange(): return lax.all_to_all(tiles, axes, split_axis=0, concat_axis=0, tiled=True)  67.3 us
    pallas_call x11, Pallas kernels, kernel(): pl.pallas_call(run, out_shape=outs, in_specs=specs, out_specs=out_specs,...  20.6 us
    all_to_all x3, starting transfers between devices, exchange(): return lax.all_to_all(tiles, axes, split_axis=0, concat_axis=0, tiled=True)  17 us
    ppermute x6, waiting for transfers between devices, from_neighbours(): parts.append(lax.ppermute(shard, axis, pairs))  13.2 us
    ppermute x6, starting transfers between devices, from_neighbours(): parts.append(lax.ppermute(shard, axis, pairs))  9.08 us
  transfers between devices with their start and end apart: 11, of which 8 were waited for; matrix products, arithmetic and copies ran while one was open for 0% of the time, Pallas kernels for 5%

profile of v8, /device:TPU:2, one launch (start us, length us, event | category | flops | bytes accessed | tf_op | source)
XLA Modules:
  0.0 136.2 jit_solution(3001631833987111593)
XLA Ops:
  0.6 0.0 copy-start
  0.6 2.9 %shard_map.221 = (bf16[8,32,512]{2,1,0:T(8,128)(2,1)}, bf16[128,768]{1,0:T(8,128)(2,1)}, f32[24,128]{1,0:T(8,128)}) custom-call(bf16[24,4096]{1,0:T(8,128)(2,1)} %refs_1_.2, f32[1,4096]{1,0:T(1,128)} %bitcast.31, bf16[128,256]{1,0:T(8,128)(2,1)} %refs_2_.3, bf16[128,256]{1,0:T(8,128)(2,1)} %refs_3_.3, bf16[128,256]{1,0:T(8,128)(2,1)} %refs_4_.2, ...), custom_call_target="tpu_custom_call" | custom-call | tf_op jit(solution)/shard_map/pallas_call | solution.py:97
  3.5 8.5 %all-to-all-start = ((bf16[8,32,512]{2,1,0:T(8,128)(2,1)}), bf16[8,32,512]{2,1,0:T(8,128)(2,1)S(1)}, u32[]{:S(2)}, u32[]{:S(2)}) async-start(bf16[8,32,512]{2,1,0:T(8,128)(2,1)} %get-tuple-element.15.refs_0_), calls=%async_computation | async-start | bytes 524288 | tf_op jit(solution)/shard_map/all_to_all | solution.py:17
  12.0 1.5 %collective-permute-start.2 = (bf16[128,768]{1,0:T(8,128)(2,1)}, bf16[128,768]{1,0:T(8,128)(2,1)S(1)}, u32[]{:S(2)}, u32[]{:S(2)}) collective-permute-start(bf16[128,768]{1,0:T(8,128)(2,1)} %get-tuple-element.16.refs_1_), channel_id=1, source_target_pairs={{0,8},{8,16},{16,24},{24,0},{1,9},{9,17},{17,25},{25,1},{2,10},{10... | collective-permute-start | bytes 589832 | tf_op jit(solution)/shard_map/ppermute | solution.py:25
  13.5 1.1 collective-permute-start.1
  14.6 2.2 %collective-permute-start = (bf16[128,768]{1,0:T(8,128)(2,1)}, bf16[128,768]{1,0:T(8,128)(2,1)}, u32[]{:S(2)}, u32[]{:S(2)}) collective-permute-start(bf16[128,768]{1,0:T(8,128)(2,1)} %get-tuple-element.16.refs_1_), channel_id=1, source_target_pairs={{0,24},{8,0},{16,8},{24,16},{1,25},{9,1},{17,9},{25,17},{2,26},{10... | collective-permute-start | bytes 589832 | tf_op jit(solution)/shard_map/ppermute | solution.py:25
  16.8 3.2 %collective-permute-done.2.refs_4_ = bf16[128,768]{1,0:T(8,128)(2,1)S(1)} collective-permute-done((bf16[128,768]{1,0:T(8,128)(2,1)}, bf16[128,768]{1,0:T(8,128)(2,1)S(1)}, u32[]{:S(2)}, u32[]{:S(2)}) %collective-permute-start.2) | collective-permute-done | bytes 196640 | tf_op jit(solution)/shard_map/ppermute | solution.py:25
  20.0 0.0 copy-start.10
  20.0 3.0 %collective-permute-done.1.refs_3_ = bf16[128,768]{1,0:T(8,128)(2,1)S(1)} collective-permute-done((bf16[128,768]{1,0:T(8,128)(2,1)}, bf16[128,768]{1,0:T(8,128)(2,1)S(1)}, u32[]{:S(2)}, u32[]{:S(2)}) %collective-permute-start.1) | collective-permute-done | bytes 196640 | tf_op jit(solution)/shard_map/ppermute | solution.py:25
  23.0 0.0 copy-done.10
  23.0 0.0 copy-start.11
  23.0 0.7 copy-done.11
  23.7 1.3 collective-permute-done.refs_2_
  25.0 0.0 all-to-all-done.refs_0_.refs_4_
  25.0 0.0 copy-start.3
  25.0 1.8 %shard_map.222 = bf16[8,24,768]{2,1,0:T(8,128)(2,1)S(1)} custom-call(bf16[8,32,512]{2,1,0:T(8,128)(2,1)S(1)} %all-to-all-done.refs_0_.refs_4_, bf16[128,768]{1,0:T(8,128)(2,1)} %get-tuple-element.16.refs_1_, bf16[128,768]{1,0:T(8,128)(2,1)} %collective-permute-done.refs_2_, bf16[128,768]{1,0:T(8,128)(2,1)} %copy-done.11, bf16[128,768]{1,0:T(8,128)(2,1)} %copy-done.10), custom_call_target="tpu_custom_call" | custom-call | flops 150994944 | tf_op jit(solution)/shard_map/pallas_call | solution.py:97
  26.7 18.8 %all_to_all.35.refs_0_ = bf16[8,24,768]{2,1,0:T(8,128)(2,1)S(1)} all-to-all(bf16[8,24,768]{2,1,0:T(8,128)(2,1)S(1)} %shard_map.222), channel_id=1, replica_groups=mesh['z'=8,'x'=4,'y'=4,'c'=2] {'z'}, dimensions={0} | all-to-all | bytes 589824 | tf_op jit(solution)/shard_map/all_to_all | solution.py:17
  45.5 0.0 copy-done
  45.5 2.3 %shard_map.223 = (bf16[8,24,512]{2,1,0:T(8,128)(2,1)S(1)}, f32[24,256]{1,0:T(8,128)}, f32[24,256]{1,0:T(8,128)}) custom-call(bf16[8,24,768]{2,1,0:T(8,128)(2,1)S(1)} %all_to_all.35.refs_0_, f32[24,128]{1,0:T(8,128)} %get-tuple-element.17.refs_1_.refs_2_, f32[24,2,128,128]{3,2,1,0:T(8,128)S(1)} %copy-done, f32[1,128]{1,0:T(1,128)} %bitcast.35, ...), custom_call_target="tpu_custom_call" | custom-call | flops 50331648 | tf_op jit(solution)/shard_map/pallas_call | solution.py:97
  47.8 0.0 copy-done.3
  47.8 0.0 copy-start.7
  47.8 0.7 copy-done.7
  48.5 4.5 %all-to-all-start.2 = ((bf16[8,24,512]{2,1,0:T(8,128)(2,1)}), bf16[8,24,512]{2,1,0:T(8,128)(2,1)S(1)}, u32[]{:S(2)}, u32[]{:S(2)}) async-start(bf16[8,24,512]{2,1,0:T(8,128)(2,1)} %copy-done.7), calls=%async_computation.2 | async-start | bytes 393216 | tf_op jit(solution)/shard_map/all_to_all | solution.py:17
  53.0 1.1 shard_map.225.refs_2_
  54.1 0.0 copy-start.2
  54.1 0.2 collective-permute-start.5
  54.3 2.3 %collective-permute-start.4 = (bf16[768,256]{1,0:T(8,128)(2,1)S(1)}, bf16[768,256]{1,0:T(8,128)(2,1)}, u32[]{:S(2)}, u32[]{:S(2)}) collective-permute-start(bf16[768,256]{1,0:T(8,128)(2,1)S(1)} %shard_map.225.refs_2_), channel_id=1, source_target_pairs={{0,16},{8,24},{16,0},{24,8},{1,17},{9,25},{17,1},{25,9},{2,18},{10... | collective-permute-start | bytes 1179656 | tf_op jit(solution)/shard_map/ppermute | solution.py:25
  56.6 1.8 %collective-permute-start.3 = (bf16[768,256]{1,0:T(8,128)(2,1)S(1)}, bf16[768,256]{1,0:T(8,128)(2,1)}, u32[]{:S(2)}, u32[]{:S(2)}) collective-permute-start(bf16[768,256]{1,0:T(8,128)(2,1)S(1)} %shard_map.225.refs_2_), channel_id=1, source_target_pairs={{0,24},{8,0},{16,8},{24,16},{1,25},{9,1},{17,9},{25,17},{2,26},{10... | collective-permute-start | bytes 1179656 | tf_op jit(solution)/shard_map/ppermute | solution.py:25
  58.4 1.4 %all-to-all-done.2.refs_0_ = bf16[8,24,512]{2,1,0:T(8,128)(2,1)S(1)} async-done(((bf16[8,24,512]{2,1,0:T(8,128)(2,1)}), bf16[8,24,512]{2,1,0:T(8,128)(2,1)S(1)}, u32[]{:S(2)}, u32[]{:S(2)}) %all-to-all-start.2) | async-done | bytes 196640 | tf_op jit(solution)/shard_map/all_to_all | solution.py:17
  59.8 0.0 copy-start.6
  59.8 0.9 copy-done.6
  60.7 0.7 shard_map.224
  61.4 0.0 copy-start.8
  61.4 4.0 %all-to-all-start.3 = ((bf16[8,24,512]{2,1,0:T(8,128)(2,1)}), bf16[8,24,512]{2,1,0:T(8,128)(2,1)}, u32[]{:S(2)}, u32[]{:S(2)}) async-start(bf16[8,24,512]{2,1,0:T(8,128)(2,1)} %get-tuple-element.19), calls=%async_computation.3 | async-start | bytes 393216 | tf_op jit(solution)/shard_map/all_to_all | solution.py:17
  65.5 0.0 copy-done.8
  65.5 0.0 copy-start.1
  65.5 0.0 copy-start.4
  65.5 0.0 copy-start.5
  65.5 4.5 %shard_map.226 = (f32[24,2,128,128]{3,2,1,0:T(8,128)}, f32[8,192]{1,0:T(8,128)}) custom-call(f32[24,256]{1,0:T(8,128)} %get-tuple-element.20.refs_0_, f32[24,256]{1,0:T(8,128)} %get-tuple-element.21.refs_1_, f32[24,128]{1,0:T(8,128)} %get-tuple-element.17.refs_1_.refs_2_, f32[24,2,128,128]{3,2,1,0:T(8,128)} %refs_3_.5, bf16[8,32,512]{2,1,0:T(8,128)(2,1)} %copy-done.3), custom_call_target="tpu_custom_call" | custom-call | flops 100000000 | tf_op jit(solution)/shard_map/pallas_call | solution.py:97
  70.1 0.0 collective-permute-done.5.refs_5_
  70.1 0.0 collective-permute-done.4.refs_4_
  70.1 5.7 %collective-permute-done.3.refs_3_ = bf16[768,256]{1,0:T(8,128)(2,1)} collective-permute-done((bf16[768,256]{1,0:T(8,128)(2,1)S(1)}, bf16[768,256]{1,0:T(8,128)(2,1)}, u32[]{:S(2)}, u32[]{:S(2)}) %collective-permute-start.3) | collective-permute-done | bytes 393248 | tf_op jit(solution)/shard_map/ppermute | solution.py:25
  75.8 0.1 all-to-all-done.3.refs_0_
  75.9 0.0 copy-done.2
  75.9 3.4 %shard_map.227 = bf16[4,4,104,256]{3,2,1,0:T(8,128)(2,1)S(1)} custom-call(bf16[8,24,512]{2,1,0:T(8,128)(2,1)} %all-to-all-done.3.refs_0_, f32[1,4096]{1,0:T(1,128)} %bitcast.29, bf16[768,256]{1,0:T(8,128)(2,1)} %copy-done.2, bf16[768,256]{1,0:T(8,128)(2,1)} %collective-permute-done.3.refs_3_, bf16[768,256]{1,0:T(8,128)(2,1)} %collective-permute-done.4.refs_4_, ...), custom_call_target="tpu_custom_call" | custom-call | flops 201326592 | tf_op jit(solution)/shard_map/pallas_call | solution.py:97
  79.4 19.9 %all_to_all.36 = bf16[16,104,256]{2,1,0:T(8,128)(2,1)S(1)} all-to-all(bf16[16,104,256]{2,1,0:T(8,128)(2,1)S(1)} %bitcast.21), channel_id=1, replica_groups=mesh['z'=8,'x'=4,'y'=4,'c'=2] {'x','y'}, dimensions={0} | all-to-all | bytes 1703936 | tf_op jit(solution)/shard_map/all_to_all | solution.py:17
  99.3 0.0 collective-permute-start.6
  99.3 2.4 %collective-permute-done.6 = bf16[16,104,256]{2,1,0:T(8,128)(2,1)S(1)} collective-permute-done((bf16[16,104,256]{2,1,0:T(8,128)(2,1)S(1)}, bf16[16,104,256]{2,1,0:T(8,128)(2,1)S(1)}, u32[]{:S(2)}, u32[]{:S(2)}) %collective-permute-start.6) | collective-permute-done | bytes 852000 | tf_op jit(solution)/shard_map/ppermute | solution.py:605
  101.7 0.0 copy-done.1
  101.7 0.0 copy-done.4
  101.7 0.0 copy-done.5
  101.7 1.6 %shard_map.228 = (bf16[4,5,24,512]{3,2,1,0:T(8,128)(2,1)S(1)}, bf16[96,128]{1,0:T(8,128)(2,1)S(1)}, bf16[4,24,128]{2,1,0:T(8,128)(2,1)S(1)}) custom-call(bf16[4,4,104,256]{3,2,1,0:T(8,128)(2,1)S(1)} %bitcast.20, bf16[4,4,104,256]{3,2,1,0:T(8,128)(2,1)S(1)} %bitcast.26, f32[1,4096]{1,0:T(1,128)} %bitcast.30, bf16[4096,128]{1,0:T(8,128)(2,1)S(1)} %bitcast.24, ...), custom_call_target="tpu_custom_call" | custom-call | flops 251658240 | tf_op jit(solution)/shard_map/pallas_call | solution.py:97
  103.2 0.0 copy-start.9
  103.3 0.2 collective-permute-start.7
  103.5 1.7 %collective-permute-done.7.refs_2_ = bf16[4,5,24,512]{3,2,1,0:T(8,128)(2,1)S(1)} collective-permute-done((bf16[4,5,24,512]{3,2,1,0:T(8,128)(2,1)S(1)}, bf16[4,5,24,512]{3,2,1,0:T(8,128)(2,1)S(1)}, u32[]{:S(2)}, u32[]{:S(2)}) %collective-permute-start.7) | collective-permute-done | bytes 491552 | tf_op jit(solution)/shard_map/ppermute | solution.py:623
  105.2 0.3 shard_map.229
  105.5 16.4 %all_to_all.37 = bf16[16,24,768]{2,1,0:T(8,128)(2,1)S(1)} all-to-all(bf16[16,24,768]{2,1,0:T(8,128)(2,1)S(1)} %bitcast.23), channel_id=1, replica_groups=mesh['z'=8,'x'=4,'y'=4,'c'=2] {'x','y'}, dimensions={0} | all-to-all | bytes 1179648 | tf_op jit(solution)/shard_map/all_to_all | solution.py:17
  121.9 1.5 %shard_map.230 = bf16[8,24,512]{2,1,0:T(8,128)(2,1)S(1)} custom-call(bf16[4,4,24,768]{3,2,1,0:T(8,128)(2,1)S(1)} %bitcast.22, f32[8,192]{1,0:T(8,128)} %get-tuple-element.22.refs_6_.refs_1_, bf16[768,256]{1,0:T(8,128)(2,1)} %copy-done.2, bf16[768,256]{1,0:T(8,128)(2,1)} %collective-permute-done.3.refs_3_, bf16[768,256]{1,0:T(8,128)(2,1)} %collective-permute-done.4.refs_4_, ...), custom_call_target="tpu_custom_call" | custom-call | flops 100663296 | tf_op jit(solution)/shard_map/pallas_call | solution.py:97
  123.4 12.2 %all_to_all.38.refs_0_ = bf16[8,24,512]{2,1,0:T(8,128)(2,1)S(1)} all-to-all(bf16[8,24,512]{2,1,0:T(8,128)(2,1)S(1)} %shard_map.230), channel_id=1, replica_groups=mesh['z'=8,'x'=4,'y'=4,'c'=2] {'z'}, dimensions={0} | all-to-all | bytes 393216 | tf_op jit(solution)/shard_map/all_to_all | solution.py:17
  135.5 0.0 copy-done.9
  135.5 0.6 shard_map.231
Async XLA Ops:
  0.6 44.9 %copy-start = (f32[24,2,128,128]{3,2,1,0:T(8,128)S(1)}, f32[24,2,128,128]{3,2,1,0:T(8,128)}, u32[]{:S(2)}) copy-start(f32[24,2,128,128]{3,2,1,0:T(8,128)} %refs_3_.5) | copy-start | bytes 9437188
  3.5 21.4 %all-to-all-start = ((bf16[8,32,512]{2,1,0:T(8,128)(2,1)}), bf16[8,32,512]{2,1,0:T(8,128)(2,1)S(1)}, u32[]{:S(2)}, u32[]{:S(2)}) async-start(bf16[8,32,512]{2,1,0:T(8,128)(2,1)} %get-tuple-element.15.refs_0_), calls=%async_computation | async-start | bytes 524288 | tf_op jit(solution)/shard_map/all_to_all | solution.py:17
  12.0 8.0 %collective-permute-start.2 = (bf16[128,768]{1,0:T(8,128)(2,1)}, bf16[128,768]{1,0:T(8,128)(2,1)S(1)}, u32[]{:S(2)}, u32[]{:S(2)}) collective-permute-start(bf16[128,768]{1,0:T(8,128)(2,1)} %get-tuple-element.16.refs_1_), channel_id=1, source_target_pairs={{0,8},{8,16},{16,24},{24,0},{1,9},{9,17},{17,25},{25,1},{2,10},{10... | collective-permute-start | bytes 589832 | tf_op jit(solution)/shard_map/ppermute | solution.py:25
  13.5 9.5 %collective-permute-start.1 = (bf16[128,768]{1,0:T(8,128)(2,1)}, bf16[128,768]{1,0:T(8,128)(2,1)S(1)}, u32[]{:S(2)}, u32[]{:S(2)}) collective-permute-start(bf16[128,768]{1,0:T(8,128)(2,1)} %get-tuple-element.16.refs_1_), channel_id=1, source_target_pairs={{0,16},{8,24},{16,0},{24,8},{1,17},{9,25},{17,1},{25,9},{2,18},{10... | collective-permute-start | bytes 589832 | tf_op jit(solution)/shard_map/ppermute | solution.py:25
  14.6 10.3 %collective-permute-start = (bf16[128,768]{1,0:T(8,128)(2,1)}, bf16[128,768]{1,0:T(8,128)(2,1)}, u32[]{:S(2)}, u32[]{:S(2)}) collective-permute-start(bf16[128,768]{1,0:T(8,128)(2,1)} %get-tuple-element.16.refs_1_), channel_id=1, source_target_pairs={{0,24},{8,0},{16,8},{24,16},{1,25},{9,1},{17,9},{25,17},{2,26},{10... | collective-permute-start | bytes 589832 | tf_op jit(solution)/shard_map/ppermute | solution.py:25
  20.0 3.0 %copy-start.10 = (bf16[128,768]{1,0:T(8,128)(2,1)}, bf16[128,768]{1,0:T(8,128)(2,1)S(1)}, u32[]{:S(2)}) copy-start(bf16[128,768]{1,0:T(8,128)(2,1)S(1)} %collective-permute-done.2.refs_4_) | copy-start | bytes 589828
  23.0 0.7 copy-start.11
  25.0 22.9 %copy-start.3 = (bf16[8,32,512]{2,1,0:T(8,128)(2,1)}, bf16[8,32,512]{2,1,0:T(8,128)(2,1)S(1)}, u32[]{:S(2)}) copy-start(bf16[8,32,512]{2,1,0:T(8,128)(2,1)S(1)} %all-to-all-done.refs_0_.refs_4_) | copy-start | bytes 786436
  47.8 0.7 copy-start.7
  48.5 11.3 %all-to-all-start.2 = ((bf16[8,24,512]{2,1,0:T(8,128)(2,1)}), bf16[8,24,512]{2,1,0:T(8,128)(2,1)S(1)}, u32[]{:S(2)}, u32[]{:S(2)}) async-start(bf16[8,24,512]{2,1,0:T(8,128)(2,1)} %copy-done.7), calls=%async_computation.2 | async-start | bytes 393216 | tf_op jit(solution)/shard_map/all_to_all | solution.py:17
  54.1 21.9 %copy-start.2 = (bf16[768,256]{1,0:T(8,128)(2,1)}, bf16[768,256]{1,0:T(8,128)(2,1)S(1)}, u32[]{:S(2)}) copy-start(bf16[768,256]{1,0:T(8,128)(2,1)S(1)} %shard_map.225.refs_2_) | copy-start | bytes 1179652
  54.1 16.0 %collective-permute-start.5 = (bf16[768,256]{1,0:T(8,128)(2,1)S(1)}, bf16[768,256]{1,0:T(8,128)(2,1)}, u32[]{:S(2)}, u32[]{:S(2)}) collective-permute-start(bf16[768,256]{1,0:T(8,128)(2,1)S(1)} %shard_map.225.refs_2_), channel_id=1, source_target_pairs={{0,8},{8,16},{16,24},{24,0},{1,9},{9,17},{17,25},{25,1},{2,10},{10... | collective-permute-start | bytes 1179656 | tf_op jit(solution)/shard_map/ppermute | solution.py:25
  54.3 15.8 %collective-permute-start.4 = (bf16[768,256]{1,0:T(8,128)(2,1)S(1)}, bf16[768,256]{1,0:T(8,128)(2,1)}, u32[]{:S(2)}, u32[]{:S(2)}) collective-permute-start(bf16[768,256]{1,0:T(8,128)(2,1)S(1)} %shard_map.225.refs_2_), channel_id=1, source_target_pairs={{0,16},{8,24},{16,0},{24,8},{1,17},{9,25},{17,1},{25,9},{2,18},{10... | collective-permute-start | bytes 1179656 | tf_op jit(solution)/shard_map/ppermute | solution.py:25
  56.6 19.2 %collective-permute-start.3 = (bf16[768,256]{1,0:T(8,128)(2,1)S(1)}, bf16[768,256]{1,0:T(8,128)(2,1)}, u32[]{:S(2)}, u32[]{:S(2)}) collective-permute-start(bf16[768,256]{1,0:T(8,128)(2,1)S(1)} %shard_map.225.refs_2_), channel_id=1, source_target_pairs={{0,24},{8,0},{16,8},{24,16},{1,25},{9,1},{17,9},{25,17},{2,26},{10... | collective-permute-start | bytes 1179656 | tf_op jit(solution)/shard_map/ppermute | solution.py:25
  59.8 0.9 copy-start.6
  61.4 4.0 %copy-start.8 = (f32[24,512]{1,0:T(8,128)}, f32[24,512]{1,0:T(8,128)S(1)}, u32[]{:S(2)}) copy-start(f32[24,512]{1,0:T(8,128)S(1)} %get-tuple-element.26.refs_1_) | copy-start | bytes 147460
  61.4 14.5 %all-to-all-start.3 = ((bf16[8,24,512]{2,1,0:T(8,128)(2,1)}), bf16[8,24,512]{2,1,0:T(8,128)(2,1)}, u32[]{:S(2)}, u32[]{:S(2)}) async-start(bf16[8,24,512]{2,1,0:T(8,128)(2,1)} %get-tuple-element.19), calls=%async_computation.3 | async-start | bytes 393216 | tf_op jit(solution)/shard_map/all_to_all | solution.py:17
  65.5 36.2 %copy-start.1 = (bf16[1,128,4096]{2,1,0:T(8,128)(2,1)S(1)}, bf16[1,128,4096]{2,1,0:T(8,128)(2,1)}, u32[]{:S(2)}) copy-start(bf16[1,128,4096]{2,1,0:T(8,128)(2,1)} %param.39) | copy-start | bytes 3145732
  65.5 36.2 %copy-start.4 = (bf16[1,4096,128]{2,1,0:T(8,128)(2,1)S(1)}, bf16[1,4096,128]{2,1,0:T(8,128)(2,1)}, u32[]{:S(2)}) copy-start(bf16[1,4096,128]{2,1,0:T(8,128)(2,1)} %param.37) | copy-start | bytes 3145732
  65.5 36.2 %copy-start.5 = (bf16[1,4096,128]{2,1,0:T(8,128)(2,1)S(1)}, bf16[1,4096,128]{2,1,0:T(8,128)(2,1)}, u32[]{:S(2)}) copy-start(bf16[1,4096,128]{2,1,0:T(8,128)(2,1)} %param.38) | copy-start | bytes 3145732
  99.3 2.4 %collective-permute-start.6 = (bf16[16,104,256]{2,1,0:T(8,128)(2,1)S(1)}, bf16[16,104,256]{2,1,0:T(8,128)(2,1)S(1)}, u32[]{:S(2)}, u32[]{:S(2)}) collective-permute-start(bf16[16,104,256]{2,1,0:T(8,128)(2,1)S(1)} %all_to_all.36), channel_id=1, source_target_pairs={{0,1},{1,0},{2,3},{3,2},{4,5},{5,4},{6,7},{7,6},{8,9},{9,8},{10,11... | collective-permute-start | bytes 2555912 | tf_op jit(solution)/shard_map/ppermute | solution.py:605
  103.2 32.3 %copy-start.9 = (f32[24,512]{1,0:T(8,128)S(1)}, f32[24,512]{1,0:T(8,128)}, u32[]{:S(2)}) copy-start(f32[24,512]{1,0:T(8,128)} %copy-done.8) | copy-start | bytes 147460
  103.3 2.0 %collective-permute-start.7 = (bf16[4,5,24,512]{3,2,1,0:T(8,128)(2,1)S(1)}, bf16[4,5,24,512]{3,2,1,0:T(8,128)(2,1)S(1)}, u32[]{:S(2)}, u32[]{:S(2)}) collective-permute-start(bf16[4,5,24,512]{3,2,1,0:T(8,128)(2,1)S(1)} %get-tuple-element.25), channel_id=1, source_target_pairs={{0,1},{1,0},{2,3},{3,2},{4,5},{5,4},{6,7},{7,6},{8,9},{9,8},{10,11... | collective-permute-start | bytes 1474568 | tf_op jit(solution)/shard_map/ppermute | solution.py:623
